TPU v7x, 256 devices: a whole 4x4x8 slice. The times are simulated.
256 devices in a mesh: sp: 32 (over z, y), tp: 8 (over x, core).
Axes of the slice: x: 4, y: 4, z: 8, core: 2. Of those that a mesh axis runs over, the one named last changes fastest.
Arguments:
- mixer_input: bfloat16 [4096, 1024], P('sp', 'tp'), may hold values from -1800 to 1800
- time_step: float32 [2, 64], P(None, 'tp'), may hold values from 0 to 2, as said below
- damping: float32 [2, 4096, 64], P(None, 'sp', 'tp'), may hold values from 0 to 2
- input_map: bfloat16 [2, 2, 64, 64, 16], P(None, None, 'tp'), may hold values from -1 to 1
- readout: float32 [2, 2, 64, 16, 64], P(None, None, 'tp'), may hold values from -0.5 to 0.5
- skip_gain: float32 [1024], P('tp'), may hold values from -4 to 4
- out_gain: float32 [1024], P('tp'), may hold values from 0.1 to 1.9
- out_weight: bfloat16 [1024, 2048], replicated, may hold values from -0.1875 to 0.1875
- residual: bfloat16 [4096, 2048], P(('sp', 'tp')), may hold values from -6 to 6
- channel_gain: float32 [2048], replicated, may hold values from 0.1 to 1.9
- value_weight: bfloat16 [2048, 6144], P('sp', 'tp'), may hold values from -0.125 to 0.125
- gate_weight: bfloat16 [2048, 6144], P('sp', 'tp'), may hold values from -0.125 to 0.125
- value_taps: float32 [3, 6144], P(None, 'tp'), may hold values from -3 to 3
- gate_taps: float32 [3, 6144], P(None, 'tp'), may hold values from -3 to 3
- down_weight: bfloat16 [6144, 2048], P('tp', 'sp'), may hold values from -0.078125 to 0.078125
Outputs:
- output: bfloat16 [4096, 2048], P(('sp', 'tp'))
Inputs may be any that keep to these rules, and one draw needn't show every extreme that they name: `time_step`: positive.
All inputs are finite; a program needn't handle non-finite values.
Results may differ from a plain program's by a relative error of at most 0.017.
Values may be sent and summed in bfloat16 or wider, within the bound.
No kernel may reach another device: no remote copies, remote signals or barrier semaphores. Data moves between devices by JAX's collectives and lax.ppermute only.
A program may use at most 64 MiB of HBM per device.

v0:
```python
import math

import jax
import jax.numpy as jnp
from jax import lax
from jax.sharding import PartitionSpec as P

norm_eps = 1e-06


def sent_to_all(array, axis):
    copies = jnp.broadcast_to(array, (lax.axis_size(axis), *array.shape))
    return lax.all_to_all(copies, axis, split_axis=0, concat_axis=0, tiled=True)


def collected_together(array, axis):
    leaves = jax.tree.leaves(array)
    sequence = sorted(range(len(leaves)), key=lambda k: -leaves[k].size)
    width = (1, *leaves[sequence[0]].shape)[-1]
    lines = [
        jnp.pad(leaves[k].reshape(-1), (0, -leaves[k].size % width)).reshape(-1, width)
        for k in sequence
    ]
    both, at, found = (sent_to_all(jnp.concatenate(lines), axis), 0, {})
    for k, line in zip(sequence, lines):
        share = both[:, at : at + len(line)].reshape(len(both), -1)
        found[k] = share[:, : leaves[k].size].reshape(-1, *leaves[k].shape)
        at += len(line)
    numbers = iter(range(len(leaves)))
    return jax.tree.map(lambda _: found[next(numbers)], array)


def folded_in_pairs(pieces, combine):
    while len(jax.tree.leaves(pieces)[0]) > 1:
        pieces = jax.vmap(combine)(
            *(jax.tree.map(lambda part: part[side::2], pieces) for side in (0, 1))
        )
    return jax.tree.map(lambda part: part[0], pieces)


def prefix(array, axis, combine, identity, reverse):
    size, position = (lax.axis_size(axis), lax.axis_index(axis))
    passed = jnp.arange(size) > position if reverse else jnp.arange(size) < position

    def kept(part, zero, own):
        part = jnp.where(
            passed.reshape(-1, *(1 for _ in own.shape)), part, jnp.asarray(zero, own.dtype)
        )
        return part[::-1] if reverse else part

    pieces = collected_together(array, axis)
    return folded_in_pairs(jax.tree.map(kept, pieces, identity, array), combine)


def rows_first(arrays, axis, dims):
    turned = [jnp.moveaxis(a, dim, 0) for a, dim in zip(arrays, dims)]
    widths = [t[0].size for t in turned]
    both = jnp.concatenate([t.reshape(-1, w) for t, w in zip(turned, widths)], axis=1)
    filled = lax.all_gather(both, axis, axis=0, tiled=True)
    tiles = jnp.split(filled, [sum(widths[:k]) for k in range(1, len(widths))], axis=1)
    return tuple(
        (
            jnp.moveaxis(b.reshape(-1, *t.shape[1:]), 0, dim)
            for b, t, dim in zip(tiles, turned, dims)
        )
    )


def over_copies(array, axis):
    everything = sent_to_all(array, axis)
    return jnp.sum(everything, axis=0)


def joined_along(tiles, dim):
    tiles = jnp.moveaxis(tiles, 0, dim)
    dims = tiles.shape
    return tiles.reshape(*dims[:dim], dims[dim] * dims[dim + 1], *dims[dim + 2 :])


def gather_directly(array, axis, dim):
    return joined_along(sent_to_all(array, axis), dim)


def with_halo(cells, sides, width):
    for axis, dim in sides:
        count = lax.axis_size(axis)
        ends = count - 1
        head = lax.slice_in_dim(cells, 0, width, axis=dim)
        tail = lax.slice_in_dim(cells, cells.shape[dim] - width, cells.shape[dim], axis=dim)
        cells = jnp.concatenate(
            [
                lax.ppermute(tail, axis, [(i, (i + 1) % count) for i in range(ends)]),
                cells,
                lax.ppermute(head, axis, [((i + 1) % count, i) for i in range(ends)]),
            ],
            axis=dim,
        )
    return cells


def cut_along(array, dim, size):
    dims = array.shape
    tiles = array.reshape(*dims[:dim], size, dims[dim] // size, *dims[dim + 1 :])
    return jnp.moveaxis(tiles, dim, 0)


def summed_on_arrival(array, axis, dim):
    tiles = cut_along(array, dim, lax.axis_size(axis))
    arrived = lax.all_to_all(tiles, axis, split_axis=0, concat_axis=0, tiled=True)
    return arrived.astype(jnp.float32).sum(axis=0)


def combine(earlier, latter):
    prod_real = latter[0] * earlier[0] - latter[1] * earlier[1]
    prod_imag = latter[0] * earlier[1] + latter[1] * earlier[0]
    sum_real = latter[0] * earlier[2] - latter[1] * earlier[3] + latter[2]
    sum_imag = latter[0] * earlier[3] + latter[1] * earlier[2] + latter[3]
    return (prod_real, prod_imag, sum_real, sum_imag)


def moved_rows(values, offset, filler_value, backward):
    filler = jnp.full((offset, values.shape[1]), filler_value, jnp.float32)
    if backward:
        return jnp.concatenate((values[offset:], filler), axis=0)
    return jnp.concatenate((filler, values[:-offset]), axis=0)


def prefix_rows(elements, backward):
    row_count = elements[0].shape[0]
    fills = (1.0, 0.0, 0.0, 0.0)
    offset = 1
    while offset < row_count:
        earlier = tuple(
            (moved_rows(elements[index], offset, fills[index], backward) for index in range(4))
        )
        elements = combine(earlier, elements)
        offset = offset * 2
    return elements


def mixer_branch(mixer_input, time_step, damping, input_map, readout):
    tok_rows = mixer_input.shape[0]
    group_count = time_step.shape[1]
    states = input_map.shape[3]
    channels = input_map.shape[4]
    flat_width = group_count * states
    frequency = math.pi * jnp.arange(states, dtype=jnp.float32)
    ones_narrow = jnp.eye(group_count, dtype=jnp.bfloat16)
    ones_wide = jnp.eye(group_count, dtype=jnp.float32)
    sign_pair = jnp.array([1.0, -1.0], jnp.float32)
    mixed_sum = jnp.zeros((tok_rows, group_count * channels), jnp.float32)
    for direction in range(2):
        step_size = time_step[direction]
        rotation = (step_size[:, None] * frequency[None, :]).reshape(flat_width)
        in_scale = jnp.repeat(jnp.sqrt(-jnp.expm1(-step_size)), states)
        magnitude = jnp.repeat(
            jnp.exp(-0.5 * step_size[None, :] - damping[direction]), states, axis=1
        )
        decay_real = magnitude * jnp.cos(rotation)[None, :]
        decay_imag = magnitude * jnp.sin(rotation)[None, :]
        in_block = jnp.einsum("pgnh,gk->ghpkn", input_map[direction], ones_narrow).reshape(
            group_count * channels, 2 * flat_width
        )
        projected = jnp.dot(mixer_input, in_block, preferred_element_type=jnp.float32)
        drive_real = projected[:, :flat_width] * in_scale[None, :]
        drive_imag = projected[:, flat_width:] * in_scale[None, :]
        backward = direction == 1
        scanned = prefix_rows((decay_real, decay_imag, drive_real, drive_imag), backward)
        last_row = 0 if backward else tok_rows - 1
        totals = (
            scanned[0][last_row],
            scanned[1][last_row],
            scanned[2][last_row],
            scanned[3][last_row],
        )
        zero_row = jnp.zeros((flat_width,), jnp.float32)
        identity = (jnp.ones((flat_width,), jnp.float32), zero_row, zero_row, zero_row)
        carried = prefix(totals, "sp", combine, identity, backward)
        state_real = (
            scanned[2] + scanned[0] * carried[2][None, :] - scanned[1] * carried[3][None, :]
        )
        state_imag = (
            scanned[3] + scanned[0] * carried[3][None, :] + scanned[1] * carried[2][None, :]
        )
        signed = readout[direction] * sign_pair[:, None, None, None]
        out_block = jnp.einsum("pghn,gk->pgnkh", signed, ones_wide).reshape(
            2 * flat_width, group_count * channels
        )
        both_parts = jnp.concatenate((state_real, state_imag), axis=1)
        mixed_sum = mixed_sum + jnp.dot(both_parts, out_block)
    return mixed_sum


def body(
    mixer_input,
    time_step,
    damping,
    input_map,
    readout,
    skip_gain,
    out_gain,
    out_weight,
    residual,
    channel_gain,
    value_weight,
    gate_weight,
    value_taps,
    gate_taps,
    down_weight,
):
    value_full, gate_full, down_full = rows_first(
        (value_weight, gate_weight, down_weight), "sp", (0, 0, 1)
    )
    tok_rows, local_width = mixer_input.shape
    tp_count = lax.axis_size("tp")
    mixed_y = mixer_branch(mixer_input, time_step, damping, input_map, readout)
    mixed_y = mixed_y + skip_gain[None, :] * mixer_input.astype(jnp.float32)
    square_sum = over_copies(jnp.sum(mixed_y * mixed_y, axis=1), "tp")
    inverse = lax.rsqrt(square_sum / (local_width * tp_count) + norm_eps)
    normed_mix = (mixed_y * inverse[:, None] * out_gain[None, :]).astype(jnp.bfloat16)
    token_block = lax.all_to_all(normed_mix, "tp", split_axis=0, concat_axis=1, tiled=True)
    mixed_rows = jnp.dot(token_block, out_weight, preferred_element_type=jnp.float32)
    hidden_state = (residual.astype(jnp.float32) + mixed_rows).astype(jnp.bfloat16)
    state_wide = hidden_state.astype(jnp.float32)
    scale_rows = lax.rsqrt(jnp.mean(state_wide * state_wide, axis=1, keepdims=True) + norm_eps)
    normed = (state_wide * scale_rows * channel_gain[None, :]).astype(jnp.bfloat16)
    block_rows = gather_directly(normed, "tp", 0)
    hidden_width = value_weight.shape[1]
    value_up = jnp.dot(block_rows, value_full, preferred_element_type=jnp.float32)
    gate_up = jnp.dot(block_rows, gate_full, preferred_element_type=jnp.float32)
    both_up = jnp.concatenate((value_up.astype(jnp.bfloat16), gate_up.astype(jnp.bfloat16)), axis=1)
    padded = with_halo(both_up, (("sp", 0),), 1)
    tap_table = jnp.concatenate((value_taps, gate_taps), axis=1)
    convolved = (
        tap_table[0] * padded[:-2].astype(jnp.float32)
        + tap_table[1] * padded[1:-1].astype(jnp.float32)
        + tap_table[2] * padded[2:].astype(jnp.float32)
    )
    hidden = (convolved[:, :hidden_width] * jax.nn.silu(convolved[:, hidden_width:])).astype(
        jnp.bfloat16
    )
    summed = summed_on_arrival(
        jnp.dot(hidden, down_full, preferred_element_type=jnp.float32).astype(jnp.bfloat16), "tp", 0
    )
    return (state_wide + summed).astype(jnp.bfloat16)


def solution(mesh):
    in_specs = (
        P("sp", "tp"),
        P(None, "tp"),
        P(None, "sp", "tp"),
        P(None, None, "tp", None, None),
        P(None, None, "tp", None, None),
        P("tp"),
        P("tp"),
        P(),
        P(("sp", "tp"), None),
        P(),
        P("sp", "tp"),
        P("sp", "tp"),
        P(None, "tp"),
        P(None, "tp"),
        P("tp", "sp"),
    )
    out_specs = P(("sp", "tp"), None)
    return jax.shard_map(body, mesh=mesh, in_specs=in_specs, out_specs=out_specs, check_vma=False)
```

profile of v0, /device:TPU:88, one launch (start us, length us, event | category | flops | bytes accessed | tf_op | source)
XLA Modules:
  0.0 160.0 jit_solution(956104621476776901)
XLA Ops:
  6.5 1.8 %pad_maximum_fusion.5 = bf16[64,2304]{1,0:T(8,128)(2,1)} fusion(bf16[64,768]{1,0:T(8,128)(2,1)} %bitcast.160, bf16[64,768]{1,0:T(8,128)(2,1)} %param.27, bf16[64,768]{1,0:T(8,128)(2,1)} %param.26), kind=kLoop, calls=%fused_computation.56 | loop fusion | flops 884736 | bytes 589824 | tf_op jit(solution)/shard_map/concatenate | solution.py:58
  8.3 0.8 slice_bitcast_fusion.2
  9.4 0.9 slice_bitcast_fusion
  10.7 0.3 reshape.158
  11.0 0.8 negate_sqrt_fusion
  11.9 1.0 convolution_bitcast_fusion
  13.7 0.2 subtract_add_fusion.2
  14.1 0.2 subtract_add_fusion.1
  14.6 0.2 subtract_add_fusion
  15.0 0.2 fusion.35
  15.4 0.2 fusion.47
  16.3 0.8 broadcast_in_dim.90
  17.0 10.6 %all-to-all-start.1 = ((f32[32,4,512]{2,1,0:T(4,128)}), f32[32,4,512]{2,1,0:T(4,128)S(1)}, u32[]{:S(2)}, u32[]{:S(2)}) async-start(f32[32,4,512]{2,1,0:T(4,128)} %broadcast_in_dim.90), calls=%async_computation.1 | async-start | bytes 524288 | tf_op jit(solution)/shard_map/all_to_all | solution.py:13
  27.7 0.3 reshape.151
  28.4 0.2 convolution_bitcast_fusion.1
  29.0 0.2 subtract_add_fusion.6
  29.3 0.2 subtract_add_fusion.5
  29.8 0.2 subtract_add_fusion.4
  30.2 0.2 fusion.29
  30.6 0.2 fusion.41
  31.4 0.3 copy-done.1
  32.0 0.3 multiply_bitcast_fusion
  32.2 1.1 reshape.156
  33.3 0.3 reshape.163
  33.7 5.9 %all-to-all-done.1 = f32[32,4,512]{2,1,0:T(4,128)S(1)} async-done(((f32[32,4,512]{2,1,0:T(4,128)}), f32[32,4,512]{2,1,0:T(4,128)S(1)}, u32[]{:S(2)}, u32[]{:S(2)}) %all-to-all-start.1) | async-done | bytes 262176 | tf_op jit(solution)/shard_map/all_to_all | solution.py:13
  39.6 0.8 broadcast_in_dim.84
  40.3 7.8 %all-to-all-start = ((f32[32,4,512]{2,1,0:T(4,128)}), f32[32,4,512]{2,1,0:T(4,128)S(1)}, u32[]{:S(2)}, u32[]{:S(2)}) async-start(f32[32,4,512]{2,1,0:T(4,128)} %broadcast_in_dim.84), calls=%async_computation | async-start | bytes 524288 | tf_op jit(solution)/shard_map/all_to_all | solution.py:13
  48.2 0.2 fusion.92
  50.1 7.8 %all-to-all-done = f32[32,4,512]{2,1,0:T(4,128)S(1)} async-done(((f32[32,4,512]{2,1,0:T(4,128)}), f32[32,4,512]{2,1,0:T(4,128)S(1)}, u32[]{:S(2)}, u32[]{:S(2)}) %all-to-all-start) | async-done | bytes 262176 | tf_op jit(solution)/shard_map/all_to_all | solution.py:13
  57.9 0.2 fusion.93
  59.2 0.2 fusion.18
  59.6 0.3 multiply_reduce_fusion.1
  59.9 9.6 %all_to_all.45 = f32[8,1,128]{2,1,0:T(1,128)S(1)} all-to-all(f32[8,1,128]{2,1,0:T(1,128)S(1)} %broadcast_in_dim.91), channel_id=1, replica_groups=mesh['sp'=32,'tp'=8] {'tp'}, dimensions={0} | all-to-all | bytes 8192 | tf_op jit(solution)/shard_map/all_to_all | solution.py:13
  69.6 7.8 %all_to_all.46 = bf16[8,16,128]{2,1,0:T(8,128)(2,1)S(1)} all-to-all(bf16[8,16,128]{2,1,0:T(8,128)(2,1)S(1)} %bitcast.159), channel_id=1, replica_groups=mesh['sp'=32,'tp'=8] {'tp'}, dimensions={0} | all-to-all | bytes 65536 | tf_op jit(solution)/shard_map/all_to_all | solution.py:221
  77.5 3.0 %multiply_reduce_fusion = (f32[16]{0:T(128)S(1)}, f32[16,2048]{1,0:T(8,128)S(1)}) fusion(bf16[1024,2048]{1,0:T(8,128)(2,1)} %param.23, bf16[16,2048]{1,0:T(8,128)(2,1)S(1)} %copy-done.3, bf16[8,16,128]{2,1,0:T(8,128)(2,1)S(1)} %all_to_all.46), kind=kOutput, calls=%fused_computation.172 | convolution fusion | flops 67305456 | bytes 4423744 | tf_op jit(solution)/shard_map/dot_general | solution.py:222
  80.6 0.9 broadcast_in_dim.92
  81.5 3.5 %all-to-all-start.4 = ((bf16[8,16,2048]{2,1,0:T(8,128)(2,1)}), bf16[8,16,2048]{2,1,0:T(8,128)(2,1)S(1)}, u32[]{:S(2)}, u32[]{:S(2)}) async-start(bf16[8,16,2048]{2,1,0:T(8,128)(2,1)} %broadcast_in_dim.92), calls=%async_computation.4 | async-start | bytes 1048576 | tf_op jit(solution)/shard_map/all_to_all | solution.py:13
  85.0 10.2 %all-to-all-done.4 = bf16[8,16,2048]{2,1,0:T(8,128)(2,1)S(1)} async-done(((bf16[8,16,2048]{2,1,0:T(8,128)(2,1)}), bf16[8,16,2048]{2,1,0:T(8,128)(2,1)S(1)}, u32[]{:S(2)}, u32[]{:S(2)}) %all-to-all-start.4) | async-done | bytes 524320 | tf_op jit(solution)/shard_map/all_to_all | solution.py:13
  95.2 20.6 %all-gather.2.cloned.1.call-done = bf16[2048,2304]{1,0:T(8,128)(2,1)} async-done(((bf16[64,2304]{1,0:T(8,128)(2,1)}), bf16[2048,2304]{1,0:T(8,128)(2,1)}) %all-gather.2.cloned.1.call-update) | async-done | bytes 9437200 | tf_op jit(solution)/shard_map/all_gather | solution.py:59
  115.8 2.5 %fusion.11 = bf16[128,768]{1,0:T(8,128)(2,1)S(1)} fusion(bf16[128,2048]{1,0:T(8,128)(2,1)S(1)} %bitcast.156, bf16[2048,2304]{1,0:T(8,128)(2,1)} %all-gather.2.cloned.1.call-done), kind=kOutput, calls=%fused_computation.12 | convolution fusion | flops 402751488 | bytes 3866624 | tf_op jit(solution)/shard_map/dot_general | solution.py:229
  118.3 2.5 %fusion.14 = bf16[128,768]{1,0:T(8,128)(2,1)S(1)} fusion(bf16[128,2048]{1,0:T(8,128)(2,1)S(1)} %bitcast.157, bf16[2048,2304]{1,0:T(8,128)(2,1)} %all-gather.2.cloned.1.call-done), kind=kOutput, calls=%fused_computation.13 | convolution fusion | flops 402751488 | bytes 3866624 | tf_op jit(solution)/shard_map/dot_general | solution.py:230
  120.9 6.2 %collective-permute-start = (bf16[1,1536]{1,0:T(2,128)(2,1)S(1)}, bf16[1,1536]{1,0:T(2,128)(2,1)S(1)}, u32[]{:S(2)}, u32[]{:S(2)}) collective-permute-start(bf16[1,1536]{1,0:T(2,128)(2,1)S(1)} %get-tuple-element.70), channel_id=1, source_target_pairs={{0,8},{8,16},{16,24},{24,32},{32,40},{40,48},{48,56},{56,64},{64,7... | collective-permute-start | bytes 9224 | tf_op jit(solution)/shard_map/ppermute | solution.py:92
  127.0 1.9 %collective-permute-start.1 = (bf16[1,1536]{1,0:T(2,128)(2,1)S(1)}, bf16[1,1536]{1,0:T(2,128)(2,1)S(1)}, u32[]{:S(2)}, u32[]{:S(2)}) collective-permute-start(bf16[1,1536]{1,0:T(2,128)(2,1)S(1)} %get-tuple-element.71), channel_id=1, source_target_pairs={{8,0},{16,8},{24,16},{32,24},{40,32},{48,40},{56,48},{64,56},{72,6... | collective-permute-start | bytes 9224 | tf_op jit(solution)/shard_map/ppermute | solution.py:94
  129.0 5.6 %collective-permute-done.1 = bf16[1,1536]{1,0:T(2,128)(2,1)S(1)} collective-permute-done((bf16[1,1536]{1,0:T(2,128)(2,1)S(1)}, bf16[1,1536]{1,0:T(2,128)(2,1)S(1)}, u32[]{:S(2)}, u32[]{:S(2)}) %collective-permute-start.1) | collective-permute-done | bytes 3104 | tf_op jit(solution)/shard_map/ppermute | solution.py:94
  134.7 0.3 multiply_add_fusion
  135.0 3.1 %fusion.6 = bf16[128,2048]{1,0:T(8,128)(2,1)S(1)} fusion(bf16[2048,2304]{1,0:T(8,128)(2,1)} %all-gather.2.cloned.1.call-done, f32[128,1536]{1,0:T(8,128)S(1)} %multiply_add_fusion), kind=kOutput, calls=%fused_computation.6 | convolution fusion | flops 403505152 | bytes 4456448 | tf_op jit(solution)/shard_map/dot_general | solution.py:243
  138.0 14.4 %all_to_all.47 = bf16[8,16,2048]{2,1,0:T(8,128)(2,1)S(1)} all-to-all(bf16[8,16,2048]{2,1,0:T(8,128)(2,1)S(1)} %bitcast.158), channel_id=1, replica_groups=mesh['sp'=32,'tp'=8] {'tp'}, dimensions={0} | all-to-all | bytes 1048576 | tf_op jit(solution)/shard_map/all_to_all | solution.py:109
  152.5 0.6 add_convert_fusion
  (223 shorter events, 8.1 us)
Async XLA Ops:
  6.5 6.5 %copy-start.7 = (f32[2,128,8]{1,2,0:T(8,128)S(1)}, f32[2,128,8]{1,2,0:T(8,128)}, u32[]{:S(2)}) copy-start(f32[2,128,8]{1,2,0:T(8,128)} %param.18) | copy-start | bytes 24580
  6.5 109.3 %all-gather.2.cloned.1.call-start = ((), (), s32[]{:S(2)}) async-start(), calls=%async_computation.6 | async-start | bytes 9732096 | tf_op jit(solution)/shard_map/all_gather | solution.py:59
  15.8 12.6 %copy-start.2 = (bf16[128,128]{1,0:T(8,128)(2,1)S(1)}, bf16[128,128]{1,0:T(8,128)(2,1)}, u32[]{:S(2)}) copy-start(bf16[128,128]{1,0:T(8,128)(2,1)} %param.16) | copy-start | bytes 98308
  17.0 22.6 %all-to-all-start.1 = ((f32[32,4,512]{2,1,0:T(4,128)}), f32[32,4,512]{2,1,0:T(4,128)S(1)}, u32[]{:S(2)}, u32[]{:S(2)}) async-start(f32[32,4,512]{2,1,0:T(4,128)} %broadcast_in_dim.90), calls=%async_computation.1 | async-start | bytes 524288 | tf_op jit(solution)/shard_map/all_to_all | solution.py:13
  30.8 1.0 copy-start.1
  30.8 0.9 copy-start.9
  33.7 25.5 %copy-start = (bf16[1024,128]{0,1:T(8,128)(2,1)S(1)}, bf16[1024,128]{0,1:T(8,128)(2,1)}, u32[]{:S(2)}) copy-start(bf16[1024,128]{0,1:T(8,128)(2,1)} %reshape.156) | copy-start | bytes 786436
  40.3 17.5 %all-to-all-start = ((f32[32,4,512]{2,1,0:T(4,128)}), f32[32,4,512]{2,1,0:T(4,128)S(1)}, u32[]{:S(2)}, u32[]{:S(2)}) async-start(f32[32,4,512]{2,1,0:T(4,128)} %broadcast_in_dim.84), calls=%async_computation | async-start | bytes 524288 | tf_op jit(solution)/shard_map/all_to_all | solution.py:13
  48.5 11.1 %copy-start.10 = (f32[128]{0:T(128)S(1)}, f32[128]{0:T(128)}, u32[]{:S(2)}) copy-start(f32[128]{0:T(128)} %param.21) | copy-start | bytes 1540
  49.2 20.4 %copy-start.8 = (f32[128]{0:T(128)S(1)}, f32[128]{0:T(128)}, u32[]{:S(2)}) copy-start(f32[128]{0:T(128)} %param.22) | copy-start | bytes 1540
  49.4 28.1 %copy-start.3 = (bf16[16,2048]{1,0:T(8,128)(2,1)S(1)}, bf16[16,2048]{1,0:T(8,128)(2,1)}, u32[]{:S(2)}) copy-start(bf16[16,2048]{1,0:T(8,128)(2,1)} %param.24) | copy-start | bytes 196612
  59.0 21.5 %copy-start.6 = (f32[2048]{0:T(1024)S(1)}, f32[2048]{0:T(1024)}, u32[]{:S(2)}) copy-start(f32[2048]{0:T(1024)} %param.25) | copy-start | bytes 24580
  59.4 25.6 %copy-start.4 = (f32[3,768]{1,0:T(4,128)S(1)}, f32[3,768]{1,0:T(4,128)}, u32[]{:S(2)}) copy-start(f32[3,768]{1,0:T(4,128)} %param.28) | copy-start | bytes 27652
  59.4 25.6 %copy-start.5 = (f32[3,768]{1,0:T(4,128)S(1)}, f32[3,768]{1,0:T(4,128)}, u32[]{:S(2)}) copy-start(f32[3,768]{1,0:T(4,128)} %param.29) | copy-start | bytes 27652
  81.5 13.7 %all-to-all-start.4 = ((bf16[8,16,2048]{2,1,0:T(8,128)(2,1)}), bf16[8,16,2048]{2,1,0:T(8,128)(2,1)S(1)}, u32[]{:S(2)}, u32[]{:S(2)}) async-start(bf16[8,16,2048]{2,1,0:T(8,128)(2,1)} %broadcast_in_dim.92), calls=%async_computation.4 | async-start | bytes 1048576 | tf_op jit(solution)/shard_map/all_to_all | solution.py:13
  120.9 8.2 %collective-permute-start = (bf16[1,1536]{1,0:T(2,128)(2,1)S(1)}, bf16[1,1536]{1,0:T(2,128)(2,1)S(1)}, u32[]{:S(2)}, u32[]{:S(2)}) collective-permute-start(bf16[1,1536]{1,0:T(2,128)(2,1)S(1)} %get-tuple-element.70), channel_id=1, source_target_pairs={{0,8},{8,16},{16,24},{24,32},{32,40},{40,48},{48,56},{56,64},{64,7... | collective-permute-start | bytes 9224 | tf_op jit(solution)/shard_map/ppermute | solution.py:92
  127.0 7.6 %collective-permute-start.1 = (bf16[1,1536]{1,0:T(2,128)(2,1)S(1)}, bf16[1,1536]{1,0:T(2,128)(2,1)S(1)}, u32[]{:S(2)}, u32[]{:S(2)}) collective-permute-start(bf16[1,1536]{1,0:T(2,128)(2,1)S(1)} %get-tuple-element.71), channel_id=1, source_target_pairs={{8,0},{16,8},{24,16},{32,24},{40,32},{48,40},{56,48},{64,56},{72,6... | collective-permute-start | bytes 9224 | tf_op jit(solution)/shard_map/ppermute | solution.py:94
Sparse Core Ops, SparseCore 0:
  9.9 105.8 all-gather.1
where the time goes:
time: 161 us; the launch traced here: 160 us
  waiting for transfers between devices  50.1 us (31%)
  blocking collectives  31.8 us (20%)
  starting transfers between devices  30 us (19%)
  between operations  14.7 us (9%)
  matrix products  12.8 us (8%)
  other arithmetic  10.3 us (6%)
  local copies, waits for them, and re-layouts  10.2 us (6%)
    all_to_all x3, waiting for transfers between devices, sent_to_all(): return lax.all_to_all(copies, axis, split_axis=0, concat_axis=0, tiled=True)  23.8 us
    all_to_all x3, starting transfers between devices, sent_to_all(): return lax.all_to_all(copies, axis, split_axis=0, concat_axis=0, tiled=True)  21.9 us
    all_gather x1, waiting for transfers between devices, rows_first(): filled = lax.all_gather(both, axis, axis=0, tiled=True)  20.6 us
    all_to_all x1, blocking collectives, summed_on_arrival(): lax.all_to_all(tiles, axis, split_axis=0, concat_axis=0, tiled=True)  14.4 us
    all_to_all x1, blocking collectives, sent_to_all(): return lax.all_to_all(copies, axis, split_axis=0, concat_axis=0, tiled=True)  9.62 us
    all_to_all x1, blocking collectives, body(): lax.all_to_all(normed_mix, 'tp', split_axis=0, concat_axis=1, tiled=True)  7.82 us
    ppermute x1, starting transfers between devices, with_halo(): lax.ppermute(tail, axis, [(i, (i + 1) % count) for i in range(ends)])  6.18 us
    ppermute x1, waiting for transfers between devices, with_halo(): lax.ppermute(head, axis, [((i + 1) % count, i) for i in range(ends)])  5.63 us
  transfers between devices with their start and end apart: 6, of which 5 were waited for; matrix products, arithmetic and copies ran while one was open for 14% of the time, Pallas kernels for 0%

commit v1 on v0

v1 whole, which is shorter than its diff:
```python
import math

import jax
import jax.numpy as jnp
from jax import lax
from jax.experimental import pallas as pl
from jax.experimental.pallas import tpu as pltpu
from jax.sharding import Mesh
from jax.sharding import PartitionSpec as P


norm_eps = 1e-06
SP = ("z", "yh", "yl")
TP = ("x", "c")
VMEM = pl.BlockSpec(memory_space=pltpu.VMEM)
SMEM = pl.BlockSpec(memory_space=pltpu.SMEM)


def shifted(array, axis, step):
    n = lax.axis_size(axis)
    return lax.ppermute(array, axis, [(i, (i + step) % n) for i in range(n)])


def sent_to_all(array, axis):
    copies = jnp.broadcast_to(array, (lax.axis_size(axis), *array.shape))
    return lax.all_to_all(copies, axis, split_axis=0, concat_axis=0, tiled=True)


def step_decays(table, damp_ref):
    rows = damp_ref.shape[2]
    half = damp_ref.shape[1], rows
    fwd = jnp.exp(-jnp.broadcast_to(table[3][:, :1], half) - damp_ref[0])
    bwd = jnp.exp(-jnp.broadcast_to(table[3][:, 64:65], half) - damp_ref[1])
    return fwd, bwd


def local_kernel(x_ref, table_ref, damp_ref, map_ref, end_ref, dre_ref, dim_ref):
    rows = x_ref.shape[0]
    groups = map_ref.shape[2]
    width = map_ref.shape[3]
    x = x_ref[...]
    scale = table_ref[2]
    owner = lax.broadcasted_iota(jnp.int32, (groups * width, 256), 0) // width
    for g in range(groups):
        block = jnp.concatenate(
            [map_ref[0, 0, g], map_ref[1, 0, g], map_ref[0, 1, g], map_ref[1, 1, g]], axis=1
        ).astype(jnp.float32)
        block = jnp.concatenate([block] * groups, axis=0)
        block = jnp.where(owner == g, block, 0.0).astype(jnp.bfloat16)
        drive = jnp.dot(x, block, preferred_element_type=jnp.float32)
        dre_ref[:, g, :] = drive[:, :128] * scale[g : g + 1, :]
        dim_ref[:, g, :] = drive[:, 128:] * scale[g : g + 1, :]
    cos, sin = table_ref[0], table_ref[1]
    lane_fwd = lax.broadcasted_iota(jnp.int32, (groups, 128), 1) < 64
    fwd, bwd = step_decays(table_ref, damp_ref)
    real = jnp.zeros((groups, 128), jnp.float32)
    imag = jnp.zeros((groups, 128), jnp.float32)
    for i in range(rows):
        j = rows - 1 - i
        size = jnp.where(
            lane_fwd,
            jnp.broadcast_to(fwd[:, i : i + 1], (groups, 128)),
            jnp.broadcast_to(bwd[:, j : j + 1], (groups, 128)),
        )
        dec_re, dec_im = size * cos, size * sin
        drive_re = jnp.where(lane_fwd, dre_ref[i], dre_ref[j])
        drive_im = jnp.where(lane_fwd, dim_ref[i], dim_ref[j])
        real, imag = (
            dec_re * real - dec_im * imag + drive_re,
            dec_re * imag + dec_im * real + drive_im,
        )
    total = jnp.sum(damp_ref[...], axis=2, keepdims=True)
    total = jnp.where(
        lane_fwd,
        jnp.broadcast_to(total[0], (groups, 128)),
        jnp.broadcast_to(total[1], (groups, 128)),
    )
    end_ref[:, :128] = real
    end_ref[:, 128:256] = imag
    end_ref[:, 256:] = total + rows * table_ref[3]


def mix_kernel(
    at_ref,
    ends_ref,
    dre_ref,
    dim_ref,
    table_ref,
    damp_ref,
    read_ref,
    x_ref,
    skip_ref,
    gain_ref,
    out_ref,
    fre_ref,
    fim_ref,
    bre_ref,
    bim_ref,
):
    rows = x_ref.shape[0]
    groups = dre_ref.shape[1]
    blocks = ends_ref.shape[0]
    at = at_ref[0]
    cos, sin = table_ref[0], table_ref[1]
    lane_fwd = lax.broadcasted_iota(jnp.int32, (groups, 128), 1) < 64
    block_re, block_im = cos, sin
    power = 1
    while power < rows:
        block_re, block_im = block_re * block_re - block_im * block_im, 2.0 * block_re * block_im
        power *= 2
    real = jnp.zeros((groups, 128), jnp.float32)
    imag = jnp.zeros((groups, 128), jnp.float32)
    for i in range(blocks):
        j = blocks - 1 - i
        part = jnp.where(lane_fwd, ends_ref[i, :, 256:], ends_ref[j, :, 256:])
        size = jnp.exp(-part)
        dec_re, dec_im = size * block_re, size * block_im
        end_re = jnp.where(lane_fwd, ends_ref[i, :, :128], ends_ref[j, :, :128])
        end_im = jnp.where(lane_fwd, ends_ref[i, :, 128:256], ends_ref[j, :, 128:256])
        next_re = dec_re * real - dec_im * imag + end_re
        next_im = dec_re * imag + dec_im * real + end_im
        keep_fwd = jnp.where(i < at, 1, 0)
        keep_bwd = jnp.where(j > at, 1, 0)
        keep = jnp.where(lane_fwd, keep_fwd, keep_bwd) == 1
        real = jnp.where(keep, next_re, real)
        imag = jnp.where(keep, next_im, imag)
    fwd, bwd = step_decays(table_ref, damp_ref)
    for i in range(rows):
        j = rows - 1 - i
        size = jnp.where(
            lane_fwd,
            jnp.broadcast_to(fwd[:, i : i + 1], (groups, 128)),
            jnp.broadcast_to(bwd[:, j : j + 1], (groups, 128)),
        )
        dec_re, dec_im = size * cos, size * sin
        drive_re = jnp.where(lane_fwd, dre_ref[i], dre_ref[j])
        drive_im = jnp.where(lane_fwd, dim_ref[i], dim_ref[j])
        real, imag = (
            dec_re * real - dec_im * imag + drive_re,
            dec_re * imag + dec_im * real + drive_im,
        )
        fre_ref[i] = real
        fim_ref[i] = imag
        bre_ref[j] = real
        bim_ref[j] = imag
    width = read_ref.shape[3]
    channels = groups * width
    table = jnp.concatenate(
        [
            read_ref[0, 0].reshape(channels, 64),
            read_ref[1, 0].reshape(channels, 64),
            -read_ref[0, 1].reshape(channels, 64),
            -read_ref[1, 1].reshape(channels, 64),
        ],
        axis=1,
    )
    owner = lax.broadcasted_iota(jnp.int32, (channels, 256), 0) // width
    row_fwd = lax.broadcasted_iota(jnp.int32, (rows, 128), 1) < 64
    mixed = skip_ref[...] * x_ref[...].astype(jnp.float32)
    for g in range(groups):
        state = jnp.concatenate(
            [
                jnp.where(row_fwd, fre_ref[:, g, :], bre_ref[:, g, :]),
                jnp.where(row_fwd, fim_ref[:, g, :], bim_ref[:, g, :]),
            ],
            axis=1,
        ).astype(jnp.bfloat16)
        part = jnp.where(owner == g, table, 0.0).astype(jnp.bfloat16)
        mixed = mixed + lax.dot_general(
            state, part, (((1,), (1,)), ((), ())), preferred_element_type=jnp.float32
        )
    parts = out_ref.shape[0]
    own = rows // parts
    for p in range(parts):
        out_ref[p, :own, :] = mixed[p * own : (p + 1) * own, :]
        out_ref[p, own:, :] = jnp.broadcast_to(gain_ref[...], (8, channels))


def mixer_branch(mixer_input, time_step, damping, input_map, readout, skip_gain, out_gain):
    rows = mixer_input.shape[0]
    groups = time_step.shape[1]
    states = input_map.shape[3]
    frequency = math.pi * jnp.arange(states, dtype=jnp.float32)
    step = time_step.T[:, :, None]
    shape = (groups, 2, states)
    rotation = step * frequency
    table = jnp.stack(
        [
            jnp.cos(rotation),
            jnp.sin(rotation),
            jnp.broadcast_to(jnp.sqrt(-jnp.expm1(-step)), shape),
            jnp.broadcast_to(0.5 * step, shape),
        ]
    ).reshape(4, groups, 2 * states)
    damp = jnp.swapaxes(damping, 1, 2)
    maps = jnp.swapaxes(input_map, 3, 4)
    drive_shape = jax.ShapeDtypeStruct((rows, groups, 2 * states), jnp.float32)
    ends, drive_re, drive_im = pl.pallas_call(
        local_kernel,
        out_shape=(
            jax.ShapeDtypeStruct((groups, 6 * states), jnp.float32),
            drive_shape,
            drive_shape,
        ),
        in_specs=[VMEM] * 4,
        out_specs=(VMEM,) * 3,
        name="mixer_local",
        cost_estimate=pl.CostEstimate(
            flops=300_000_000, bytes_accessed=2_000_000, transcendentals=0
        ),
    )(mixer_input, table, damp, maps)
    all_ends = sent_to_all(ends, SP)
    at = lax.axis_index(SP).astype(jnp.int32).reshape(1)
    scratch = pltpu.VMEM((rows, groups, 2 * states), jnp.float32)
    parts = lax.axis_size(TP)
    return pl.pallas_call(
        mix_kernel,
        out_shape=jax.ShapeDtypeStruct(
            (parts, rows // parts + 8, mixer_input.shape[1]), jnp.float32
        ),
        in_specs=[SMEM] + [VMEM] * 9,
        out_specs=VMEM,
        scratch_shapes=[scratch] * 4,
        name="mixer_out",
        cost_estimate=pl.CostEstimate(
            flops=300_000_000, bytes_accessed=2_000_000, transcendentals=0
        ),
    )(
        at,
        all_ends,
        drive_re,
        drive_im,
        table,
        damp,
        readout,
        mixer_input,
        skip_gain[None, :],
        out_gain[None, :],
    )


def z_ring(block):
    found = {0: block}
    up = down = block
    for s in range(1, 4):
        up = shifted(up, "z", 1)
        down = shifted(down, "z", -1)
        found[8 - s], found[s] = up, down
    half = block.shape[0] // 2
    far_up = shifted(up[:half], "z", 1)
    found[4] = (far_up, shifted(down[half:], "z", -1))
    return found


def edge_rows(cells):
    last = cells.shape[1] - 1
    edges = jnp.concatenate((cells[0, :1], cells[0, last:], cells[1, :1], cells[1, last:]))
    near = lax.ppermute(edges, "yl", [(0, 1), (1, 0)])
    count = lax.axis_size("z")
    pairs = [(2 * i + 1, 2 * i + 2) for i in range(count - 1)]
    far = lax.ppermute(
        jnp.where(lax.axis_index("yl") == 0, edges[:1], edges[3:]),
        ("z", "yl"),
        pairs + [(j, i) for i, j in pairs],
    )
    return near, far


def ffn_kernel(at_ref, cells_ref, near_ref, far_ref, vtap_ref, gtap_ref, *refs):
    line = refs[:9]
    out_ref, whole_ref, rows_ref = refs[9:]
    z, low = at_ref[0], at_ref[1]
    tok = cells_ref.shape[1]
    total = tok + 16
    width = vtap_ref.shape[1]
    cut = line[0].shape[0]
    for ref in range(9):
        size = line[ref].shape[0]
        start = lax.rem(z + (ref if ref < 5 else ref - 1), 8) * cut
        if ref == 5:
            start = start + cut // 2
        whole_ref[pl.ds(pl.multiple_of(start, cut // 2), size), :] = line[ref][...]
    row = lax.broadcasted_iota(jnp.int32, (16, cells_ref.shape[2]), 0)
    even = jnp.full(row.shape, low, jnp.int32) == 0
    near = [
        jnp.broadcast_to(near_ref[k : k + 1, :].astype(jnp.float32), row.shape) for k in range(4)
    ]
    far = jnp.broadcast_to(far_ref[...].astype(jnp.float32), row.shape)
    sides = (
        (jnp.where(even, near[0], near[2]), jnp.where(even, far, near[1])),
        (jnp.where(even, near[2], far), jnp.where(even, near[1], near[3])),
    )
    for k in range(2):
        after, before = sides[k]
        tile = jnp.where(row == 0, after, jnp.where(row == 1, before, 0.0))
        rows_ref[k * total : k * total + tok, :] = cells_ref[k]
        rows_ref[k * total + tok : (k + 1) * total, :] = tile.astype(jnp.bfloat16)
    both = jnp.dot(
        rows_ref[...], whole_ref[:, : 2 * width], preferred_element_type=jnp.float32
    )
    both = both.astype(jnp.bfloat16).astype(jnp.float32)

    def convolved(up, taps):
        mid, after, before = up[:tok], up[tok : tok + 1], up[tok + 1 : tok + 2]
        at = lax.broadcasted_iota(jnp.int32, mid.shape, 0)
        prev = jnp.where(at == 0, jnp.broadcast_to(before, mid.shape), pltpu.roll(mid, 1, 0))
        foll = jnp.where(
            at == tok - 1, jnp.broadcast_to(after, mid.shape), pltpu.roll(mid, tok - 1, 0)
        )
        return taps[0:1] * prev + taps[1:2] * mid + taps[2:3] * foll

    hidden = []
    for k in range(2):
        part = both[k * total : (k + 1) * total]
        value = convolved(part[:, :width], vtap_ref[...])
        gate = convolved(part[:, width:], gtap_ref[...])
        hidden.append((value * (gate / (1.0 + jnp.exp(-gate)))).astype(jnp.bfloat16))
    sums = lax.dot_general(
        jnp.concatenate(hidden, axis=0),
        whole_ref[:, 2 * width :],
        (((1,), (1,)), ((), ())),
        preferred_element_type=jnp.float32,
    ).astype(jnp.bfloat16)
    own = out_ref.shape[1]
    for p in range(out_ref.shape[0]):
        out_ref[p] = sums[p * own : (p + 1) * own]


def body(
    mixer_input,
    time_step,
    damping,
    input_map,
    readout,
    skip_gain,
    out_gain,
    out_weight,
    residual,
    channel_gain,
    value_weight,
    gate_weight,
    value_taps,
    gate_taps,
    down_weight,
):
    half = value_weight.shape[1] // 2
    halves = [
        jnp.concatenate((value_weight[:, cut], gate_weight[:, cut], down_weight.T[:, cut]), axis=1)
        for cut in (slice(0, half), slice(half, 2 * half))
    ]
    crossed = lax.all_to_all(
        jnp.stack((halves[0], halves[0], halves[1], halves[1])), ("yh", "yl"), 0, 0, tiled=True
    )
    pieces = z_ring(crossed.reshape(-1, 3 * half))
    mixed_y = mixer_branch(
        mixer_input, time_step, damping, input_map, readout, skip_gain, out_gain
    )
    tok_rows, local_width = mixer_input.shape
    tp_count = lax.axis_size(TP)
    own_rows = tok_rows // tp_count
    arrived = lax.all_to_all(mixed_y, TP, 0, 0, tiled=True)
    gains = arrived[:, own_rows].reshape(tp_count * local_width)
    rows_y = jnp.moveaxis(arrived[:, :own_rows], 0, 1).reshape(own_rows, tp_count * local_width)
    inverse = lax.rsqrt(jnp.mean(rows_y * rows_y, axis=1, keepdims=True) + norm_eps)
    token_block = (rows_y * inverse * gains[None, :]).astype(jnp.bfloat16)
    mixed_rows = jnp.dot(token_block, out_weight, preferred_element_type=jnp.float32)
    hidden_state = (residual.astype(jnp.float32) + mixed_rows).astype(jnp.bfloat16)
    state_wide = hidden_state.astype(jnp.float32)
    scale_rows = lax.rsqrt(jnp.mean(state_wide * state_wide, axis=1, keepdims=True) + norm_eps)
    normed = (state_wide * scale_rows * channel_gain[None, :]).astype(jnp.bfloat16)
    model = normed.shape[1]
    cells = sent_to_all(normed, ("yh", *TP)).reshape(2, tok_rows, model)
    near, far = edge_rows(cells)
    place = jnp.stack([lax.axis_index("z"), lax.axis_index("yl")]).astype(jnp.int32)
    shift = lax.axis_index("yh") * half
    taps = [lax.dynamic_slice(t, (0, shift), (3, half)) for t in (value_taps, gate_taps)]
    ordered = [*(pieces[d] for d in range(4)), *pieces[4], *(pieces[d] for d in range(5, 8))]
    partial = pl.pallas_call(
        ffn_kernel,
        out_shape=jax.ShapeDtypeStruct((2 * tp_count, own_rows, model), jnp.bfloat16),
        in_specs=[SMEM] + [VMEM] * (5 + len(ordered)),
        out_specs=VMEM,
        scratch_shapes=[
            pltpu.VMEM((model, 3 * half), jnp.bfloat16),
            pltpu.VMEM((2 * (tok_rows + 16), model), jnp.bfloat16),
        ],
        name="ffn",
        cost_estimate=pl.CostEstimate(
            flops=1_300_000_000, bytes_accessed=6_000_000, transcendentals=100_000
        ),
    )(place, cells, near, far, *taps, *ordered)
    parts = lax.all_to_all(partial, ("yh", *TP), 0, 0, tiled=True)
    summed = parts.astype(jnp.float32).sum(axis=0)
    return (state_wide + summed).astype(jnp.bfloat16)


def solution(mesh):
    fine = Mesh(mesh.devices.reshape(8, 2, 2, 4, 2), ("z", "yh", "yl", "x", "c"))
    in_specs = (
        P(SP, TP),
        P(None, TP),
        P(None, SP, TP),
        P(None, None, TP, None, None),
        P(None, None, TP, None, None),
        P(TP),
        P(TP),
        P(),
        P((*SP, *TP), None),
        P(),
        P(SP, TP),
        P(SP, TP),
        P(None, TP),
        P(None, TP),
        P(TP, SP),
    )
    out_specs = P((*SP, *TP), None)

    return jax.shard_map(body, mesh=fine, in_specs=in_specs, out_specs=out_specs, check_vma=False)
```

time: 161 us -> 139 us (0.86)
  the two profiles are of different devices: /device:TPU:88 before, /device:TPU:1 now
where the time goes in v1:
time: 139 us; the launch traced here: 138 us
  waiting for transfers between devices  45.5 us (33%)
  starting transfers between devices  39.7 us (29%)
  blocking collectives  24.6 us (18%)
  Pallas kernels  13 us (9%)
  local copies, waits for them, and re-layouts  7.97 us (6%)
  other arithmetic  3.95 us (3%)
  matrix products  3 us (2%)
    ppermute x8, waiting for transfers between devices, shifted(): return lax.ppermute(array, axis, [(i, (i + step) % n) for i in range(n)])  27.1 us
    all_to_all x1, blocking collectives, body(): parts = lax.all_to_all(partial, ('yh', *TP), 0, 0, tiled=True)  24.6 us
    all_to_all x2, starting transfers between devices, sent_to_all(): return lax.all_to_all(copies, axis, split_axis=0, concat_axis=0, tiled=True)  16.3 us
    ppermute x8, starting transfers between devices, shifted(): return lax.ppermute(array, axis, [(i, (i + step) % n) for i in range(n)])  10.8 us
    all_to_all x2, waiting for transfers between devices, sent_to_all(): return lax.all_to_all(copies, axis, split_axis=0, concat_axis=0, tiled=True)  10.4 us
    all_to_all x1, starting transfers between devices, body(): arrived = lax.all_to_all(mixed_y, TP, 0, 0, tiled=True)  7.87 us
    pallas_call x1, Pallas kernels, body(): pl.pallas_call(ffn_kernel, out_shape=jax.ShapeDtypeStruct((2 * tp_count,...  6.4 us
    pallas_call x1, Pallas kernels, mixer_branch(): pl.pallas_call(mix_kernel, out_shape=jax.ShapeDtypeStruct((parts, rows //...  3.75 us
  transfers between devices with their start and end apart: 14, of which 8 were waited for; matrix products, arithmetic and copies ran while one was open for 7% of the time, Pallas kernels for 3%

profile of v1, /device:TPU:1, one launch (start us, length us, event | category | flops | bytes accessed | tf_op | source)
XLA Modules:
  0.0 137.9 jit_solution(5525900162254003602)
XLA Ops:
  0.0 0.1 mul.103
  0.1 0.7 negate_sqrt_fusion
  0.8 0.1 copy.20
  0.9 0.1 stack_broadcast_in_dim.14
  1.0 0.1 stack_broadcast_in_dim.15
  1.0 0.1 copy.21
  1.2 0.1 stack_broadcast_in_dim.17
  1.3 0.8 copy.19
  2.1 0.1 mul.99
  2.2 0.6 pad_maximum_fusion.1.table_ref
  2.9 2.9 %mixer_local.1 = (f32[8,384]{1,0:T(8,128)}, f32[128,8,128]{2,1,0:T(8,128)}, f32[128,8,128]{2,1,0:T(8,128)}) custom-call(bf16[128,128]{1,0:T(8,128)(2,1)} %x_ref.3, f32[4,8,128]{2,1,0:T(8,128)} %pad_maximum_fusion.1.table_ref, f32[2,8,128]{2,1,0:T(8,128)} %bitcast.56, bf16[2,2,8,16,64]{4,3,2,1,0:T(8,128)(2,1)} %bitcast.61), custom_call_target="tpu_custom_call" | custom-call | flops 300000000 | bytes 2000000 | tf_op jit(solution)/shard_map/mixer_local/pallas_call | solution.py:198
  5.7 1.5 %broadcast_in_dim.8 = f32[32,8,384]{2,1,0:T(8,128)} broadcast(f32[8,384]{1,0:T(8,128)} %get-tuple-element.8), dimensions={1,2} | broadcast | bytes 405504 | tf_op jit(solution)/shard_map/broadcast_in_dim | solution.py:25
  7.2 12.0 %all-to-all-start = ((f32[32,8,384]{2,1,0:T(8,128)}), f32[32,8,384]{2,1,0:T(8,128)S(1)}, u32[]{:S(2)}, u32[]{:S(2)}) async-start(f32[32,8,384]{2,1,0:T(8,128)} %broadcast_in_dim.8), calls=%async_computation | async-start | bytes 786432 | tf_op jit(solution)/shard_map/all_to_all | solution.py:26
  19.2 0.8 fusion.8
  20.1 0.8 fusion.9
  20.9 0.8 fusion.10
  21.8 0.9 pad_maximum_fusion
  22.7 10.4 %all-to-all-done.ends_ref = f32[32,8,384]{2,1,0:T(8,128)S(1)} async-done(((f32[32,8,384]{2,1,0:T(8,128)}), f32[32,8,384]{2,1,0:T(8,128)S(1)}, u32[]{:S(2)}, u32[]{:S(2)}) %all-to-all-start) | async-done | bytes 393248 | tf_op jit(solution)/shard_map/all_to_all | solution.py:26
  33.1 3.5 %all-to-all-start.3 = ((bf16[4,64,1152]{2,1,0:T(8,128)(2,1)}), bf16[4,64,1152]{2,1,0:T(8,128)(2,1)S(1)}, u32[]{:S(2)}, u32[]{:S(2)}) async-start(bf16[4,64,1152]{2,1,0:T(8,128)(2,1)} %pad_maximum_fusion), calls=%async_computation.3 | async-start | bytes 1179648 | tf_op jit(solution)/shard_map/all_to_all | solution.py:351
  36.6 3.8 %mixer_out.1 = f32[8,24,128]{2,1,0:T(8,128)} custom-call(s32[1]{0:T(128)} %bitcast.at_ref, f32[32,8,384]{2,1,0:T(8,128)} %copy-done.2, f32[128,8,128]{2,1,0:T(8,128)} %get-tuple-element.9.dre_ref, f32[128,8,128]{2,1,0:T(8,128)} %get-tuple-element.10.dim_ref, f32[4,8,128]{2,1,0:T(8,128)} %pad_maximum_fusion.1.table_ref, f32[2,8,128]{2,1,0:T(8,128)} %bitcast.57, ...), custom_call_target="tpu_custom_call" | custom-call | flops 300000000 | bytes 2000000 | tf_op jit(solution)/shard_map/mixer_out/pallas_call | solution.py:216
  40.3 3.7 %all-to-all-done.3 = bf16[4,64,1152]{2,1,0:T(8,128)(2,1)S(1)} async-done(((bf16[4,64,1152]{2,1,0:T(8,128)(2,1)}), bf16[4,64,1152]{2,1,0:T(8,128)(2,1)S(1)}, u32[]{:S(2)}, u32[]{:S(2)}) %all-to-all-start.3) | async-done | bytes 589856 | tf_op jit(solution)/shard_map/all_to_all | solution.py:351
  44.1 7.9 %all-to-all-start.1 = ((f32[8,24,128]{2,1,0:T(8,128)}), f32[8,24,128]{2,1,0:T(8,128)S(1)}, u32[]{:S(2)}, u32[]{:S(2)}) async-start(f32[8,24,128]{2,1,0:T(8,128)} %mixer_out.1), calls=%async_computation.1 | async-start | bytes 196608 | tf_op jit(solution)/shard_map/all_to_all | solution.py:361
  51.9 0.7 collective-permute-start.5
  52.6 2.0 %collective-permute-start.2 = (bf16[256,1152]{1,0:T(8,128)(2,1)S(1)}, bf16[256,1152]{1,0:T(8,128)(2,1)S(1)}, u32[]{:S(2)}, u32[]{:S(2)}) collective-permute-start(bf16[256,1152]{1,0:T(8,128)(2,1)S(1)} %bitcast.52), channel_id=1, source_target_pairs={{0,224},{32,0},{64,32},{96,64},{128,96},{160,128},{192,160},{224,1... | collective-permute-start | bytes 1769480 | tf_op jit(solution)/shard_map/ppermute | solution.py:21
  54.6 2.3 %all-to-all-done.1 = f32[8,24,128]{2,1,0:T(8,128)S(1)} async-done(((f32[8,24,128]{2,1,0:T(8,128)}), f32[8,24,128]{2,1,0:T(8,128)S(1)}, u32[]{:S(2)}, u32[]{:S(2)}) %all-to-all-start.1) | async-done | bytes 98336 | tf_op jit(solution)/shard_map/all_to_all | solution.py:361
  56.9 0.1 fusion.4
  57.1 3.0 %multiply_reduce_fusion = (f32[16]{0:T(128)S(1)}, f32[16,2048]{1,0:T(8,128)S(1)}) fusion(bf16[1024,2048]{1,0:T(8,128)(2,1)} %param.22, f32[1024]{0:T(1024)S(1)} %bitcast.55, f32[16]{0:T(128)S(1)} %add_rsqrt_fusion.1, bf16[16,2048]{1,0:T(8,128)(2,1)S(1)} %copy-done.8, f32[8,24,128]{2,1,0:T(8,128)S(1)} %all-to-all-done.1), kind=kOutput, calls=%fused_computation.9 | convolution fusion | flops 67354608 | bytes 4461120 | tf_op jit(solution)/shard_map/dot_general | solution.py:366
  60.1 0.1 multiply_convert_fusion
  60.2 1.1 broadcast_in_dim.20
  61.3 4.3 %all-to-all-start.2 = ((bf16[16,16,2048]{2,1,0:T(8,128)(2,1)}), bf16[16,16,2048]{2,1,0:T(8,128)(2,1)S(1)}, u32[]{:S(2)}, u32[]{:S(2)}) async-start(bf16[16,16,2048]{2,1,0:T(8,128)(2,1)} %broadcast_in_dim.20), calls=%async_computation.2 | async-start | bytes 2097152 | tf_op jit(solution)/shard_map/all_to_all | solution.py:26
  65.5 2.5 %collective-permute-done.5.refs_8_ = bf16[256,1152]{1,0:T(8,128)(2,1)S(1)} collective-permute-done((bf16[256,1152]{1,0:T(8,128)(2,1)S(1)}, bf16[256,1152]{1,0:T(8,128)(2,1)S(1)}, u32[]{:S(2)}, u32[]{:S(2)}) %collective-permute-start.5) | collective-permute-done | bytes 589856 | tf_op jit(solution)/shard_map/ppermute | solution.py:21
  68.0 2.7 %collective-permute-start.3 = (bf16[256,1152]{1,0:T(8,128)(2,1)S(1)}, bf16[256,1152]{1,0:T(8,128)(2,1)}, u32[]{:S(2)}, u32[]{:S(2)}) collective-permute-start(bf16[256,1152]{1,0:T(8,128)(2,1)S(1)} %collective-permute-done.2.refs_1_), channel_id=1, source_target_pairs={{0,224},{32,0},{64,32},{96,64},{128,96},{160,128},{192,160},{224,1... | collective-permute-start | bytes 1769480 | tf_op jit(solution)/shard_map/ppermute | solution.py:21
  70.7 0.6 constant_dynamic-slice_fusion
  71.3 12.1 %collective-permute-done.6.refs_7_ = bf16[256,1152]{1,0:T(8,128)(2,1)} collective-permute-done((bf16[256,1152]{1,0:T(8,128)(2,1)S(1)}, bf16[256,1152]{1,0:T(8,128)(2,1)}, u32[]{:S(2)}, u32[]{:S(2)}) %collective-permute-start.6) | collective-permute-done | bytes 589856 | tf_op jit(solution)/shard_map/ppermute | solution.py:21
  83.4 2.7 %collective-permute-start.4 = (bf16[256,1152]{1,0:T(8,128)(2,1)}, bf16[256,1152]{1,0:T(8,128)(2,1)S(1)}, u32[]{:S(2)}, u32[]{:S(2)}) collective-permute-start(bf16[256,1152]{1,0:T(8,128)(2,1)} %collective-permute-done.3.refs_2_), channel_id=1, source_target_pairs={{0,224},{32,0},{64,32},{96,64},{128,96},{160,128},{192,160},{224,1... | collective-permute-start | bytes 1769480 | tf_op jit(solution)/shard_map/ppermute | solution.py:21
  86.1 0.7 collective-permute-start.1
  86.8 11.2 %collective-permute-done.7.refs_6_ = bf16[256,1152]{1,0:T(8,128)(2,1)S(1)} collective-permute-done((bf16[256,1152]{1,0:T(8,128)(2,1)}, bf16[256,1152]{1,0:T(8,128)(2,1)S(1)}, u32[]{:S(2)}, u32[]{:S(2)}) %collective-permute-start.7) | collective-permute-done | bytes 589856 | tf_op jit(solution)/shard_map/ppermute | solution.py:21
  98.0 0.1 collective-permute-start.8
  98.1 2.7 %collective-permute-start.9 = (bf16[128,1152]{1,0:T(8,128)(2,1)S(1)}, bf16[128,1152]{1,0:T(8,128)(2,1)S(1)}, u32[]{:S(2)}, u32[]{:S(2)}) collective-permute-start(bf16[128,1152]{1,0:T(8,128)(2,1)S(1)} %slice.65), channel_id=1, source_target_pairs={{0,224},{32,0},{64,32},{96,64},{128,96},{160,128},{192,160},{224,1... | collective-permute-start | bytes 884744 | tf_op jit(solution)/shard_map/ppermute | solution.py:21
  100.9 0.6 collective-permute-start
  101.5 0.6 pad_add_fusion.at_ref
  102.1 2.0 %collective-permute-done.near_ref = bf16[4,2048]{1,0:T(4,128)(2,1)S(1)} collective-permute-done((bf16[4,2048]{1,0:T(4,128)(2,1)S(1)}, bf16[4,2048]{1,0:T(4,128)(2,1)S(1)}, u32[]{:S(2)}, u32[]{:S(2)}) %collective-permute-start) | collective-permute-done | bytes 16416 | tf_op jit(solution)/shard_map/ppermute | solution.py:258
  104.1 1.3 collective-permute-done.8.refs_4_
  105.5 0.7 copy-done.7
  106.1 6.4 %ffn.1 = bf16[16,16,2048]{2,1,0:T(8,128)(2,1)} custom-call(s32[2]{0:T(128)} %pad_add_fusion.at_ref, bf16[2,128,2048]{2,1,0:T(8,128)(2,1)} %bitcast.50, bf16[4,2048]{1,0:T(4,128)(2,1)} %copy-done.9, bf16[1,2048]{1,0:T(2,128)(2,1)} %copy-done.10, f32[3,384]{1,0:T(4,128)} %get-tuple-element.28.vtap_ref, f32[3,384]{1,0:T(4,128)} %get-tuple-element.27.gtap_ref, ...), custom_call_target="tpu_custom_call" | custom-call | flops 1300000000 | bytes 6000000 | tf_op jit(solution)/shard_map/ffn/pallas_call | solution.py:378
  112.5 24.6 %all_to_all.25 = bf16[16,16,2048]{2,1,0:T(8,128)(2,1)S(1)} all-to-all(bf16[16,16,2048]{2,1,0:T(8,128)(2,1)} %ffn.1), channel_id=1, replica_groups=mesh['z'=8,'yh'=2,'yl'=2,'x'=4,'c'=2] {'yh','x','c'}, dimensions={0} | all-to-all | bytes 2097152 | tf_op jit(solution)/shard_map/all_to_all | solution.py:392
  137.1 0.1 convert_reduce_fusion
  137.3 0.6 add_convert_fusion
  (49 shorter events, 0.5 us)
Async XLA Ops:
  0.0 57.1 %copy-start.8 = (bf16[16,2048]{1,0:T(8,128)(2,1)S(1)}, bf16[16,2048]{1,0:T(8,128)(2,1)}, u32[]{:S(2)}) copy-start(bf16[16,2048]{1,0:T(8,128)(2,1)} %param.23) | copy-start | bytes 196612
  7.2 25.9 %all-to-all-start = ((f32[32,8,384]{2,1,0:T(8,128)}), f32[32,8,384]{2,1,0:T(8,128)S(1)}, u32[]{:S(2)}, u32[]{:S(2)}) async-start(f32[32,8,384]{2,1,0:T(8,128)} %broadcast_in_dim.8), calls=%async_computation | async-start | bytes 786432 | tf_op jit(solution)/shard_map/all_to_all | solution.py:26
  21.8 38.3 %copy-start.11 = (f32[2048]{0:T(1024)S(1)}, f32[2048]{0:T(1024)}, u32[]{:S(2)}) copy-start(f32[2048]{0:T(1024)} %param.24) | copy-start | bytes 24580
  33.1 3.5 %copy-start.2 = (f32[32,8,384]{2,1,0:T(8,128)}, f32[32,8,384]{2,1,0:T(8,128)S(1)}, u32[]{:S(2)}) copy-start(f32[32,8,384]{2,1,0:T(8,128)S(1)} %all-to-all-done.ends_ref) | copy-start | bytes 1179652
  33.1 11.0 %all-to-all-start.3 = ((bf16[4,64,1152]{2,1,0:T(8,128)(2,1)}), bf16[4,64,1152]{2,1,0:T(8,128)(2,1)S(1)}, u32[]{:S(2)}, u32[]{:S(2)}) async-start(bf16[4,64,1152]{2,1,0:T(8,128)(2,1)} %pad_maximum_fusion), calls=%async_computation.3 | async-start | bytes 1179648 | tf_op jit(solution)/shard_map/all_to_all | solution.py:351
  40.3 30.4 %copy-start.12 = (f32[3,768]{1,0:T(4,128)S(1)}, f32[3,768]{1,0:T(4,128)}, u32[]{:S(2)}) copy-start(f32[3,768]{1,0:T(4,128)} %param.28) | copy-start | bytes 27652
  40.3 30.4 %copy-start.13 = (f32[3,768]{1,0:T(4,128)S(1)}, f32[3,768]{1,0:T(4,128)}, u32[]{:S(2)}) copy-start(f32[3,768]{1,0:T(4,128)} %param.27) | copy-start | bytes 27652
  44.1 53.9 %copy-start.1 = (bf16[4,64,1152]{2,1,0:T(8,128)(2,1)}, bf16[4,64,1152]{2,1,0:T(8,128)(2,1)S(1)}, u32[]{:S(2)}) copy-start(bf16[4,64,1152]{2,1,0:T(8,128)(2,1)S(1)} %all-to-all-done.3) | copy-start | bytes 1769476
  44.1 12.8 %all-to-all-start.1 = ((f32[8,24,128]{2,1,0:T(8,128)}), f32[8,24,128]{2,1,0:T(8,128)S(1)}, u32[]{:S(2)}, u32[]{:S(2)}) async-start(f32[8,24,128]{2,1,0:T(8,128)} %mixer_out.1), calls=%async_computation.1 | async-start | bytes 196608 | tf_op jit(solution)/shard_map/all_to_all | solution.py:361
  51.9 16.1 %collective-permute-start.5 = (bf16[256,1152]{1,0:T(8,128)(2,1)S(1)}, bf16[256,1152]{1,0:T(8,128)(2,1)S(1)}, u32[]{:S(2)}, u32[]{:S(2)}) collective-permute-start(bf16[256,1152]{1,0:T(8,128)(2,1)S(1)} %bitcast.51), channel_id=1, source_target_pairs={{0,32},{32,64},{64,96},{96,128},{128,160},{160,192},{192,224},{224... | collective-permute-start | bytes 1769480 | tf_op jit(solution)/shard_map/ppermute | solution.py:21
  52.6 15.4 %collective-permute-start.2 = (bf16[256,1152]{1,0:T(8,128)(2,1)S(1)}, bf16[256,1152]{1,0:T(8,128)(2,1)S(1)}, u32[]{:S(2)}, u32[]{:S(2)}) collective-permute-start(bf16[256,1152]{1,0:T(8,128)(2,1)S(1)} %bitcast.52), channel_id=1, source_target_pairs={{0,224},{32,0},{64,32},{96,64},{128,96},{160,128},{192,160},{224,1... | collective-permute-start | bytes 1769480 | tf_op jit(solution)/shard_map/ppermute | solution.py:21
  61.3 24.8 %all-to-all-start.2 = ((bf16[16,16,2048]{2,1,0:T(8,128)(2,1)}), bf16[16,16,2048]{2,1,0:T(8,128)(2,1)S(1)}, u32[]{:S(2)}, u32[]{:S(2)}) async-start(bf16[16,16,2048]{2,1,0:T(8,128)(2,1)} %broadcast_in_dim.20), calls=%async_computation.2 | async-start | bytes 2097152 | tf_op jit(solution)/shard_map/all_to_all | solution.py:26
  68.0 37.4 %copy-start.5 = (bf16[256,1152]{1,0:T(8,128)(2,1)}, bf16[256,1152]{1,0:T(8,128)(2,1)S(1)}, u32[]{:S(2)}) copy-start(bf16[256,1152]{1,0:T(8,128)(2,1)S(1)} %collective-permute-done.5.refs_8_) | copy-start | bytes 1769476
  68.0 15.3 %collective-permute-start.6 = (bf16[256,1152]{1,0:T(8,128)(2,1)S(1)}, bf16[256,1152]{1,0:T(8,128)(2,1)}, u32[]{:S(2)}, u32[]{:S(2)}) collective-permute-start(bf16[256,1152]{1,0:T(8,128)(2,1)S(1)} %collective-permute-done.5.refs_8_), channel_id=1, source_target_pairs={{0,32},{32,64},{64,96},{96,128},{128,160},{160,192},{192,224},{224... | collective-permute-start | bytes 1769480 | tf_op jit(solution)/shard_map/ppermute | solution.py:21
  68.0 15.3 %copy-start.6 = (bf16[256,1152]{1,0:T(8,128)(2,1)}, bf16[256,1152]{1,0:T(8,128)(2,1)S(1)}, u32[]{:S(2)}) copy-start(bf16[256,1152]{1,0:T(8,128)(2,1)S(1)} %collective-permute-done.2.refs_1_) | copy-start | bytes 1769476
  68.0 15.3 %collective-permute-start.3 = (bf16[256,1152]{1,0:T(8,128)(2,1)S(1)}, bf16[256,1152]{1,0:T(8,128)(2,1)}, u32[]{:S(2)}, u32[]{:S(2)}) collective-permute-start(bf16[256,1152]{1,0:T(8,128)(2,1)S(1)} %collective-permute-done.2.refs_1_), channel_id=1, source_target_pairs={{0,224},{32,0},{64,32},{96,64},{128,96},{160,128},{192,160},{224,1... | collective-permute-start | bytes 1769480 | tf_op jit(solution)/shard_map/ppermute | solution.py:21
  83.4 14.6 %collective-permute-start.7 = (bf16[256,1152]{1,0:T(8,128)(2,1)}, bf16[256,1152]{1,0:T(8,128)(2,1)S(1)}, u32[]{:S(2)}, u32[]{:S(2)}) collective-permute-start(bf16[256,1152]{1,0:T(8,128)(2,1)} %collective-permute-done.6.refs_7_), channel_id=1, source_target_pairs={{0,32},{32,64},{64,96},{96,128},{128,160},{160,192},{192,224},{224... | collective-permute-start | bytes 1769480 | tf_op jit(solution)/shard_map/ppermute | solution.py:21
  83.4 14.7 %collective-permute-start.4 = (bf16[256,1152]{1,0:T(8,128)(2,1)}, bf16[256,1152]{1,0:T(8,128)(2,1)S(1)}, u32[]{:S(2)}, u32[]{:S(2)}) collective-permute-start(bf16[256,1152]{1,0:T(8,128)(2,1)} %collective-permute-done.3.refs_2_), channel_id=1, source_target_pairs={{0,224},{32,0},{64,32},{96,64},{128,96},{160,128},{192,160},{224,1... | collective-permute-start | bytes 1769480 | tf_op jit(solution)/shard_map/ppermute | solution.py:21
  86.1 19.4 %copy-start = (bf16[16,16,2048]{2,1,0:T(8,128)(2,1)}, bf16[16,16,2048]{2,1,0:T(8,128)(2,1)S(1)}, u32[]{:S(2)}) copy-start(bf16[16,16,2048]{2,1,0:T(8,128)(2,1)S(1)} %all-to-all-done.2) | copy-start | bytes 3145732
  86.1 16.0 %collective-permute-start.1 = (bf16[1,2048]{1,0:T(2,128)(2,1)S(1)}, bf16[1,2048]{1,0:T(2,128)(2,1)S(1)}, u32[]{:S(2)}, u32[]{:S(2)}) collective-permute-start(bf16[1,2048]{1,0:T(2,128)(2,1)S(1)} %broadcast_select_fusion), channel_id=1, source_target_pairs={{8,32},{40,64},{72,96},{104,128},{136,160},{168,192},{200,224},{32... | collective-permute-start | bytes 12296 | tf_op jit(solution)/shard_map/ppermute | solution.py:261
  98.0 7.5 %copy-start.3 = (bf16[256,1152]{1,0:T(8,128)(2,1)}, bf16[256,1152]{1,0:T(8,128)(2,1)S(1)}, u32[]{:S(2)}) copy-start(bf16[256,1152]{1,0:T(8,128)(2,1)S(1)} %collective-permute-done.7.refs_6_) | copy-start | bytes 1769476
  98.0 7.4 %collective-permute-start.8 = (bf16[128,1152]{1,0:T(8,128)(2,1)S(1)}, bf16[128,1152]{1,0:T(8,128)(2,1)}, u32[]{:S(2)}, u32[]{:S(2)}) collective-permute-start(bf16[128,1152]{1,0:T(8,128)(2,1)S(1)} %slice.64), channel_id=1, source_target_pairs={{0,32},{32,64},{64,96},{96,128},{128,160},{160,192},{192,224},{224... | collective-permute-start | bytes 884744 | tf_op jit(solution)/shard_map/ppermute | solution.py:21
  98.1 7.3 %copy-start.4 = (bf16[256,1152]{1,0:T(8,128)(2,1)}, bf16[256,1152]{1,0:T(8,128)(2,1)S(1)}, u32[]{:S(2)}) copy-start(bf16[256,1152]{1,0:T(8,128)(2,1)S(1)} %collective-permute-done.4.refs_3_) | copy-start | bytes 1769476
  98.1 7.2 %collective-permute-start.9 = (bf16[128,1152]{1,0:T(8,128)(2,1)S(1)}, bf16[128,1152]{1,0:T(8,128)(2,1)S(1)}, u32[]{:S(2)}, u32[]{:S(2)}) collective-permute-start(bf16[128,1152]{1,0:T(8,128)(2,1)S(1)} %slice.65), channel_id=1, source_target_pairs={{0,224},{32,0},{64,32},{96,64},{128,96},{160,128},{192,160},{224,1... | collective-permute-start | bytes 884744 | tf_op jit(solution)/shard_map/ppermute | solution.py:21
  100.9 3.2 %collective-permute-start = (bf16[4,2048]{1,0:T(4,128)(2,1)S(1)}, bf16[4,2048]{1,0:T(4,128)(2,1)S(1)}, u32[]{:S(2)}, u32[]{:S(2)}) collective-permute-start(bf16[4,2048]{1,0:T(4,128)(2,1)S(1)} %pad_maximum_fusion.2), channel_id=1, source_target_pairs={{0,8},{8,0},{1,9},{9,1},{2,10},{10,2},{3,11},{11,3},{4,12},{12,4},... | collective-permute-start | bytes 49160 | tf_op jit(solution)/shard_map/ppermute | solution.py:258
  102.1 3.3 %copy-start.10 = (bf16[1,2048]{1,0:T(2,128)(2,1)}, bf16[1,2048]{1,0:T(2,128)(2,1)S(1)}, u32[]{:S(2)}) copy-start(bf16[1,2048]{1,0:T(2,128)(2,1)S(1)} %collective-permute-done.1.far_ref) | copy-start | bytes 12292
  104.1 1.4 copy-start.9
  105.4 0.7 copy-start.7

commit v2 on v1

--- a/solution.py
+++ b/solution.py
@@ -12,6 +12,7 @@
 norm_eps = 1e-06
 SP = ("z", "yh", "yl")
 TP = ("x", "c")
+PAIR = ("yl", "x", "c")
 VMEM = pl.BlockSpec(memory_space=pltpu.VMEM)
 SMEM = pl.BlockSpec(memory_space=pltpu.SMEM)
 
@@ -19,11 +20,6 @@
 def shifted(array, axis, step):
     n = lax.axis_size(axis)
     return lax.ppermute(array, axis, [(i, (i + step) % n) for i in range(n)])
-
-
-def sent_to_all(array, axis):
-    copies = jnp.broadcast_to(array, (lax.axis_size(axis), *array.shape))
-    return lax.all_to_all(copies, axis, split_axis=0, concat_axis=0, tiled=True)
 
 
 def step_decays(table, damp_ref):
@@ -75,9 +71,16 @@
         jnp.broadcast_to(total[0], (groups, 128)),
         jnp.broadcast_to(total[1], (groups, 128)),
     )
-    end_ref[:, :128] = real
-    end_ref[:, 128:256] = imag
-    end_ref[:, 256:] = total + rows * table_ref[3]
+    total = total + rows * table_ref[3]
+    high = total.astype(jnp.bfloat16)
+    low = (total - high.astype(jnp.float32)).astype(jnp.bfloat16).astype(jnp.float32)
+    lane = lax.broadcasted_iota(jnp.int32, (groups, 128), 1)
+    total = jnp.where(lane % 64 < 32, high.astype(jnp.float32), low).astype(jnp.bfloat16)
+    real, imag = real.astype(jnp.bfloat16), imag.astype(jnp.bfloat16)
+    for p in range(end_ref.shape[0]):
+        end_ref[p, :, :128] = real
+        end_ref[p, :, 128:256] = imag
+        end_ref[p, :, 256:] = total
 
 
 def mix_kernel(
@@ -108,15 +111,21 @@
     while power < rows:
         block_re, block_im = block_re * block_re - block_im * block_im, 2.0 * block_re * block_im
         power *= 2
+    lane_high = lax.broadcasted_iota(jnp.int32, (groups, 128), 1) % 64 < 32
+
+    def picked(i, j, at):
+        fwd_part = ends_ref[i, :, at : at + 128].astype(jnp.float32)
+        return jnp.where(lane_fwd, fwd_part, ends_ref[j, :, at : at + 128].astype(jnp.float32))
+
     real = jnp.zeros((groups, 128), jnp.float32)
     imag = jnp.zeros((groups, 128), jnp.float32)
     for i in range(blocks):
         j = blocks - 1 - i
-        part = jnp.where(lane_fwd, ends_ref[i, :, 256:], ends_ref[j, :, 256:])
+        part = picked(i, j, 256)
+        part = part + jnp.where(lane_high, pltpu.roll(part, 96, 1), pltpu.roll(part, 32, 1))
         size = jnp.exp(-part)
         dec_re, dec_im = size * block_re, size * block_im
-        end_re = jnp.where(lane_fwd, ends_ref[i, :, :128], ends_ref[j, :, :128])
-        end_im = jnp.where(lane_fwd, ends_ref[i, :, 128:256], ends_ref[j, :, 128:256])
+        end_re, end_im = picked(i, j, 0), picked(i, j, 128)
         next_re = dec_re * real - dec_im * imag + end_re
         next_im = dec_re * imag + dec_im * real + end_im
         keep_fwd = jnp.where(i < at, 1, 0)
@@ -169,11 +178,17 @@
         mixed = mixed + lax.dot_general(
             state, part, (((1,), (1,)), ((), ())), preferred_element_type=jnp.float32
         )
-    parts = out_ref.shape[0]
-    own = rows // parts
-    for p in range(parts):
-        out_ref[p, :own, :] = mixed[p * own : (p + 1) * own, :]
-        out_ref[p, own:, :] = jnp.broadcast_to(gain_ref[...], (8, channels))
+    high = gain_ref[...].astype(jnp.bfloat16).astype(jnp.float32)
+    mid = (gain_ref[...] - high).astype(jnp.bfloat16).astype(jnp.float32)
+    low = gain_ref[...] - high - mid
+    row = lax.broadcasted_iota(jnp.int32, (16, channels), 0)
+    tail = jnp.zeros(row.shape, jnp.float32)
+    for k, part in enumerate((high, mid, low)):
+        tail = jnp.where(row == k, jnp.broadcast_to(part, row.shape), tail)
+    mixed, tail = mixed.astype(jnp.bfloat16), tail.astype(jnp.bfloat16)
+    for p in range(out_ref.shape[0]):
+        out_ref[p, :rows, :] = mixed
+        out_ref[p, rows:, :] = tail
 
 
 def mixer_branch(mixer_input, time_step, damping, input_map, readout, skip_gain, out_gain):
@@ -198,7 +213,7 @@
     ends, drive_re, drive_im = pl.pallas_call(
         local_kernel,
         out_shape=(
-            jax.ShapeDtypeStruct((groups, 6 * states), jnp.float32),
+            jax.ShapeDtypeStruct((lax.axis_size(SP), groups, 6 * states), jnp.bfloat16),
             drive_shape,
             drive_shape,
         ),
@@ -209,14 +224,14 @@
             flops=300_000_000, bytes_accessed=2_000_000, transcendentals=0
         ),
     )(mixer_input, table, damp, maps)
-    all_ends = sent_to_all(ends, SP)
+    all_ends = lax.all_to_all(ends, SP, 0, 0, tiled=True)
     at = lax.axis_index(SP).astype(jnp.int32).reshape(1)
     scratch = pltpu.VMEM((rows, groups, 2 * states), jnp.float32)
-    parts = lax.axis_size(TP)
+    copies = lax.axis_size(PAIR)
     return pl.pallas_call(
         mix_kernel,
         out_shape=jax.ShapeDtypeStruct(
-            (parts, rows // parts + 8, mixer_input.shape[1]), jnp.float32
+            (copies, rows + 16, mixer_input.shape[1]), jnp.bfloat16
         ),
         in_specs=[SMEM] + [VMEM] * 9,
         out_specs=VMEM,
@@ -242,59 +257,124 @@
 def z_ring(block):
     found = {0: block}
     up = down = block
-    for s in range(1, 4):
-        up = shifted(up, "z", 1)
-        down = shifted(down, "z", -1)
-        found[8 - s], found[s] = up, down
-    half = block.shape[0] // 2
-    far_up = shifted(up[:half], "z", 1)
-    found[4] = (far_up, shifted(down[half:], "z", -1))
-    return found
-
-
-def edge_rows(cells):
-    last = cells.shape[1] - 1
-    edges = jnp.concatenate((cells[0, :1], cells[0, last:], cells[1, :1], cells[1, last:]))
-    near = lax.ppermute(edges, "yl", [(0, 1), (1, 0)])
-    count = lax.axis_size("z")
-    pairs = [(2 * i + 1, 2 * i + 2) for i in range(count - 1)]
-    far = lax.ppermute(
-        jnp.where(lax.axis_index("yl") == 0, edges[:1], edges[3:]),
-        ("z", "yl"),
-        pairs + [(j, i) for i, j in pairs],
-    )
+    for s in range(1, 5):
+        found[8 - s] = up = shifted(up, "z", 1)
+        if s < 4:
+            found[s] = down = shifted(down, "z", -1)
+    return [found[d] for d in range(8)]
+
+
+def pair_rows(rows):
+    both = jnp.stack((rows, lax.ppermute(rows, "yl", [(0, 1), (1, 0)])))
+    quad = jnp.concatenate((both, lax.ppermute(both, "c", [(0, 1), (1, 0)])))
+    pieces = {0: quad}
+    for d in (1, 3, 2):
+        pieces[d] = shifted(quad, "x", -d)
+    return [pieces[d] for d in range(4)]
+
+
+def edges_passed(near, far):
+    pairs = [(2 * i + 1, 2 * i + 2) for i in range(lax.axis_size("z") - 1)]
+    far = lax.ppermute(far, ("z", "yh"), pairs + [(j, i) for i, j in pairs])
+    near = lax.ppermute(near, "yh", [(0, 1), (1, 0)])
     return near, far
 
 
+def pack_kernel(value_ref, gate_ref, down_ref, out_ref):
+    half = value_ref.shape[1] // 2
+    for k in range(out_ref.shape[0]):
+        cut = slice(k % 2 * half, (k % 2 + 1) * half)
+        out_ref[k, :, :half] = value_ref[:, cut]
+        out_ref[k, :, half : 2 * half] = gate_ref[:, cut]
+        out_ref[k, :, 2 * half :] = down_ref[:, cut]
+
+
+def pair_gains(mixed_ref, tok):
+    parts = [mixed_ref[p, tok:, :].astype(jnp.float32) for p in range(mixed_ref.shape[0] // 2)]
+    return jnp.concatenate([g[0:1] + g[1:2] + g[2:3] for g in parts], axis=1)
+
+
+def pair_residual(at_ref, pieces, state_ref):
+    low, x, core = at_ref[0], at_ref[1], at_ref[2]
+    own = pieces[0].shape[1]
+    for dx, ref in enumerate(pieces):
+        for k in range(4):
+            row = lax.rem(low + k % 2, 2) * 8 + lax.rem(x + dx, 4) * 2 + lax.rem(core + k // 2, 2)
+            state_ref[pl.ds(pl.multiple_of(row * own, own), own), :] = ref[k]
+
+
+def normed_rows(mixed, resid, gains, weight, gain):
+    mixed = mixed.astype(jnp.float32)
+    inverse = lax.rsqrt(jnp.mean(mixed * mixed, axis=1, keepdims=True) + norm_eps)
+    normed_mix = (mixed * inverse * gains).astype(jnp.bfloat16)
+    added = jnp.dot(normed_mix, weight, preferred_element_type=jnp.float32)
+    state = (resid.astype(jnp.float32) + added).astype(jnp.bfloat16)
+    wide = state.astype(jnp.float32)
+    scale = lax.rsqrt(jnp.mean(wide * wide, axis=1, keepdims=True) + norm_eps)
+    return state, (wide * scale * gain).astype(jnp.bfloat16)
+
+
+def edge_kernel(at_ref, mixed_ref, weight_ref, gain_ref, r0, r1, r2, r3, *refs):
+    near_ref, far_ref, state_ref = refs
+    tok = mixed_ref.shape[1] - 16
+    parts = mixed_ref.shape[0] // 2
+    pair_residual(at_ref, (r0, r1, r2, r3), state_ref)
+    cuts = (0, slice(0, 16)), (1, slice(tok - 16, tok))
+    mixed = [
+        jnp.concatenate([mixed_ref[k * parts + p, cut, :] for p in range(parts)], axis=1)
+        for k, cut in cuts
+    ]
+    resid = [state_ref[0:16, :], state_ref[2 * tok - 16 : 2 * tok, :]]
+    _, normed = normed_rows(
+        jnp.concatenate(mixed),
+        jnp.concatenate(resid),
+        pair_gains(mixed_ref, tok),
+        weight_ref[...],
+        gain_ref[...],
+    )
+    normed = normed.astype(jnp.float32)
+    first, last = normed[:1], normed[31:]
+    even = jnp.full(first.shape, at_ref[3], jnp.int32) == 0
+    near_ref[...] = jnp.where(even, last, first).astype(jnp.bfloat16)
+    far_ref[...] = jnp.where(even, first, last).astype(jnp.bfloat16)
+
+
+def rows_kernel(at_ref, mixed_ref, weight_ref, gain_ref, r0, r1, r2, r3, *refs):
+    normed_ref, own_ref, state_ref = refs
+    tok = mixed_ref.shape[1] - 16
+    parts = mixed_ref.shape[0] // 2
+    own = own_ref.shape[0]
+    pair_residual(at_ref, (r0, r1, r2, r3), state_ref)
+    gains = pair_gains(mixed_ref, tok)
+    for k in range(2):
+        cut = slice(k * tok, (k + 1) * tok)
+        mixed = jnp.concatenate([mixed_ref[k * parts + p, :tok, :] for p in range(parts)], axis=1)
+        state_ref[cut, :], normed_ref[cut, :] = normed_rows(
+            mixed, state_ref[cut, :], gains, weight_ref[...], gain_ref[...]
+        )
+    start = (at_ref[0] * 8 + at_ref[1] * 2 + at_ref[2]) * own
+    own_ref[...] = state_ref[pl.ds(pl.multiple_of(start, own), own), :]
+
+
 def ffn_kernel(at_ref, cells_ref, near_ref, far_ref, vtap_ref, gtap_ref, *refs):
-    line = refs[:9]
-    out_ref, whole_ref, rows_ref = refs[9:]
-    z, low = at_ref[0], at_ref[1]
-    tok = cells_ref.shape[1]
-    total = tok + 16
+    line = refs[:8]
+    keep_ref, send_ref, whole_ref, rows_ref, sums_ref = refs[8:]
+    z = at_ref[0]
+    tok, model = cells_ref.shape
     width = vtap_ref.shape[1]
     cut = line[0].shape[0]
-    for ref in range(9):
-        size = line[ref].shape[0]
-        start = lax.rem(z + (ref if ref < 5 else ref - 1), 8) * cut
-        if ref == 5:
-            start = start + cut // 2
-        whole_ref[pl.ds(pl.multiple_of(start, cut // 2), size), :] = line[ref][...]
-    row = lax.broadcasted_iota(jnp.int32, (16, cells_ref.shape[2]), 0)
-    even = jnp.full(row.shape, low, jnp.int32) == 0
-    near = [
-        jnp.broadcast_to(near_ref[k : k + 1, :].astype(jnp.float32), row.shape) for k in range(4)
-    ]
+    for d in range(8):
+        start = pl.multiple_of(lax.rem(z + d, 8) * cut, cut)
+        whole_ref[pl.ds(start, cut), :] = line[d][...]
+    row = lax.broadcasted_iota(jnp.int32, (16, model), 0)
+    even = jnp.full(row.shape, at_ref[1], jnp.int32) == 0
+    near = jnp.broadcast_to(near_ref[...].astype(jnp.float32), row.shape)
     far = jnp.broadcast_to(far_ref[...].astype(jnp.float32), row.shape)
-    sides = (
-        (jnp.where(even, near[0], near[2]), jnp.where(even, far, near[1])),
-        (jnp.where(even, near[2], far), jnp.where(even, near[1], near[3])),
-    )
-    for k in range(2):
-        after, before = sides[k]
-        tile = jnp.where(row == 0, after, jnp.where(row == 1, before, 0.0))
-        rows_ref[k * total : k * total + tok, :] = cells_ref[k]
-        rows_ref[k * total + tok : (k + 1) * total, :] = tile.astype(jnp.bfloat16)
+    after = jnp.where(even, near, far)
+    before = jnp.where(even, far, near)
+    tile = jnp.where(row == 0, after, jnp.where(row == 1, before, 0.0))
+    rows_ref[:tok, :] = cells_ref[...]
+    rows_ref[tok:, :] = tile.astype(jnp.bfloat16)
     both = jnp.dot(
         rows_ref[...], whole_ref[:, : 2 * width], preferred_element_type=jnp.float32
     )
@@ -309,21 +389,22 @@
         )
         return taps[0:1] * prev + taps[1:2] * mid + taps[2:3] * foll
 
-    hidden = []
-    for k in range(2):
-        part = both[k * total : (k + 1) * total]
-        value = convolved(part[:, :width], vtap_ref[...])
-        gate = convolved(part[:, width:], gtap_ref[...])
-        hidden.append((value * (gate / (1.0 + jnp.exp(-gate)))).astype(jnp.bfloat16))
-    sums = lax.dot_general(
-        jnp.concatenate(hidden, axis=0),
+    value = convolved(both[:, :width], vtap_ref[...])
+    gate = convolved(both[:, width:], gtap_ref[...])
+    hidden = (value * (gate / (1.0 + jnp.exp(-gate)))).astype(jnp.bfloat16)
+    sums_ref[...] = lax.dot_general(
+        hidden,
         whole_ref[:, 2 * width :],
         (((1,), (1,)), ((), ())),
         preferred_element_type=jnp.float32,
     ).astype(jnp.bfloat16)
-    own = out_ref.shape[1]
-    for p in range(out_ref.shape[0]):
-        out_ref[p] = sums[p * own : (p + 1) * own]
+    own = keep_ref.shape[1]
+    core = at_ref[2]
+    for p in range(keep_ref.shape[0]):
+        start = pl.multiple_of((2 * p + core) * own, own)
+        keep_ref[p] = sums_ref[pl.ds(start, own), :]
+        start = pl.multiple_of((2 * p + 1 - core) * own, own)
+        send_ref[p] = sums_ref[pl.ds(start, own), :]
 
 
 def body(
@@ -344,52 +425,81 @@
     down_weight,
 ):
     half = value_weight.shape[1] // 2
-    halves = [
-        jnp.concatenate((value_weight[:, cut], gate_weight[:, cut], down_weight.T[:, cut]), axis=1)
-        for cut in (slice(0, half), slice(half, 2 * half))
-    ]
-    crossed = lax.all_to_all(
-        jnp.stack((halves[0], halves[0], halves[1], halves[1])), ("yh", "yl"), 0, 0, tiled=True
-    )
+    packed = pl.pallas_call(
+        pack_kernel,
+        out_shape=jax.ShapeDtypeStruct((4, value_weight.shape[0], 3 * half), jnp.bfloat16),
+        in_specs=[VMEM] * 3,
+        out_specs=VMEM,
+        name="pack",
+    )(value_weight, gate_weight, down_weight.T)
+    crossed = lax.all_to_all(packed, ("yh", "yl"), 0, 0, tiled=True)
     pieces = z_ring(crossed.reshape(-1, 3 * half))
+    pair_resid = pair_rows(residual)
     mixed_y = mixer_branch(
         mixer_input, time_step, damping, input_map, readout, skip_gain, out_gain
     )
-    tok_rows, local_width = mixer_input.shape
+    tok_rows = mixer_input.shape[0]
+    own_rows, model = residual.shape
     tp_count = lax.axis_size(TP)
-    own_rows = tok_rows // tp_count
-    arrived = lax.all_to_all(mixed_y, TP, 0, 0, tiled=True)
-    gains = arrived[:, own_rows].reshape(tp_count * local_width)
-    rows_y = jnp.moveaxis(arrived[:, :own_rows], 0, 1).reshape(own_rows, tp_count * local_width)
-    inverse = lax.rsqrt(jnp.mean(rows_y * rows_y, axis=1, keepdims=True) + norm_eps)
-    token_block = (rows_y * inverse * gains[None, :]).astype(jnp.bfloat16)
-    mixed_rows = jnp.dot(token_block, out_weight, preferred_element_type=jnp.float32)
-    hidden_state = (residual.astype(jnp.float32) + mixed_rows).astype(jnp.bfloat16)
+    arrived = lax.all_to_all(mixed_y, PAIR, 0, 0, tiled=True)
+    row_args = (
+        jnp.stack([lax.axis_index(a) for a in (*PAIR, "yh")]).astype(jnp.int32),
+        arrived,
+        out_weight,
+        channel_gain[None, :],
+        *pair_resid,
+    )
+    state_scratch = [pltpu.VMEM((2 * tok_rows, model), jnp.bfloat16)]
+    edge = jax.ShapeDtypeStruct((1, model), jnp.bfloat16)
+    near, far = pl.pallas_call(
+        edge_kernel,
+        out_shape=(edge, edge),
+        in_specs=[SMEM] + [VMEM] * 7,
+        out_specs=(VMEM, VMEM),
+        scratch_shapes=state_scratch,
+        name="edge",
+        cost_estimate=pl.CostEstimate(
+            flops=300_000_000, bytes_accessed=6_000_000, transcendentals=0
+        ),
+    )(*row_args)
+    near, far = edges_passed(near, far)
+    cells, hidden_state = pl.pallas_call(
+        rows_kernel,
+        out_shape=(
+            jax.ShapeDtypeStruct((2 * tok_rows, model), jnp.bfloat16),
+            jax.ShapeDtypeStruct((own_rows, model), jnp.bfloat16),
+        ),
+        in_specs=[SMEM] + [VMEM] * 7,
+        out_specs=(VMEM, VMEM),
+        scratch_shapes=state_scratch,
+        name="rows",
+        cost_estimate=pl.CostEstimate(
+            flops=1_000_000_000, bytes_accessed=6_000_000, transcendentals=0
+        ),
+    )(*row_args)
     state_wide = hidden_state.astype(jnp.float32)
-    scale_rows = lax.rsqrt(jnp.mean(state_wide * state_wide, axis=1, keepdims=True) + norm_eps)
-    normed = (state_wide * scale_rows * channel_gain[None, :]).astype(jnp.bfloat16)
-    model = normed.shape[1]
-    cells = sent_to_all(normed, ("yh", *TP)).reshape(2, tok_rows, model)
-    near, far = edge_rows(cells)
-    place = jnp.stack([lax.axis_index("z"), lax.axis_index("yl")]).astype(jnp.int32)
-    shift = lax.axis_index("yh") * half
+    place = jnp.stack([lax.axis_index(a) for a in ("z", "yh", "c")]).astype(jnp.int32)
+    shift = lax.axis_index("yl") * half
     taps = [lax.dynamic_slice(t, (0, shift), (3, half)) for t in (value_taps, gate_taps)]
-    ordered = [*(pieces[d] for d in range(4)), *pieces[4], *(pieces[d] for d in range(5, 8))]
-    partial = pl.pallas_call(
+    share = jax.ShapeDtypeStruct((tp_count, own_rows, model), jnp.bfloat16)
+    keep, send = pl.pallas_call(
         ffn_kernel,
-        out_shape=jax.ShapeDtypeStruct((2 * tp_count, own_rows, model), jnp.bfloat16),
-        in_specs=[SMEM] + [VMEM] * (5 + len(ordered)),
-        out_specs=VMEM,
+        out_shape=(share, share),
+        in_specs=[SMEM] + [VMEM] * (5 + len(pieces)),
+        out_specs=(VMEM, VMEM),
         scratch_shapes=[
             pltpu.VMEM((model, 3 * half), jnp.bfloat16),
-            pltpu.VMEM((2 * (tok_rows + 16), model), jnp.bfloat16),
+            pltpu.VMEM((2 * tok_rows + 16, model), jnp.bfloat16),
+            pltpu.VMEM((2 * tok_rows, model), jnp.bfloat16),
         ],
         name="ffn",
         cost_estimate=pl.CostEstimate(
             flops=1_300_000_000, bytes_accessed=6_000_000, transcendentals=100_000
         ),
-    )(place, cells, near, far, *taps, *ordered)
-    parts = lax.all_to_all(partial, ("yh", *TP), 0, 0, tiled=True)
+    )(place, cells, near, far, *taps, *pieces)
+    other = lax.ppermute(send, "c", [(0, 1), (1, 0)])
+    both = (keep.astype(jnp.float32) + other.astype(jnp.float32)).astype(jnp.bfloat16)
+    parts = lax.all_to_all(both, ("yl", "x"), 0, 0, tiled=True)
     summed = parts.astype(jnp.float32).sum(axis=0)
     return (state_wide + summed).astype(jnp.bfloat16)
 

time: 139 us -> 144 us (1.036)
  the two profiles are of different devices: /device:TPU:1 before, /device:TPU:32 now
where the time goes in v2:
time: 144 us; the launch traced here: 143 us
  waiting for transfers between devices  45.5 us (32%)
  starting transfers between devices  34.1 us (24%)
  blocking collectives  28.6 us (20%)
  Pallas kernels  25.3 us (18%)
  other arithmetic  5.36 us (4%)
  local copies, waits for them, and re-layouts  4.23 us (3%)
    ppermute x10, waiting for transfers between devices, shifted(): return lax.ppermute(array, axis, [(i, (i + step) % n) for i in range(n)])  34.1 us
    all_to_all x1, blocking collectives, body(): crossed = lax.all_to_all(packed, ('yh', 'yl'), 0, 0, tiled=True)  14.6 us
    all_to_all x1, blocking collectives, body(): parts = lax.all_to_all(both, ('yl', 'x'), 0, 0, tiled=True)  13.9 us
    ppermute x10, starting transfers between devices, shifted(): return lax.ppermute(array, axis, [(i, (i + step) % n) for i in range(n)])  13.4 us
    all_to_all x1, starting transfers between devices, mixer_branch(): all_ends = lax.all_to_all(ends, SP, 0, 0, tiled=True)  9.61 us
    all_to_all x1, waiting for transfers between devices, mixer_branch(): all_ends = lax.all_to_all(ends, SP, 0, 0, tiled=True)  9.19 us
    pallas_call x1, Pallas kernels, body(): pl.pallas_call(ffn_kernel, out_shape=(share, share), in_specs=[SMEM] + [V...  6.56 us
    pallas_call x1, Pallas kernels, body(): pl.pallas_call(rows_kernel, out_shape=(jax.ShapeDtypeStruct((2 * tok_rows...  5.64 us
  transfers between devices with their start and end apart: 17, of which 7 were waited for; matrix products, arithmetic and copies ran while one was open for 4% of the time, Pallas kernels for 12%

profile of v2, /device:TPU:32, one launch (start us, length us, event | category | flops | bytes accessed | tf_op | source)
XLA Modules:
  0.0 143.2 jit_solution(13937163776991382540)
XLA Ops:
  0.0 1.9 %pack.1 = bf16[4,64,1152]{2,1,0:T(8,128)(2,1)} custom-call(bf16[64,768]{1,0:T(8,128)(2,1)} %value_ref.1, bf16[64,768]{1,0:T(8,128)(2,1)} %gate_ref.1, bf16[64,768]{1,0:T(8,128)(2,1)} %bitcast.25), custom_call_target="tpu_custom_call" | custom-call | tf_op jit(solution)/shard_map/pack/pallas_call | solution.py:428
  1.9 14.6 %all_to_all.20 = bf16[4,64,1152]{2,1,0:T(8,128)(2,1)S(1)} all-to-all(bf16[4,64,1152]{2,1,0:T(8,128)(2,1)} %pack.1), channel_id=1, replica_groups=mesh['z'=8,'yh'=2,'yl'=2,'x'=4,'c'=2] {'yh','yl'}, dimensions={0} | all-to-all | bytes 1179648 | tf_op jit(solution)/shard_map/all_to_all | solution.py:435
  16.5 1.9 %collective-permute-start.10 = (bf16[256,1152]{1,0:T(8,128)(2,1)S(1)}, bf16[256,1152]{1,0:T(8,128)(2,1)S(1)}, u32[]{:S(2)}, u32[]{:S(2)}) collective-permute-start(bf16[256,1152]{1,0:T(8,128)(2,1)S(1)} %bitcast.18), channel_id=1, source_target_pairs={{0,32},{32,64},{64,96},{96,128},{128,160},{160,192},{192,224},{224... | collective-permute-start | bytes 1769480 | tf_op jit(solution)/shard_map/ppermute | solution.py:22
  18.5 0.1 collective-permute-start.7
  18.6 11.6 %collective-permute-done.10.refs_7_ = bf16[256,1152]{1,0:T(8,128)(2,1)S(1)} collective-permute-done((bf16[256,1152]{1,0:T(8,128)(2,1)S(1)}, bf16[256,1152]{1,0:T(8,128)(2,1)S(1)}, u32[]{:S(2)}, u32[]{:S(2)}) %collective-permute-start.10) | collective-permute-done | bytes 589856 | tf_op jit(solution)/shard_map/ppermute | solution.py:22
  30.2 1.9 %collective-permute-start.11 = (bf16[256,1152]{1,0:T(8,128)(2,1)S(1)}, bf16[256,1152]{1,0:T(8,128)(2,1)S(1)}, u32[]{:S(2)}, u32[]{:S(2)}) collective-permute-start(bf16[256,1152]{1,0:T(8,128)(2,1)S(1)} %collective-permute-done.10.refs_7_), channel_id=1, source_target_pairs={{0,32},{32,64},{64,96},{96,128},{128,160},{160,192},{192,224},{224... | collective-permute-start | bytes 1769480 | tf_op jit(solution)/shard_map/ppermute | solution.py:22
  32.1 0.6 collective-permute-start
  32.7 0.8 copy.16
  33.5 0.1 mul.58
  33.6 0.1 mul.62
  33.7 2.4 %collective-permute-start.8 = (bf16[256,1152]{1,0:T(8,128)(2,1)S(1)}, bf16[256,1152]{1,0:T(8,128)(2,1)}, u32[]{:S(2)}, u32[]{:S(2)}) collective-permute-start(bf16[256,1152]{1,0:T(8,128)(2,1)S(1)} %collective-permute-done.7.refs_1_), channel_id=1, source_target_pairs={{0,224},{32,0},{64,32},{96,64},{128,96},{160,128},{192,160},{224,1... | collective-permute-start | bytes 1769480 | tf_op jit(solution)/shard_map/ppermute | solution.py:22
  36.1 9.6 %collective-permute-done.11.refs_6_ = bf16[256,1152]{1,0:T(8,128)(2,1)S(1)} collective-permute-done((bf16[256,1152]{1,0:T(8,128)(2,1)S(1)}, bf16[256,1152]{1,0:T(8,128)(2,1)S(1)}, u32[]{:S(2)}, u32[]{:S(2)}) %collective-permute-start.11) | collective-permute-done | bytes 589856 | tf_op jit(solution)/shard_map/ppermute | solution.py:22
  45.7 0.7 negate_sqrt_fusion
  46.4 0.1 copy.17
  46.6 0.1 stack_broadcast_in_dim.15
  46.8 0.1 stack_broadcast_in_dim.17
  46.9 0.6 pad_maximum_fusion.2.table_ref
  47.5 2.9 %mixer_local.1 = (bf16[32,8,384]{2,1,0:T(8,128)(2,1)}, f32[128,8,128]{2,1,0:T(8,128)}, f32[128,8,128]{2,1,0:T(8,128)}) custom-call(bf16[128,128]{1,0:T(8,128)(2,1)} %x_ref.3, f32[4,8,128]{2,1,0:T(8,128)} %pad_maximum_fusion.2.table_ref, f32[2,8,128]{2,1,0:T(8,128)} %bitcast.28, bf16[2,2,8,16,64]{4,3,2,1,0:T(8,128)(2,1)} %bitcast.33), custom_call_target="tpu_custom_call" | custom-call | flops 300000000 | bytes 2000000 | tf_op jit(solution)/shard_map/mixer_local/pallas_call | solution.py:213
  50.5 9.6 %all-to-all-start = ((bf16[32,8,384]{2,1,0:T(8,128)(2,1)}), bf16[32,8,384]{2,1,0:T(8,128)(2,1)S(1)}, u32[]{:S(2)}, u32[]{:S(2)}) async-start(bf16[32,8,384]{2,1,0:T(8,128)(2,1)} %get-tuple-element.14), calls=%async_computation | async-start | bytes 393216 | tf_op jit(solution)/shard_map/all_to_all | solution.py:227
  60.1 0.9 pad_maximum_fusion.1
  61.0 0.1 collective-permute-start.1
  61.1 9.2 %all-to-all-done.ends_ref = bf16[32,8,384]{2,1,0:T(8,128)(2,1)S(1)} async-done(((bf16[32,8,384]{2,1,0:T(8,128)(2,1)}), bf16[32,8,384]{2,1,0:T(8,128)(2,1)S(1)}, u32[]{:S(2)}, u32[]{:S(2)}) %all-to-all-start) | async-done | bytes 196640 | tf_op jit(solution)/shard_map/all_to_all | solution.py:227
  70.3 0.7 copy-done.6
  70.9 4.0 %mixer_out.1 = bf16[16,144,128]{2,1,0:T(8,128)(2,1)} custom-call(s32[1]{0:T(128)} %bitcast.4.at_ref, bf16[32,8,384]{2,1,0:T(8,128)(2,1)} %copy-done.6, f32[128,8,128]{2,1,0:T(8,128)} %get-tuple-element.15.dre_ref, f32[128,8,128]{2,1,0:T(8,128)} %get-tuple-element.16.dim_ref, f32[4,8,128]{2,1,0:T(8,128)} %pad_maximum_fusion.2.table_ref, ...), custom_call_target="tpu_custom_call" | custom-call | flops 300000000 | bytes 2000000 | tf_op jit(solution)/shard_map/mixer_out/pallas_call | solution.py:231
  74.9 4.4 %all-to-all-start.1 = ((bf16[16,144,128]{2,1,0:T(8,128)(2,1)}), bf16[16,144,128]{2,1,0:T(8,128)(2,1)S(1)}, u32[]{:S(2)}, u32[]{:S(2)}) async-start(bf16[16,144,128]{2,1,0:T(8,128)(2,1)} %mixer_out.1), calls=%async_computation.1 | async-start | bytes 1179648 | tf_op jit(solution)/shard_map/all_to_all | solution.py:444
  79.3 1.2 collective-permute-start.9
  80.5 0.9 collective-permute-start.13
  81.5 3.2 %collective-permute-start.2 = (bf16[4,16,2048]{2,1,0:T(8,128)(2,1)S(1)}, bf16[4,16,2048]{2,1,0:T(8,128)(2,1)S(1)}, u32[]{:S(2)}, u32[]{:S(2)}) collective-permute-start(bf16[4,16,2048]{2,1,0:T(8,128)(2,1)S(1)} %pad_maximum_fusion.r0), channel_id=1, source_target_pairs={{0,6},{2,0},{4,2},{6,4},{1,7},{3,1},{5,3},{7,5},{8,14},{10,8},{12,... | collective-permute-start | bytes 786440 | tf_op jit(solution)/shard_map/ppermute | solution.py:22
  84.7 0.9 collective-permute-start.3
  85.5 0.9 collective-permute-start.4
  86.4 0.6 pad_add_fusion.1.at_ref
  87.1 0.6 pad_add_fusion.at_ref
  87.6 0.6 constant_dynamic-slice_fusion
  88.2 6.7 %collective-permute-done.2.r1 = bf16[4,16,2048]{2,1,0:T(8,128)(2,1)S(1)} collective-permute-done((bf16[4,16,2048]{2,1,0:T(8,128)(2,1)S(1)}, bf16[4,16,2048]{2,1,0:T(8,128)(2,1)S(1)}, u32[]{:S(2)}, u32[]{:S(2)}) %collective-permute-start.2) | collective-permute-done | bytes 262176 | tf_op jit(solution)/shard_map/ppermute | solution.py:22
  94.9 1.5 %collective-permute-done.3.r2 = bf16[4,16,2048]{2,1,0:T(8,128)(2,1)S(1)} collective-permute-done((bf16[4,16,2048]{2,1,0:T(8,128)(2,1)S(1)}, bf16[4,16,2048]{2,1,0:T(8,128)(2,1)S(1)}, u32[]{:S(2)}, u32[]{:S(2)}) %collective-permute-start.3) | collective-permute-done | bytes 262176 | tf_op jit(solution)/shard_map/ppermute | solution.py:22
  96.4 4.7 %collective-permute-done.4.r3 = bf16[4,16,2048]{2,1,0:T(8,128)(2,1)S(1)} collective-permute-done((bf16[4,16,2048]{2,1,0:T(8,128)(2,1)S(1)}, bf16[4,16,2048]{2,1,0:T(8,128)(2,1)S(1)}, u32[]{:S(2)}, u32[]{:S(2)}) %collective-permute-start.4) | collective-permute-done | bytes 262176 | tf_op jit(solution)/shard_map/ppermute | solution.py:22
  101.2 0.7 copy-done.5
  101.9 0.2 copy-done
  102.1 4.3 %edge.1 = (bf16[1,2048]{1,0:T(2,128)(2,1)}, bf16[1,2048]{1,0:T(2,128)(2,1)}) custom-call(s32[4]{0:T(128)} %pad_add_fusion.at_ref, bf16[16,144,128]{2,1,0:T(8,128)(2,1)} %copy-done, bf16[1024,2048]{1,0:T(8,128)(2,1)} %weight_ref.3, f32[1,2048]{1,0:T(1,128)} %bitcast.26, bf16[4,16,2048]{2,1,0:T(8,128)(2,1)} %copy-done.1, bf16[4,16,2048]{2,1,0:T(8,128)(2,1)} %copy-done.3, ...), custom_call_target="tpu_custom_call" | custom-call | flops 300000000 | bytes 6000000 | tf_op jit(solution)/shard_map/edge/pallas_call | solution.py:454
  106.4 2.2 %collective-permute-start.5 = (bf16[1,2048]{1,0:T(2,128)(2,1)}, bf16[1,2048]{1,0:T(2,128)(2,1)S(1)}, u32[]{:S(2)}, u32[]{:S(2)}) collective-permute-start(bf16[1,2048]{1,0:T(2,128)(2,1)} %get-tuple-element.19), channel_id=1, source_target_pairs={{0,16},{16,0},{1,17},{17,1},{2,18},{18,2},{3,19},{19,3},{4,20},{20... | collective-permute-start | bytes 12296 | tf_op jit(solution)/shard_map/ppermute | solution.py:279
  108.5 3.9 %collective-permute-start.6 = (bf16[1,2048]{1,0:T(2,128)(2,1)}, bf16[1,2048]{1,0:T(2,128)(2,1)S(1)}, u32[]{:S(2)}, u32[]{:S(2)}) collective-permute-start(bf16[1,2048]{1,0:T(2,128)(2,1)} %get-tuple-element.20), channel_id=1, source_target_pairs={{16,32},{48,64},{80,96},{112,128},{144,160},{176,192},{208,224},{3... | collective-permute-start | bytes 12296 | tf_op jit(solution)/shard_map/ppermute | solution.py:278
  112.4 5.6 %rows.1 = (bf16[256,2048]{1,0:T(8,128)(2,1)}, bf16[16,2048]{1,0:T(8,128)(2,1)}) custom-call(s32[4]{0:T(128)} %pad_add_fusion.at_ref, bf16[16,144,128]{2,1,0:T(8,128)(2,1)} %copy-done, bf16[1024,2048]{1,0:T(8,128)(2,1)} %weight_ref.3, f32[1,2048]{1,0:T(1,128)} %bitcast.27, bf16[4,16,2048]{2,1,0:T(8,128)(2,1)} %copy-done.1, bf16[4,16,2048]{2,1,0:T(8,128)(2,1)} %copy-done.3, ...), custom_call_target="tpu_custom_call" | custom-call | flops 1000000000 | bytes 6000000 | tf_op jit(solution)/shard_map/rows/pallas_call | solution.py:466
  118.1 0.5 copy-done.12
  118.7 6.6 %ffn.1 = (bf16[8,16,2048]{2,1,0:T(8,128)(2,1)}, bf16[8,16,2048]{2,1,0:T(8,128)(2,1)}) custom-call(s32[3]{0:T(128)} %pad_add_fusion.1.at_ref, bf16[256,2048]{1,0:T(8,128)(2,1)} %get-tuple-element.18.cells_ref, bf16[1,2048]{1,0:T(2,128)(2,1)} %copy-done.12, bf16[1,2048]{1,0:T(2,128)(2,1)} %copy-done.13, f32[3,384]{1,0:T(4,128)} %get-tuple-element.28.vtap_ref, ...), custom_call_target="tpu_custom_call" | custom-call | flops 1300000000 | bytes 6000000 | tf_op jit(solution)/shard_map/ffn/pallas_call | solution.py:485
  125.2 2.1 %collective-permute-done.14 = bf16[8,16,2048]{2,1,0:T(8,128)(2,1)S(1)} collective-permute-done((bf16[8,16,2048]{2,1,0:T(8,128)(2,1)}, bf16[8,16,2048]{2,1,0:T(8,128)(2,1)S(1)}, u32[]{:S(2)}, u32[]{:S(2)}) %collective-permute-start.14) | collective-permute-done | bytes 524320 | tf_op jit(solution)/shard_map/ppermute | solution.py:500
  127.4 1.2 add_convert_fusion
  128.5 13.9 %all_to_all.21 = bf16[8,16,2048]{2,1,0:T(8,128)(2,1)S(1)} all-to-all(bf16[8,16,2048]{2,1,0:T(8,128)(2,1)S(1)} %add_convert_fusion), channel_id=1, replica_groups=mesh['z'=8,'yh'=2,'yl'=2,'x'=4,'c'=2] {'yl','x'}, dimensions={0} | all-to-all | bytes 1048576 | tf_op jit(solution)/shard_map/all_to_all | solution.py:502
  142.5 0.6 add_convert_fusion.1
  (49 shorter events, 0.6 us)
Async XLA Ops:
  0.0 81.4 %copy-start.10 = (bf16[16,2048]{1,0:T(8,128)(2,1)S(1)}, bf16[16,2048]{1,0:T(8,128)(2,1)}, u32[]{:S(2)}) copy-start(bf16[16,2048]{1,0:T(8,128)(2,1)} %param.23) | copy-start | bytes 196612
  0.0 87.6 %copy-start.15 = (f32[3,768]{1,0:T(4,128)S(1)}, f32[3,768]{1,0:T(4,128)}, u32[]{:S(2)}) copy-start(f32[3,768]{1,0:T(4,128)} %param.27) | copy-start | bytes 27652
  0.0 87.6 %copy-start.14 = (f32[3,768]{1,0:T(4,128)S(1)}, f32[3,768]{1,0:T(4,128)}, u32[]{:S(2)}) copy-start(f32[3,768]{1,0:T(4,128)} %param.28) | copy-start | bytes 27652
  16.5 89.8 %copy-start.2 = (bf16[4,64,1152]{2,1,0:T(8,128)(2,1)}, bf16[4,64,1152]{2,1,0:T(8,128)(2,1)S(1)}, u32[]{:S(2)}) copy-start(bf16[4,64,1152]{2,1,0:T(8,128)(2,1)S(1)} %all_to_all.20) | copy-start | bytes 1769476
  16.5 13.6 %collective-permute-start.10 = (bf16[256,1152]{1,0:T(8,128)(2,1)S(1)}, bf16[256,1152]{1,0:T(8,128)(2,1)S(1)}, u32[]{:S(2)}, u32[]{:S(2)}) collective-permute-start(bf16[256,1152]{1,0:T(8,128)(2,1)S(1)} %bitcast.18), channel_id=1, source_target_pairs={{0,32},{32,64},{64,96},{96,128},{128,160},{160,192},{192,224},{224... | collective-permute-start | bytes 1769480 | tf_op jit(solution)/shard_map/ppermute | solution.py:22
  18.5 15.3 %collective-permute-start.7 = (bf16[256,1152]{1,0:T(8,128)(2,1)S(1)}, bf16[256,1152]{1,0:T(8,128)(2,1)S(1)}, u32[]{:S(2)}, u32[]{:S(2)}) collective-permute-start(bf16[256,1152]{1,0:T(8,128)(2,1)S(1)} %bitcast.19), channel_id=1, source_target_pairs={{0,224},{32,0},{64,32},{96,64},{128,96},{160,128},{192,160},{224,1... | collective-permute-start | bytes 1769480 | tf_op jit(solution)/shard_map/ppermute | solution.py:22
  30.2 76.2 %copy-start.7 = (bf16[256,1152]{1,0:T(8,128)(2,1)}, bf16[256,1152]{1,0:T(8,128)(2,1)S(1)}, u32[]{:S(2)}) copy-start(bf16[256,1152]{1,0:T(8,128)(2,1)S(1)} %collective-permute-done.10.refs_7_) | copy-start | bytes 1769476
  30.2 15.5 %collective-permute-start.11 = (bf16[256,1152]{1,0:T(8,128)(2,1)S(1)}, bf16[256,1152]{1,0:T(8,128)(2,1)S(1)}, u32[]{:S(2)}, u32[]{:S(2)}) collective-permute-start(bf16[256,1152]{1,0:T(8,128)(2,1)S(1)} %collective-permute-done.10.refs_7_), channel_id=1, source_target_pairs={{0,32},{32,64},{64,96},{96,128},{128,160},{160,192},{192,224},{224... | collective-permute-start | bytes 1769480 | tf_op jit(solution)/shard_map/ppermute | solution.py:22
  32.1 28.0 %collective-permute-start = (bf16[16,2048]{1,0:T(8,128)(2,1)}, bf16[16,2048]{1,0:T(8,128)(2,1)S(1)}, u32[]{:S(2)}, u32[]{:S(2)}) collective-permute-start(bf16[16,2048]{1,0:T(8,128)(2,1)} %param.23), channel_id=1, source_target_pairs={{0,8},{8,0},{1,9},{9,1},{2,10},{10,2},{3,11},{11,3},{4,12},{12,4},... | collective-permute-start | bytes 196616 | tf_op jit(solution)/shard_map/ppermute | solution.py:268
  33.7 72.6 %copy-start.8 = (bf16[256,1152]{1,0:T(8,128)(2,1)}, bf16[256,1152]{1,0:T(8,128)(2,1)S(1)}, u32[]{:S(2)}) copy-start(bf16[256,1152]{1,0:T(8,128)(2,1)S(1)} %collective-permute-done.7.refs_1_) | copy-start | bytes 1769476
  33.7 45.6 %collective-permute-start.8 = (bf16[256,1152]{1,0:T(8,128)(2,1)S(1)}, bf16[256,1152]{1,0:T(8,128)(2,1)}, u32[]{:S(2)}, u32[]{:S(2)}) collective-permute-start(bf16[256,1152]{1,0:T(8,128)(2,1)S(1)} %collective-permute-done.7.refs_1_), channel_id=1, source_target_pairs={{0,224},{32,0},{64,32},{96,64},{128,96},{160,128},{192,160},{224,1... | collective-permute-start | bytes 1769480 | tf_op jit(solution)/shard_map/ppermute | solution.py:22
  45.7 35.7 %copy-start.9 = (bf16[256,1152]{1,0:T(8,128)(2,1)}, bf16[256,1152]{1,0:T(8,128)(2,1)S(1)}, u32[]{:S(2)}) copy-start(bf16[256,1152]{1,0:T(8,128)(2,1)S(1)} %collective-permute-done.11.refs_6_) | copy-start | bytes 1769476
  45.7 34.7 %collective-permute-start.12 = (bf16[256,1152]{1,0:T(8,128)(2,1)S(1)}, bf16[256,1152]{1,0:T(8,128)(2,1)}, u32[]{:S(2)}, u32[]{:S(2)}) collective-permute-start(bf16[256,1152]{1,0:T(8,128)(2,1)S(1)} %collective-permute-done.11.refs_6_), channel_id=1, source_target_pairs={{0,32},{32,64},{64,96},{96,128},{128,160},{160,192},{192,224},{224... | collective-permute-start | bytes 1769480 | tf_op jit(solution)/shard_map/ppermute | solution.py:22
  50.5 19.8 %all-to-all-start = ((bf16[32,8,384]{2,1,0:T(8,128)(2,1)}), bf16[32,8,384]{2,1,0:T(8,128)(2,1)S(1)}, u32[]{:S(2)}, u32[]{:S(2)}) async-start(bf16[32,8,384]{2,1,0:T(8,128)(2,1)} %get-tuple-element.14), calls=%async_computation | async-start | bytes 393216 | tf_op jit(solution)/shard_map/all_to_all | solution.py:227
  61.0 20.5 %collective-permute-start.1 = (bf16[2,16,2048]{2,1,0:T(8,128)(2,1)S(1)}, bf16[2,16,2048]{2,1,0:T(8,128)(2,1)S(1)}, u32[]{:S(2)}, u32[]{:S(2)}) collective-permute-start(bf16[2,16,2048]{2,1,0:T(8,128)(2,1)S(1)} %pad_maximum_fusion.1), channel_id=1, source_target_pairs={{0,1},{1,0},{2,3},{3,2},{4,5},{5,4},{6,7},{7,6},{8,9},{9,8},{10,11... | collective-permute-start | bytes 393224 | tf_op jit(solution)/shard_map/ppermute | solution.py:269
  70.3 0.7 copy-start.6
  74.9 26.3 %all-to-all-start.1 = ((bf16[16,144,128]{2,1,0:T(8,128)(2,1)}), bf16[16,144,128]{2,1,0:T(8,128)(2,1)S(1)}, u32[]{:S(2)}, u32[]{:S(2)}) async-start(bf16[16,144,128]{2,1,0:T(8,128)(2,1)} %mixer_out.1), calls=%async_computation.1 | async-start | bytes 1179648 | tf_op jit(solution)/shard_map/all_to_all | solution.py:444
  79.3 38.8 %collective-permute-start.9 = (bf16[256,1152]{1,0:T(8,128)(2,1)}, bf16[256,1152]{1,0:T(8,128)(2,1)}, u32[]{:S(2)}, u32[]{:S(2)}) collective-permute-start(bf16[256,1152]{1,0:T(8,128)(2,1)} %collective-permute-done.8.refs_2_), channel_id=1, source_target_pairs={{0,224},{32,0},{64,32},{96,64},{128,96},{160,128},{192,160},{224,1... | collective-permute-start | bytes 1769480 | tf_op jit(solution)/shard_map/ppermute | solution.py:22
  80.5 37.6 %collective-permute-start.13 = (bf16[256,1152]{1,0:T(8,128)(2,1)}, bf16[256,1152]{1,0:T(8,128)(2,1)}, u32[]{:S(2)}, u32[]{:S(2)}) collective-permute-start(bf16[256,1152]{1,0:T(8,128)(2,1)} %collective-permute-done.12.refs_5_), channel_id=1, source_target_pairs={{0,32},{32,64},{64,96},{96,128},{128,160},{160,192},{192,224},{224... | collective-permute-start | bytes 1769480 | tf_op jit(solution)/shard_map/ppermute | solution.py:22
  81.5 19.7 %copy-start.1 = (bf16[4,16,2048]{2,1,0:T(8,128)(2,1)}, bf16[4,16,2048]{2,1,0:T(8,128)(2,1)S(1)}, u32[]{:S(2)}) copy-start(bf16[4,16,2048]{2,1,0:T(8,128)(2,1)S(1)} %pad_maximum_fusion.r0) | copy-start | bytes 786436
  81.5 13.4 %collective-permute-start.2 = (bf16[4,16,2048]{2,1,0:T(8,128)(2,1)S(1)}, bf16[4,16,2048]{2,1,0:T(8,128)(2,1)S(1)}, u32[]{:S(2)}, u32[]{:S(2)}) collective-permute-start(bf16[4,16,2048]{2,1,0:T(8,128)(2,1)S(1)} %pad_maximum_fusion.r0), channel_id=1, source_target_pairs={{0,6},{2,0},{4,2},{6,4},{1,7},{3,1},{5,3},{7,5},{8,14},{10,8},{12,... | collective-permute-start | bytes 786440 | tf_op jit(solution)/shard_map/ppermute | solution.py:22
  84.7 11.7 %collective-permute-start.3 = (bf16[4,16,2048]{2,1,0:T(8,128)(2,1)S(1)}, bf16[4,16,2048]{2,1,0:T(8,128)(2,1)S(1)}, u32[]{:S(2)}, u32[]{:S(2)}) collective-permute-start(bf16[4,16,2048]{2,1,0:T(8,128)(2,1)S(1)} %pad_maximum_fusion.r0), channel_id=1, source_target_pairs={{0,4},{2,6},{4,0},{6,2},{1,5},{3,7},{5,1},{7,3},{8,12},{10,14},{12... | collective-permute-start | bytes 786440 | tf_op jit(solution)/shard_map/ppermute | solution.py:22
  85.5 15.6 %collective-permute-start.4 = (bf16[4,16,2048]{2,1,0:T(8,128)(2,1)S(1)}, bf16[4,16,2048]{2,1,0:T(8,128)(2,1)S(1)}, u32[]{:S(2)}, u32[]{:S(2)}) collective-permute-start(bf16[4,16,2048]{2,1,0:T(8,128)(2,1)S(1)} %pad_maximum_fusion.r0), channel_id=1, source_target_pairs={{0,2},{2,4},{4,6},{6,0},{1,3},{3,5},{5,7},{7,1},{8,10},{10,12},{12... | collective-permute-start | bytes 786440 | tf_op jit(solution)/shard_map/ppermute | solution.py:22
  94.9 6.3 %copy-start.3 = (bf16[4,16,2048]{2,1,0:T(8,128)(2,1)}, bf16[4,16,2048]{2,1,0:T(8,128)(2,1)S(1)}, u32[]{:S(2)}) copy-start(bf16[4,16,2048]{2,1,0:T(8,128)(2,1)S(1)} %collective-permute-done.2.r1) | copy-start | bytes 786436
  96.4 4.8 %copy-start.4 = (bf16[4,16,2048]{2,1,0:T(8,128)(2,1)}, bf16[4,16,2048]{2,1,0:T(8,128)(2,1)S(1)}, u32[]{:S(2)}) copy-start(bf16[4,16,2048]{2,1,0:T(8,128)(2,1)S(1)} %collective-permute-done.3.r2) | copy-start | bytes 786436
  101.2 0.7 copy-start.5
  101.2 0.9 copy-start
  106.4 11.7 %collective-permute-start.5 = (bf16[1,2048]{1,0:T(2,128)(2,1)}, bf16[1,2048]{1,0:T(2,128)(2,1)S(1)}, u32[]{:S(2)}, u32[]{:S(2)}) collective-permute-start(bf16[1,2048]{1,0:T(2,128)(2,1)} %get-tuple-element.19), channel_id=1, source_target_pairs={{0,16},{16,0},{1,17},{17,1},{2,18},{18,2},{3,19},{19,3},{4,20},{20... | collective-permute-start | bytes 12296 | tf_op jit(solution)/shard_map/ppermute | solution.py:279
  108.5 9.5 %collective-permute-start.6 = (bf16[1,2048]{1,0:T(2,128)(2,1)}, bf16[1,2048]{1,0:T(2,128)(2,1)S(1)}, u32[]{:S(2)}, u32[]{:S(2)}) collective-permute-start(bf16[1,2048]{1,0:T(2,128)(2,1)} %get-tuple-element.20), channel_id=1, source_target_pairs={{16,32},{48,64},{80,96},{112,128},{144,160},{176,192},{208,224},{3... | collective-permute-start | bytes 12296 | tf_op jit(solution)/shard_map/ppermute | solution.py:278
  118.1 0.6 copy-start.12
  118.1 0.6 copy-start.13
  118.7 23.8 %copy-start.11 = (bf16[16,2048]{1,0:T(8,128)(2,1)S(1)}, bf16[16,2048]{1,0:T(8,128)(2,1)}, u32[]{:S(2)}) copy-start(bf16[16,2048]{1,0:T(8,128)(2,1)} %get-tuple-element.17) | copy-start | bytes 196612
  125.2 2.1 %collective-permute-start.14 = (bf16[8,16,2048]{2,1,0:T(8,128)(2,1)}, bf16[8,16,2048]{2,1,0:T(8,128)(2,1)S(1)}, u32[]{:S(2)}, u32[]{:S(2)}) collective-permute-start(bf16[8,16,2048]{2,1,0:T(8,128)(2,1)} %get-tuple-element.22), channel_id=1, source_target_pairs={{0,1},{1,0},{2,3},{3,2},{4,5},{5,4},{6,7},{7,6},{8,9},{9,8},{10,11... | collective-permute-start | bytes 1572872 | tf_op jit(solution)/shard_map/ppermute | solution.py:500

commit v3 on v2

--- a/solution.py
+++ b/solution.py
@@ -13,6 +13,7 @@
 SP = ("z", "yh", "yl")
 TP = ("x", "c")
 PAIR = ("yl", "x", "c")
+CHIPS = ("yl", "x")
 VMEM = pl.BlockSpec(memory_space=pltpu.VMEM)
 SMEM = pl.BlockSpec(memory_space=pltpu.SMEM)
 
@@ -227,7 +228,7 @@
     all_ends = lax.all_to_all(ends, SP, 0, 0, tiled=True)
     at = lax.axis_index(SP).astype(jnp.int32).reshape(1)
     scratch = pltpu.VMEM((rows, groups, 2 * states), jnp.float32)
-    copies = lax.axis_size(PAIR)
+    copies = lax.axis_size(CHIPS)
     return pl.pallas_call(
         mix_kernel,
         out_shape=jax.ShapeDtypeStruct(
@@ -289,9 +290,19 @@
         out_ref[k, :, 2 * half :] = down_ref[:, cut]
 
 
-def pair_gains(mixed_ref, tok):
-    parts = [mixed_ref[p, tok:, :].astype(jnp.float32) for p in range(mixed_ref.shape[0] // 2)]
-    return jnp.concatenate([g[0:1] + g[1:2] + g[2:3] for g in parts], axis=1)
+def pair_mixed(at_ref, own_ref, beside_ref, k, cut):
+    parts = []
+    for x in range(4):
+        own = own_ref[4 * k + x, cut, :].astype(jnp.float32)
+        beside = beside_ref[4 * k + x, cut, :].astype(jnp.float32)
+        north = jnp.full(own.shape, at_ref[2], jnp.int32) == 1
+        parts += [jnp.where(north, beside, own), jnp.where(north, own, beside)]
+    return jnp.concatenate(parts, axis=1)
+
+
+def pair_gains(at_ref, own_ref, beside_ref, tok):
+    g = pair_mixed(at_ref, own_ref, beside_ref, 0, slice(tok, tok + 16))
+    return g[0:1] + g[1:2] + g[2:3]
 
 
 def pair_residual(at_ref, pieces, state_ref):
@@ -304,7 +315,6 @@
 
 
 def normed_rows(mixed, resid, gains, weight, gain):
-    mixed = mixed.astype(jnp.float32)
     inverse = lax.rsqrt(jnp.mean(mixed * mixed, axis=1, keepdims=True) + norm_eps)
     normed_mix = (mixed * inverse * gains).astype(jnp.bfloat16)
     added = jnp.dot(normed_mix, weight, preferred_element_type=jnp.float32)
@@ -314,21 +324,17 @@
     return state, (wide * scale * gain).astype(jnp.bfloat16)
 
 
-def edge_kernel(at_ref, mixed_ref, weight_ref, gain_ref, r0, r1, r2, r3, *refs):
+def edge_kernel(at_ref, mixed_ref, beside_ref, weight_ref, gain_ref, r0, r1, r2, r3, *refs):
     near_ref, far_ref, state_ref = refs
     tok = mixed_ref.shape[1] - 16
-    parts = mixed_ref.shape[0] // 2
     pair_residual(at_ref, (r0, r1, r2, r3), state_ref)
     cuts = (0, slice(0, 16)), (1, slice(tok - 16, tok))
-    mixed = [
-        jnp.concatenate([mixed_ref[k * parts + p, cut, :] for p in range(parts)], axis=1)
-        for k, cut in cuts
-    ]
+    mixed = [pair_mixed(at_ref, mixed_ref, beside_ref, k, cut) for k, cut in cuts]
     resid = [state_ref[0:16, :], state_ref[2 * tok - 16 : 2 * tok, :]]
     _, normed = normed_rows(
         jnp.concatenate(mixed),
         jnp.concatenate(resid),
-        pair_gains(mixed_ref, tok),
+        pair_gains(at_ref, mixed_ref, beside_ref, tok),
         weight_ref[...],
         gain_ref[...],
     )
@@ -339,16 +345,15 @@
     far_ref[...] = jnp.where(even, first, last).astype(jnp.bfloat16)
 
 
-def rows_kernel(at_ref, mixed_ref, weight_ref, gain_ref, r0, r1, r2, r3, *refs):
+def rows_kernel(at_ref, mixed_ref, beside_ref, weight_ref, gain_ref, r0, r1, r2, r3, *refs):
     normed_ref, own_ref, state_ref = refs
     tok = mixed_ref.shape[1] - 16
-    parts = mixed_ref.shape[0] // 2
     own = own_ref.shape[0]
     pair_residual(at_ref, (r0, r1, r2, r3), state_ref)
-    gains = pair_gains(mixed_ref, tok)
+    gains = pair_gains(at_ref, mixed_ref, beside_ref, tok)
     for k in range(2):
         cut = slice(k * tok, (k + 1) * tok)
-        mixed = jnp.concatenate([mixed_ref[k * parts + p, :tok, :] for p in range(parts)], axis=1)
+        mixed = pair_mixed(at_ref, mixed_ref, beside_ref, k, slice(0, tok))
         state_ref[cut, :], normed_ref[cut, :] = normed_rows(
             mixed, state_ref[cut, :], gains, weight_ref[...], gain_ref[...]
         )
@@ -441,10 +446,12 @@
     tok_rows = mixer_input.shape[0]
     own_rows, model = residual.shape
     tp_count = lax.axis_size(TP)
-    arrived = lax.all_to_all(mixed_y, PAIR, 0, 0, tiled=True)
+    arrived = lax.all_to_all(mixed_y, CHIPS, 0, 0, tiled=True)
+    beside = lax.ppermute(arrived, "c", [(0, 1), (1, 0)])
     row_args = (
         jnp.stack([lax.axis_index(a) for a in (*PAIR, "yh")]).astype(jnp.int32),
         arrived,
+        beside,
         out_weight,
         channel_gain[None, :],
         *pair_resid,
@@ -454,10 +461,11 @@
     near, far = pl.pallas_call(
         edge_kernel,
         out_shape=(edge, edge),
-        in_specs=[SMEM] + [VMEM] * 7,
+        in_specs=[SMEM] + [VMEM] * 8,
         out_specs=(VMEM, VMEM),
         scratch_shapes=state_scratch,
         name="edge",
+compiler_params=pltpu.CompilerParams(vmem_limit_bytes=16 * 2**20),
         cost_estimate=pl.CostEstimate(
             flops=300_000_000, bytes_accessed=6_000_000, transcendentals=0
         ),
@@ -469,10 +477,11 @@
             jax.ShapeDtypeStruct((2 * tok_rows, model), jnp.bfloat16),
             jax.ShapeDtypeStruct((own_rows, model), jnp.bfloat16),
         ),
-        in_specs=[SMEM] + [VMEM] * 7,
+        in_specs=[SMEM] + [VMEM] * 8,
         out_specs=(VMEM, VMEM),
         scratch_shapes=state_scratch,
         name="rows",
+compiler_params=pltpu.CompilerParams(vmem_limit_bytes=20 * 2**20),
         cost_estimate=pl.CostEstimate(
             flops=1_000_000_000, bytes_accessed=6_000_000, transcendentals=0
         ),
@@ -493,13 +502,14 @@
             pltpu.VMEM((2 * tok_rows, model), jnp.bfloat16),
         ],
         name="ffn",
+compiler_params=pltpu.CompilerParams(vmem_limit_bytes=26 * 2**20),
         cost_estimate=pl.CostEstimate(
             flops=1_300_000_000, bytes_accessed=6_000_000, transcendentals=100_000
         ),
     )(place, cells, near, far, *taps, *pieces)
     other = lax.ppermute(send, "c", [(0, 1), (1, 0)])
     both = (keep.astype(jnp.float32) + other.astype(jnp.float32)).astype(jnp.bfloat16)
-    parts = lax.all_to_all(both, ("yl", "x"), 0, 0, tiled=True)
+    parts = lax.all_to_all(both, CHIPS, 0, 0, tiled=True)
     summed = parts.astype(jnp.float32).sum(axis=0)
     return (state_wide + summed).astype(jnp.bfloat16)
 

time: 144 us -> 122 us (0.85)
  the two profiles are of different devices: /device:TPU:32 before, /device:TPU:112 now
where the time goes in v3:
time: 122 us; the launch traced here: 121 us
  starting transfers between devices  40.5 us (33%)
  waiting for transfers between devices  27.6 us (23%)
  blocking collectives  27.1 us (22%)
  Pallas kernels  17.4 us (14%)
  local copies, waits for them, and re-layouts  4.35 us (4%)
  other arithmetic  4.08 us (3%)
    ppermute x10, starting transfers between devices, shifted(): return lax.ppermute(array, axis, [(i, (i + step) % n) for i in range(n)])  20.5 us
    ppermute x10, waiting for transfers between devices, shifted(): return lax.ppermute(array, axis, [(i, (i + step) % n) for i in range(n)])  18.9 us
    all_to_all x1, blocking collectives, body(): parts = lax.all_to_all(both, CHIPS, 0, 0, tiled=True)  14.7 us
    all_to_all x1, blocking collectives, body(): crossed = lax.all_to_all(packed, ('yh', 'yl'), 0, 0, tiled=True)  12.4 us
    all_to_all x1, starting transfers between devices, mixer_branch(): all_ends = lax.all_to_all(ends, SP, 0, 0, tiled=True)  7.71 us
    ppermute x1, starting transfers between devices, edges_passed(): near = lax.ppermute(near, 'yh', [(0, 1), (1, 0)])  5.14 us
    ppermute x1, waiting for transfers between devices, edges_passed(): far = lax.ppermute(far, ('z', 'yh'), pairs + [(j, i) for i, j in pairs])  4.74 us
    pallas_call x1, Pallas kernels, body(): pl.pallas_call(ffn_kernel, out_shape=(share, share), in_specs=[SMEM] + [V...  4.7 us
  transfers between devices with their start and end apart: 18, of which 7 were waited for; matrix products, arithmetic and copies ran while one was open for 4% of the time, Pallas kernels for 9%

profile of v3, /device:TPU:112, one launch (start us, length us, event | category | flops | bytes accessed | tf_op | source)
XLA Modules:
  0.0 121.3 jit_solution(15982828925421215183)
XLA Ops:
  0.0 1.9 %pack.1 = bf16[4,64,1152]{2,1,0:T(8,128)(2,1)} custom-call(bf16[64,768]{1,0:T(8,128)(2,1)} %value_ref.1, bf16[64,768]{1,0:T(8,128)(2,1)} %gate_ref.1, bf16[64,768]{1,0:T(8,128)(2,1)} %bitcast.27), custom_call_target="tpu_custom_call" | custom-call | tf_op jit(solution)/shard_map/pack/pallas_call | solution.py:433
  1.9 12.4 %all_to_all.20 = bf16[4,64,1152]{2,1,0:T(8,128)(2,1)S(1)} all-to-all(bf16[4,64,1152]{2,1,0:T(8,128)(2,1)} %pack.1), channel_id=1, replica_groups=mesh['z'=8,'yh'=2,'yl'=2,'x'=4,'c'=2] {'yh','yl'}, dimensions={0} | all-to-all | bytes 1179648 | tf_op jit(solution)/shard_map/all_to_all | solution.py:440
  14.4 3.1 %collective-permute-start.11 = (bf16[256,1152]{1,0:T(8,128)(2,1)S(1)}, bf16[256,1152]{1,0:T(8,128)(2,1)S(1)}, u32[]{:S(2)}, u32[]{:S(2)}) collective-permute-start(bf16[256,1152]{1,0:T(8,128)(2,1)S(1)} %bitcast.18), channel_id=1, source_target_pairs={{0,32},{32,64},{64,96},{96,128},{128,160},{160,192},{192,224},{224... | collective-permute-start | bytes 1769480 | tf_op jit(solution)/shard_map/ppermute | solution.py:23
  17.5 1.6 %collective-permute-start.1 = (bf16[16,2048]{1,0:T(8,128)(2,1)}, bf16[16,2048]{1,0:T(8,128)(2,1)S(1)}, u32[]{:S(2)}, u32[]{:S(2)}) collective-permute-start(bf16[16,2048]{1,0:T(8,128)(2,1)} %param.23), channel_id=1, source_target_pairs={{0,8},{8,0},{1,9},{9,1},{2,10},{10,2},{3,11},{11,3},{4,12},{12,4},... | collective-permute-start | bytes 196616 | tf_op jit(solution)/shard_map/ppermute | solution.py:269
  19.1 0.8 copy.16
  19.9 0.1 mul.58
  20.0 0.1 mul.62
  20.1 8.6 %collective-permute-done.11.refs_7_ = bf16[256,1152]{1,0:T(8,128)(2,1)S(1)} collective-permute-done((bf16[256,1152]{1,0:T(8,128)(2,1)S(1)}, bf16[256,1152]{1,0:T(8,128)(2,1)S(1)}, u32[]{:S(2)}, u32[]{:S(2)}) %collective-permute-start.11) | collective-permute-done | bytes 589856 | tf_op jit(solution)/shard_map/ppermute | solution.py:23
  28.8 3.7 %collective-permute-start.12 = (bf16[256,1152]{1,0:T(8,128)(2,1)S(1)}, bf16[256,1152]{1,0:T(8,128)(2,1)}, u32[]{:S(2)}, u32[]{:S(2)}) collective-permute-start(bf16[256,1152]{1,0:T(8,128)(2,1)S(1)} %collective-permute-done.11.refs_7_), channel_id=1, source_target_pairs={{0,32},{32,64},{64,96},{96,128},{128,160},{160,192},{192,224},{224... | collective-permute-start | bytes 1769480 | tf_op jit(solution)/shard_map/ppermute | solution.py:23
  32.4 0.7 negate_sqrt_fusion
  33.1 0.1 copy.17
  33.3 0.1 stack_broadcast_in_dim.15
  33.4 0.1 copy.18
  33.5 0.1 stack_broadcast_in_dim.17
  33.7 0.6 pad_maximum_fusion.2.table_ref
  34.3 3.0 %mixer_local.1 = (bf16[32,8,384]{2,1,0:T(8,128)(2,1)}, f32[128,8,128]{2,1,0:T(8,128)}, f32[128,8,128]{2,1,0:T(8,128)}) custom-call(bf16[128,128]{1,0:T(8,128)(2,1)} %x_ref.3, f32[4,8,128]{2,1,0:T(8,128)} %pad_maximum_fusion.2.table_ref, f32[2,8,128]{2,1,0:T(8,128)} %bitcast.28, bf16[2,2,8,16,64]{4,3,2,1,0:T(8,128)(2,1)} %bitcast.33), custom_call_target="tpu_custom_call" | custom-call | flops 300000000 | bytes 2000000 | tf_op jit(solution)/shard_map/mixer_local/pallas_call | solution.py:214
  37.2 7.7 %all-to-all-start = ((bf16[32,8,384]{2,1,0:T(8,128)(2,1)}), bf16[32,8,384]{2,1,0:T(8,128)(2,1)S(1)}, u32[]{:S(2)}, u32[]{:S(2)}) async-start(bf16[32,8,384]{2,1,0:T(8,128)(2,1)} %get-tuple-element.14), calls=%async_computation | async-start | bytes 393216 | tf_op jit(solution)/shard_map/all_to_all | solution.py:228
  45.0 0.6 collective-permute-start.9
  45.6 3.0 %collective-permute-start.13 = (bf16[256,1152]{1,0:T(8,128)(2,1)}, bf16[256,1152]{1,0:T(8,128)(2,1)}, u32[]{:S(2)}, u32[]{:S(2)}) collective-permute-start(bf16[256,1152]{1,0:T(8,128)(2,1)} %collective-permute-done.12.refs_6_), channel_id=1, source_target_pairs={{0,32},{32,64},{64,96},{96,128},{128,160},{160,192},{192,224},{224... | collective-permute-start | bytes 1769480 | tf_op jit(solution)/shard_map/ppermute | solution.py:23
  48.6 0.9 pad_maximum_fusion.1
  49.5 0.1 collective-permute-start.2
  49.6 1.3 %collective-permute-done.2 = bf16[2,16,2048]{2,1,0:T(8,128)(2,1)S(1)} collective-permute-done((bf16[2,16,2048]{2,1,0:T(8,128)(2,1)S(1)}, bf16[2,16,2048]{2,1,0:T(8,128)(2,1)S(1)}, u32[]{:S(2)}, u32[]{:S(2)}) %collective-permute-start.2) | collective-permute-done | bytes 131104 | tf_op jit(solution)/shard_map/ppermute | solution.py:270
  50.9 0.9 pad_maximum_fusion.r0
  51.8 2.8 %collective-permute-start.3 = (bf16[4,16,2048]{2,1,0:T(8,128)(2,1)S(1)}, bf16[4,16,2048]{2,1,0:T(8,128)(2,1)S(1)}, u32[]{:S(2)}, u32[]{:S(2)}) collective-permute-start(bf16[4,16,2048]{2,1,0:T(8,128)(2,1)S(1)} %pad_maximum_fusion.r0), channel_id=1, source_target_pairs={{0,6},{2,0},{4,2},{6,4},{1,7},{3,1},{5,3},{7,5},{8,14},{10,8},{12,... | collective-permute-start | bytes 786440 | tf_op jit(solution)/shard_map/ppermute | solution.py:23
  54.6 0.7 copy-done.3
  55.3 3.8 %mixer_out.1 = bf16[8,144,128]{2,1,0:T(8,128)(2,1)} custom-call(s32[1]{0:T(128)} %bitcast.4.at_ref, bf16[32,8,384]{2,1,0:T(8,128)(2,1)} %copy-done.3, f32[128,8,128]{2,1,0:T(8,128)} %get-tuple-element.15.dre_ref, f32[128,8,128]{2,1,0:T(8,128)} %get-tuple-element.16.dim_ref, f32[4,8,128]{2,1,0:T(8,128)} %pad_maximum_fusion.2.table_ref, ...), custom_call_target="tpu_custom_call" | custom-call | flops 300000000 | bytes 2000000 | tf_op jit(solution)/shard_map/mixer_out/pallas_call | solution.py:232
  59.1 3.4 %all-to-all-start.1 = ((bf16[8,144,128]{2,1,0:T(8,128)(2,1)}), bf16[8,144,128]{2,1,0:T(8,128)(2,1)S(1)}, u32[]{:S(2)}, u32[]{:S(2)}) async-start(bf16[8,144,128]{2,1,0:T(8,128)(2,1)} %mixer_out.1), calls=%async_computation.1 | async-start | bytes 589824 | tf_op jit(solution)/shard_map/all_to_all | solution.py:449
  62.6 0.9 collective-permute-start.10
  63.5 2.4 %collective-permute-start.14 = (bf16[256,1152]{1,0:T(8,128)(2,1)}, bf16[256,1152]{1,0:T(8,128)(2,1)}, u32[]{:S(2)}, u32[]{:S(2)}) collective-permute-start(bf16[256,1152]{1,0:T(8,128)(2,1)} %collective-permute-done.13.refs_5_), channel_id=1, source_target_pairs={{0,32},{32,64},{64,96},{96,128},{128,160},{160,192},{192,224},{224... | collective-permute-start | bytes 1769480 | tf_op jit(solution)/shard_map/ppermute | solution.py:23
  65.9 3.3 %collective-permute-start.4 = (bf16[4,16,2048]{2,1,0:T(8,128)(2,1)S(1)}, bf16[4,16,2048]{2,1,0:T(8,128)(2,1)S(1)}, u32[]{:S(2)}, u32[]{:S(2)}) collective-permute-start(bf16[4,16,2048]{2,1,0:T(8,128)(2,1)S(1)} %pad_maximum_fusion.r0), channel_id=1, source_target_pairs={{0,4},{2,6},{4,0},{6,2},{1,5},{3,7},{5,1},{7,3},{8,12},{10,14},{12... | collective-permute-start | bytes 786440 | tf_op jit(solution)/shard_map/ppermute | solution.py:23
  69.2 0.6 collective-permute-start.5
  69.8 0.7 all-to-all-done.1.mixed_ref
  70.6 0.1 pad_add_fusion.1.at_ref
  70.6 0.1 pad_add_fusion.at_ref
  70.7 5.9 %collective-permute-done.4.r2 = bf16[4,16,2048]{2,1,0:T(8,128)(2,1)S(1)} collective-permute-done((bf16[4,16,2048]{2,1,0:T(8,128)(2,1)S(1)}, bf16[4,16,2048]{2,1,0:T(8,128)(2,1)S(1)}, u32[]{:S(2)}, u32[]{:S(2)}) %collective-permute-start.4) | collective-permute-done | bytes 262176 | tf_op jit(solution)/shard_map/ppermute | solution.py:23
  76.6 4.5 %collective-permute-done.5.r3 = bf16[4,16,2048]{2,1,0:T(8,128)(2,1)S(1)} collective-permute-done((bf16[4,16,2048]{2,1,0:T(8,128)(2,1)S(1)}, bf16[4,16,2048]{2,1,0:T(8,128)(2,1)S(1)}, u32[]{:S(2)}, u32[]{:S(2)}) %collective-permute-start.5) | collective-permute-done | bytes 262176 | tf_op jit(solution)/shard_map/ppermute | solution.py:23
  81.0 2.2 %copy-done = bf16[1024,2048]{1,0:T(8,128)(2,1)S(1)} copy-done((bf16[1024,2048]{1,0:T(8,128)(2,1)S(1)}, bf16[1024,2048]{1,0:T(8,128)(2,1)}, u32[]{:S(2)}) %copy-start) | copy-done | bytes 4194328
  83.2 1.6 %edge.1 = (bf16[1,2048]{1,0:T(2,128)(2,1)S(1)}, bf16[1,2048]{1,0:T(2,128)(2,1)S(1)}) custom-call(s32[4]{0:T(128)S(1)} %pad_add_fusion.at_ref, bf16[8,144,128]{2,1,0:T(8,128)(2,1)S(1)} %all-to-all-done.1.mixed_ref, bf16[8,144,128]{2,1,0:T(8,128)(2,1)S(1)} %collective-permute-done.beside_ref, bf16[1024,2048]{1,0:T(8,128)(2,1)S(1)} %copy-done, ...), custom_call_target="tpu_custom_call" | custom-call | flops 300000000 | bytes 6000000 | tf_op jit(solution)/shard_map/edge/pallas_call | solution.py:461
  84.8 5.1 %collective-permute-start.6 = (bf16[1,2048]{1,0:T(2,128)(2,1)S(1)}, bf16[1,2048]{1,0:T(2,128)(2,1)S(1)}, u32[]{:S(2)}, u32[]{:S(2)}) collective-permute-start(bf16[1,2048]{1,0:T(2,128)(2,1)S(1)} %get-tuple-element.19), channel_id=1, source_target_pairs={{0,16},{16,0},{1,17},{17,1},{2,18},{18,2},{3,19},{19,3},{4,20},{20... | collective-permute-start | bytes 12296 | tf_op jit(solution)/shard_map/ppermute | solution.py:280
  90.0 1.9 %collective-permute-start.7 = (bf16[1,2048]{1,0:T(2,128)(2,1)S(1)}, bf16[1,2048]{1,0:T(2,128)(2,1)S(1)}, u32[]{:S(2)}, u32[]{:S(2)}) collective-permute-start(bf16[1,2048]{1,0:T(2,128)(2,1)S(1)} %get-tuple-element.20), channel_id=1, source_target_pairs={{16,32},{48,64},{80,96},{112,128},{144,160},{176,192},{208,224},{3... | collective-permute-start | bytes 12296 | tf_op jit(solution)/shard_map/ppermute | solution.py:279
  91.9 2.5 %rows.1 = (bf16[256,2048]{1,0:T(8,128)(2,1)S(1)}, bf16[16,2048]{1,0:T(8,128)(2,1)S(1)}) custom-call(s32[4]{0:T(128)S(1)} %pad_add_fusion.at_ref, bf16[8,144,128]{2,1,0:T(8,128)(2,1)S(1)} %all-to-all-done.1.mixed_ref, bf16[8,144,128]{2,1,0:T(8,128)(2,1)S(1)} %collective-permute-done.beside_ref, bf16[1024,2048]{1,0:T(8,128)(2,1)S(1)} %copy-done.1, ...), custom_call_target="tpu_custom_call" | custom-call | flops 1000000000 | bytes 6000000 | tf_op jit(solution)/shard_map/rows/pallas_call | solution.py:474
  94.4 4.7 %collective-permute-done.7.far_ref = bf16[1,2048]{1,0:T(2,128)(2,1)S(1)} collective-permute-done((bf16[1,2048]{1,0:T(2,128)(2,1)S(1)}, bf16[1,2048]{1,0:T(2,128)(2,1)S(1)}, u32[]{:S(2)}, u32[]{:S(2)}) %collective-permute-start.7) | collective-permute-done | bytes 4128 | tf_op jit(solution)/shard_map/ppermute | solution.py:279
  99.1 4.7 %ffn.1 = (bf16[8,16,2048]{2,1,0:T(8,128)(2,1)S(1)}, bf16[8,16,2048]{2,1,0:T(8,128)(2,1)S(1)}) custom-call(s32[3]{0:T(128)S(1)} %pad_add_fusion.1.at_ref, bf16[256,2048]{1,0:T(8,128)(2,1)S(1)} %get-tuple-element.18.cells_ref, bf16[1,2048]{1,0:T(2,128)(2,1)S(1)} %collective-permute-done.6.near_ref, bf16[1,2048]{1,0:T(2,128)(2,1)S(1)} %collective-permute-done.7.far_ref, ...), custom_call_target="tpu_custom_call" | custom-call | flops 1300000000 | bytes 6000000 | tf_op jit(solution)/shard_map/ffn/pallas_call | solution.py:494
  103.8 0.1 collective-permute-start.15
  103.9 1.9 %collective-permute-done.15 = bf16[8,16,2048]{2,1,0:T(8,128)(2,1)S(1)} collective-permute-done((bf16[8,16,2048]{2,1,0:T(8,128)(2,1)S(1)}, bf16[8,16,2048]{2,1,0:T(8,128)(2,1)S(1)}, u32[]{:S(2)}, u32[]{:S(2)}) %collective-permute-start.15) | collective-permute-done | bytes 524320 | tf_op jit(solution)/shard_map/ppermute | solution.py:510
  105.8 0.1 add_convert_fusion
  105.9 14.7 %all_to_all.21 = bf16[8,16,2048]{2,1,0:T(8,128)(2,1)S(1)} all-to-all(bf16[8,16,2048]{2,1,0:T(8,128)(2,1)S(1)} %add_convert_fusion), channel_id=1, replica_groups=mesh['z'=8,'yh'=2,'yl'=2,'x'=4,'c'=2] {'yl','x'}, dimensions={0} | all-to-all | bytes 1048576 | tf_op jit(solution)/shard_map/all_to_all | solution.py:512
  120.7 0.7 add_convert_fusion.1
  (31 shorter events, 0.4 us)
Async XLA Ops:
  0.0 70.7 %copy-start.5 = (f32[3,768]{1,0:T(4,128)S(1)}, f32[3,768]{1,0:T(4,128)}, u32[]{:S(2)}) copy-start(f32[3,768]{1,0:T(4,128)} %param.27) | copy-start | bytes 27652
  0.0 70.7 %copy-start.4 = (f32[3,768]{1,0:T(4,128)S(1)}, f32[3,768]{1,0:T(4,128)}, u32[]{:S(2)}) copy-start(f32[3,768]{1,0:T(4,128)} %param.28) | copy-start | bytes 27652
  0.0 81.0 %copy-start.2 = (f32[2048]{0:T(1024)S(1)}, f32[2048]{0:T(1024)}, u32[]{:S(2)}) copy-start(f32[2048]{0:T(1024)} %param.24) | copy-start | bytes 24580
  14.4 14.4 %collective-permute-start.11 = (bf16[256,1152]{1,0:T(8,128)(2,1)S(1)}, bf16[256,1152]{1,0:T(8,128)(2,1)S(1)}, u32[]{:S(2)}, u32[]{:S(2)}) collective-permute-start(bf16[256,1152]{1,0:T(8,128)(2,1)S(1)} %bitcast.18), channel_id=1, source_target_pairs={{0,32},{32,64},{64,96},{96,128},{128,160},{160,192},{192,224},{224... | collective-permute-start | bytes 1769480 | tf_op jit(solution)/shard_map/ppermute | solution.py:23
  17.5 31.1 %collective-permute-start.1 = (bf16[16,2048]{1,0:T(8,128)(2,1)}, bf16[16,2048]{1,0:T(8,128)(2,1)S(1)}, u32[]{:S(2)}, u32[]{:S(2)}) collective-permute-start(bf16[16,2048]{1,0:T(8,128)(2,1)} %param.23), channel_id=1, source_target_pairs={{0,8},{8,0},{1,9},{9,1},{2,10},{10,2},{3,11},{11,3},{4,12},{12,4},... | collective-permute-start | bytes 196616 | tf_op jit(solution)/shard_map/ppermute | solution.py:269
  20.1 24.8 %collective-permute-start.8 = (bf16[256,1152]{1,0:T(8,128)(2,1)S(1)}, bf16[256,1152]{1,0:T(8,128)(2,1)S(1)}, u32[]{:S(2)}, u32[]{:S(2)}) collective-permute-start(bf16[256,1152]{1,0:T(8,128)(2,1)S(1)} %bitcast.19), channel_id=1, source_target_pairs={{0,224},{32,0},{64,32},{96,64},{128,96},{160,128},{192,160},{224,1... | collective-permute-start | bytes 1769480 | tf_op jit(solution)/shard_map/ppermute | solution.py:23
  28.8 16.9 %collective-permute-start.12 = (bf16[256,1152]{1,0:T(8,128)(2,1)S(1)}, bf16[256,1152]{1,0:T(8,128)(2,1)}, u32[]{:S(2)}, u32[]{:S(2)}) collective-permute-start(bf16[256,1152]{1,0:T(8,128)(2,1)S(1)} %collective-permute-done.11.refs_7_), channel_id=1, source_target_pairs={{0,32},{32,64},{64,96},{96,128},{128,160},{160,192},{192,224},{224... | collective-permute-start | bytes 1769480 | tf_op jit(solution)/shard_map/ppermute | solution.py:23
  37.2 17.4 %all-to-all-start = ((bf16[32,8,384]{2,1,0:T(8,128)(2,1)}), bf16[32,8,384]{2,1,0:T(8,128)(2,1)S(1)}, u32[]{:S(2)}, u32[]{:S(2)}) async-start(bf16[32,8,384]{2,1,0:T(8,128)(2,1)} %get-tuple-element.14), calls=%async_computation | async-start | bytes 393216 | tf_op jit(solution)/shard_map/all_to_all | solution.py:228
  45.0 17.6 %collective-permute-start.9 = (bf16[256,1152]{1,0:T(8,128)(2,1)S(1)}, bf16[256,1152]{1,0:T(8,128)(2,1)}, u32[]{:S(2)}, u32[]{:S(2)}) collective-permute-start(bf16[256,1152]{1,0:T(8,128)(2,1)S(1)} %collective-permute-done.8.refs_1_), channel_id=1, source_target_pairs={{0,224},{32,0},{64,32},{96,64},{128,96},{160,128},{192,160},{224,1... | collective-permute-start | bytes 1769480 | tf_op jit(solution)/shard_map/ppermute | solution.py:23
  45.6 17.9 %collective-permute-start.13 = (bf16[256,1152]{1,0:T(8,128)(2,1)}, bf16[256,1152]{1,0:T(8,128)(2,1)}, u32[]{:S(2)}, u32[]{:S(2)}) collective-permute-start(bf16[256,1152]{1,0:T(8,128)(2,1)} %collective-permute-done.12.refs_6_), channel_id=1, source_target_pairs={{0,32},{32,64},{64,96},{96,128},{128,160},{160,192},{192,224},{224... | collective-permute-start | bytes 1769480 | tf_op jit(solution)/shard_map/ppermute | solution.py:23
  49.5 1.4 %collective-permute-start.2 = (bf16[2,16,2048]{2,1,0:T(8,128)(2,1)S(1)}, bf16[2,16,2048]{2,1,0:T(8,128)(2,1)S(1)}, u32[]{:S(2)}, u32[]{:S(2)}) collective-permute-start(bf16[2,16,2048]{2,1,0:T(8,128)(2,1)S(1)} %pad_maximum_fusion.1), channel_id=1, source_target_pairs={{0,1},{1,0},{2,3},{3,2},{4,5},{5,4},{6,7},{7,6},{8,9},{9,8},{10,11... | collective-permute-start | bytes 393224 | tf_op jit(solution)/shard_map/ppermute | solution.py:270
  51.8 18.0 %collective-permute-start.3 = (bf16[4,16,2048]{2,1,0:T(8,128)(2,1)S(1)}, bf16[4,16,2048]{2,1,0:T(8,128)(2,1)S(1)}, u32[]{:S(2)}, u32[]{:S(2)}) collective-permute-start(bf16[4,16,2048]{2,1,0:T(8,128)(2,1)S(1)} %pad_maximum_fusion.r0), channel_id=1, source_target_pairs={{0,6},{2,0},{4,2},{6,4},{1,7},{3,1},{5,3},{7,5},{8,14},{10,8},{12,... | collective-permute-start | bytes 786440 | tf_op jit(solution)/shard_map/ppermute | solution.py:23
  54.6 0.7 copy-start.3
  59.1 11.4 %all-to-all-start.1 = ((bf16[8,144,128]{2,1,0:T(8,128)(2,1)}), bf16[8,144,128]{2,1,0:T(8,128)(2,1)S(1)}, u32[]{:S(2)}, u32[]{:S(2)}) async-start(bf16[8,144,128]{2,1,0:T(8,128)(2,1)} %mixer_out.1), calls=%async_computation.1 | async-start | bytes 589824 | tf_op jit(solution)/shard_map/all_to_all | solution.py:449
  62.6 36.5 %collective-permute-start.10 = (bf16[256,1152]{1,0:T(8,128)(2,1)}, bf16[256,1152]{1,0:T(8,128)(2,1)}, u32[]{:S(2)}, u32[]{:S(2)}) collective-permute-start(bf16[256,1152]{1,0:T(8,128)(2,1)} %collective-permute-done.9.refs_2_), channel_id=1, source_target_pairs={{0,224},{32,0},{64,32},{96,64},{128,96},{160,128},{192,160},{224,1... | collective-permute-start | bytes 1769480 | tf_op jit(solution)/shard_map/ppermute | solution.py:23
  63.5 35.6 %collective-permute-start.14 = (bf16[256,1152]{1,0:T(8,128)(2,1)}, bf16[256,1152]{1,0:T(8,128)(2,1)}, u32[]{:S(2)}, u32[]{:S(2)}) collective-permute-start(bf16[256,1152]{1,0:T(8,128)(2,1)} %collective-permute-done.13.refs_5_), channel_id=1, source_target_pairs={{0,32},{32,64},{64,96},{96,128},{128,160},{160,192},{192,224},{224... | collective-permute-start | bytes 1769480 | tf_op jit(solution)/shard_map/ppermute | solution.py:23
  65.9 10.7 %collective-permute-start.4 = (bf16[4,16,2048]{2,1,0:T(8,128)(2,1)S(1)}, bf16[4,16,2048]{2,1,0:T(8,128)(2,1)S(1)}, u32[]{:S(2)}, u32[]{:S(2)}) collective-permute-start(bf16[4,16,2048]{2,1,0:T(8,128)(2,1)S(1)} %pad_maximum_fusion.r0), channel_id=1, source_target_pairs={{0,4},{2,6},{4,0},{6,2},{1,5},{3,7},{5,1},{7,3},{8,12},{10,14},{12... | collective-permute-start | bytes 786440 | tf_op jit(solution)/shard_map/ppermute | solution.py:23
  69.2 11.8 %collective-permute-start.5 = (bf16[4,16,2048]{2,1,0:T(8,128)(2,1)S(1)}, bf16[4,16,2048]{2,1,0:T(8,128)(2,1)S(1)}, u32[]{:S(2)}, u32[]{:S(2)}) collective-permute-start(bf16[4,16,2048]{2,1,0:T(8,128)(2,1)S(1)} %pad_maximum_fusion.r0), channel_id=1, source_target_pairs={{0,2},{2,4},{4,6},{6,0},{1,3},{3,5},{5,7},{7,1},{8,10},{10,12},{12... | collective-permute-start | bytes 786440 | tf_op jit(solution)/shard_map/ppermute | solution.py:23
  70.6 10.5 %collective-permute-start = (bf16[8,144,128]{2,1,0:T(8,128)(2,1)S(1)}, bf16[8,144,128]{2,1,0:T(8,128)(2,1)S(1)}, u32[]{:S(2)}, u32[]{:S(2)}) collective-permute-start(bf16[8,144,128]{2,1,0:T(8,128)(2,1)S(1)} %all-to-all-done.1.mixed_ref), channel_id=1, source_target_pairs={{0,1},{1,0},{2,3},{3,2},{4,5},{5,4},{6,7},{7,6},{8,9},{9,8},{10,11... | collective-permute-start | bytes 884744 | tf_op jit(solution)/shard_map/ppermute | solution.py:450
  81.0 2.2 %copy-start = (bf16[1024,2048]{1,0:T(8,128)(2,1)S(1)}, bf16[1024,2048]{1,0:T(8,128)(2,1)}, u32[]{:S(2)}) copy-start(bf16[1024,2048]{1,0:T(8,128)(2,1)} %weight_ref.3) | copy-start | bytes 12582916
  83.2 8.6 %copy-start.1 = (bf16[1024,2048]{1,0:T(8,128)(2,1)S(1)}, bf16[1024,2048]{1,0:T(8,128)(2,1)}, u32[]{:S(2)}) copy-start(bf16[1024,2048]{1,0:T(8,128)(2,1)} %weight_ref.3) | copy-start | bytes 12582916
  84.8 9.5 %collective-permute-start.6 = (bf16[1,2048]{1,0:T(2,128)(2,1)S(1)}, bf16[1,2048]{1,0:T(2,128)(2,1)S(1)}, u32[]{:S(2)}, u32[]{:S(2)}) collective-permute-start(bf16[1,2048]{1,0:T(2,128)(2,1)S(1)} %get-tuple-element.19), channel_id=1, source_target_pairs={{0,16},{16,0},{1,17},{17,1},{2,18},{18,2},{3,19},{19,3},{4,20},{20... | collective-permute-start | bytes 12296 | tf_op jit(solution)/shard_map/ppermute | solution.py:280
  90.0 9.1 %collective-permute-start.7 = (bf16[1,2048]{1,0:T(2,128)(2,1)S(1)}, bf16[1,2048]{1,0:T(2,128)(2,1)S(1)}, u32[]{:S(2)}, u32[]{:S(2)}) collective-permute-start(bf16[1,2048]{1,0:T(2,128)(2,1)S(1)} %get-tuple-element.20), channel_id=1, source_target_pairs={{16,32},{48,64},{80,96},{112,128},{144,160},{176,192},{208,224},{3... | collective-permute-start | bytes 12296 | tf_op jit(solution)/shard_map/ppermute | solution.py:279
  103.8 2.0 %collective-permute-start.15 = (bf16[8,16,2048]{2,1,0:T(8,128)(2,1)S(1)}, bf16[8,16,2048]{2,1,0:T(8,128)(2,1)S(1)}, u32[]{:S(2)}, u32[]{:S(2)}) collective-permute-start(bf16[8,16,2048]{2,1,0:T(8,128)(2,1)S(1)} %get-tuple-element.22), channel_id=1, source_target_pairs={{0,1},{1,0},{2,3},{3,2},{4,5},{5,4},{6,7},{7,6},{8,9},{9,8},{10,11... | collective-permute-start | bytes 1572872 | tf_op jit(solution)/shard_map/ppermute | solution.py:510

commit v4 on v3

--- a/solution.py
+++ b/solution.py
@@ -182,7 +182,7 @@
     high = gain_ref[...].astype(jnp.bfloat16).astype(jnp.float32)
     mid = (gain_ref[...] - high).astype(jnp.bfloat16).astype(jnp.float32)
     low = gain_ref[...] - high - mid
-    row = lax.broadcasted_iota(jnp.int32, (16, channels), 0)
+    row = lax.broadcasted_iota(jnp.int32, (8, channels), 0)
     tail = jnp.zeros(row.shape, jnp.float32)
     for k, part in enumerate((high, mid, low)):
         tail = jnp.where(row == k, jnp.broadcast_to(part, row.shape), tail)
@@ -232,7 +232,7 @@
     return pl.pallas_call(
         mix_kernel,
         out_shape=jax.ShapeDtypeStruct(
-            (copies, rows + 16, mixer_input.shape[1]), jnp.bfloat16
+            (copies, rows + 8, mixer_input.shape[1]), jnp.bfloat16
         ),
         in_specs=[SMEM] + [VMEM] * 9,
         out_specs=VMEM,
@@ -301,7 +301,7 @@
 
 
 def pair_gains(at_ref, own_ref, beside_ref, tok):
-    g = pair_mixed(at_ref, own_ref, beside_ref, 0, slice(tok, tok + 16))
+    g = pair_mixed(at_ref, own_ref, beside_ref, 0, slice(tok, tok + 8))
     return g[0:1] + g[1:2] + g[2:3]
 
 
@@ -326,7 +326,7 @@
 
 def edge_kernel(at_ref, mixed_ref, beside_ref, weight_ref, gain_ref, r0, r1, r2, r3, *refs):
     near_ref, far_ref, state_ref = refs
-    tok = mixed_ref.shape[1] - 16
+    tok = mixed_ref.shape[1] - 8
     pair_residual(at_ref, (r0, r1, r2, r3), state_ref)
     cuts = (0, slice(0, 16)), (1, slice(tok - 16, tok))
     mixed = [pair_mixed(at_ref, mixed_ref, beside_ref, k, cut) for k, cut in cuts]
@@ -347,7 +347,7 @@
 
 def rows_kernel(at_ref, mixed_ref, beside_ref, weight_ref, gain_ref, r0, r1, r2, r3, *refs):
     normed_ref, own_ref, state_ref = refs
-    tok = mixed_ref.shape[1] - 16
+    tok = mixed_ref.shape[1] - 8
     own = own_ref.shape[0]
     pair_residual(at_ref, (r0, r1, r2, r3), state_ref)
     gains = pair_gains(at_ref, mixed_ref, beside_ref, tok)

time: 122 us -> 122 us (level)
  no operation moved by 1% of the time
where the time goes in v4:
time: 122 us; the launch traced here: 121 us
  starting transfers between devices  40.5 us (33%)
  waiting for transfers between devices  27.5 us (23%)
  blocking collectives  27.3 us (22%)
  Pallas kernels  17.4 us (14%)
  local copies, waits for them, and re-layouts  4.36 us (4%)
  other arithmetic  4.08 us (3%)
    ppermute x10, starting transfers between devices, shifted(): return lax.ppermute(array, axis, [(i, (i + step) % n) for i in range(n)])  20.5 us
    ppermute x10, waiting for transfers between devices, shifted(): return lax.ppermute(array, axis, [(i, (i + step) % n) for i in range(n)])  19.1 us
    all_to_all x1, blocking collectives, body(): parts = lax.all_to_all(both, CHIPS, 0, 0, tiled=True)  14.8 us
    all_to_all x1, blocking collectives, body(): crossed = lax.all_to_all(packed, ('yh', 'yl'), 0, 0, tiled=True)  12.4 us
    all_to_all x1, starting transfers between devices, mixer_branch(): all_ends = lax.all_to_all(ends, SP, 0, 0, tiled=True)  7.71 us
    ppermute x1, starting transfers between devices, edges_passed(): near = lax.ppermute(near, 'yh', [(0, 1), (1, 0)])  5.15 us
    ppermute x1, waiting for transfers between devices, edges_passed(): far = lax.ppermute(far, ('z', 'yh'), pairs + [(j, i) for i, j in pairs])  4.74 us
    pallas_call x1, Pallas kernels, body(): pl.pallas_call(ffn_kernel, out_shape=(share, share), in_specs=[SMEM] + [V...  4.7 us
  transfers between devices with their start and end apart: 18, of which 7 were waited for; matrix products, arithmetic and copies ran while one was open for 4% of the time, Pallas kernels for 9%

profile of v4, /device:TPU:112, one launch (start us, length us, event | category | flops | bytes accessed | tf_op | source)
XLA Modules:
  0.0 121.3 jit_solution(16256482052035400326)
XLA Ops:
  0.0 1.9 %pack.1 = bf16[4,64,1152]{2,1,0:T(8,128)(2,1)} custom-call(bf16[64,768]{1,0:T(8,128)(2,1)} %value_ref.1, bf16[64,768]{1,0:T(8,128)(2,1)} %gate_ref.1, bf16[64,768]{1,0:T(8,128)(2,1)} %bitcast.27), custom_call_target="tpu_custom_call" | custom-call | tf_op jit(solution)/shard_map/pack/pallas_call | solution.py:433
  1.9 12.4 %all_to_all.20 = bf16[4,64,1152]{2,1,0:T(8,128)(2,1)S(1)} all-to-all(bf16[4,64,1152]{2,1,0:T(8,128)(2,1)} %pack.1), channel_id=1, replica_groups=mesh['z'=8,'yh'=2,'yl'=2,'x'=4,'c'=2] {'yh','yl'}, dimensions={0} | all-to-all | bytes 1179648 | tf_op jit(solution)/shard_map/all_to_all | solution.py:440
  14.4 3.1 %collective-permute-start.11 = (bf16[256,1152]{1,0:T(8,128)(2,1)S(1)}, bf16[256,1152]{1,0:T(8,128)(2,1)S(1)}, u32[]{:S(2)}, u32[]{:S(2)}) collective-permute-start(bf16[256,1152]{1,0:T(8,128)(2,1)S(1)} %bitcast.18), channel_id=1, source_target_pairs={{0,32},{32,64},{64,96},{96,128},{128,160},{160,192},{192,224},{224... | collective-permute-start | bytes 1769480 | tf_op jit(solution)/shard_map/ppermute | solution.py:23
  17.5 1.6 %collective-permute-start.1 = (bf16[16,2048]{1,0:T(8,128)(2,1)}, bf16[16,2048]{1,0:T(8,128)(2,1)S(1)}, u32[]{:S(2)}, u32[]{:S(2)}) collective-permute-start(bf16[16,2048]{1,0:T(8,128)(2,1)} %param.23), channel_id=1, source_target_pairs={{0,8},{8,0},{1,9},{9,1},{2,10},{10,2},{3,11},{11,3},{4,12},{12,4},... | collective-permute-start | bytes 196616 | tf_op jit(solution)/shard_map/ppermute | solution.py:269
  19.1 0.8 copy.16
  19.9 0.1 mul.58
  20.0 0.1 mul.62
  20.1 8.6 %collective-permute-done.11.refs_7_ = bf16[256,1152]{1,0:T(8,128)(2,1)S(1)} collective-permute-done((bf16[256,1152]{1,0:T(8,128)(2,1)S(1)}, bf16[256,1152]{1,0:T(8,128)(2,1)S(1)}, u32[]{:S(2)}, u32[]{:S(2)}) %collective-permute-start.11) | collective-permute-done | bytes 589856 | tf_op jit(solution)/shard_map/ppermute | solution.py:23
  28.8 3.7 %collective-permute-start.12 = (bf16[256,1152]{1,0:T(8,128)(2,1)S(1)}, bf16[256,1152]{1,0:T(8,128)(2,1)}, u32[]{:S(2)}, u32[]{:S(2)}) collective-permute-start(bf16[256,1152]{1,0:T(8,128)(2,1)S(1)} %collective-permute-done.11.refs_7_), channel_id=1, source_target_pairs={{0,32},{32,64},{64,96},{96,128},{128,160},{160,192},{192,224},{224... | collective-permute-start | bytes 1769480 | tf_op jit(solution)/shard_map/ppermute | solution.py:23
  32.4 0.7 negate_sqrt_fusion
  33.1 0.1 copy.17
  33.3 0.1 stack_broadcast_in_dim.15
  33.4 0.1 copy.18
  33.5 0.1 stack_broadcast_in_dim.17
  33.7 0.6 pad_maximum_fusion.2.table_ref
  34.3 3.0 %mixer_local.1 = (bf16[32,8,384]{2,1,0:T(8,128)(2,1)}, f32[128,8,128]{2,1,0:T(8,128)}, f32[128,8,128]{2,1,0:T(8,128)}) custom-call(bf16[128,128]{1,0:T(8,128)(2,1)} %x_ref.3, f32[4,8,128]{2,1,0:T(8,128)} %pad_maximum_fusion.2.table_ref, f32[2,8,128]{2,1,0:T(8,128)} %bitcast.28, bf16[2,2,8,16,64]{4,3,2,1,0:T(8,128)(2,1)} %bitcast.33), custom_call_target="tpu_custom_call" | custom-call | flops 300000000 | bytes 2000000 | tf_op jit(solution)/shard_map/mixer_local/pallas_call | solution.py:214
  37.2 7.7 %all-to-all-start = ((bf16[32,8,384]{2,1,0:T(8,128)(2,1)}), bf16[32,8,384]{2,1,0:T(8,128)(2,1)S(1)}, u32[]{:S(2)}, u32[]{:S(2)}) async-start(bf16[32,8,384]{2,1,0:T(8,128)(2,1)} %get-tuple-element.14), calls=%async_computation | async-start | bytes 393216 | tf_op jit(solution)/shard_map/all_to_all | solution.py:228
  45.0 0.6 collective-permute-start.9
  45.6 3.0 %collective-permute-start.13 = (bf16[256,1152]{1,0:T(8,128)(2,1)}, bf16[256,1152]{1,0:T(8,128)(2,1)}, u32[]{:S(2)}, u32[]{:S(2)}) collective-permute-start(bf16[256,1152]{1,0:T(8,128)(2,1)} %collective-permute-done.12.refs_6_), channel_id=1, source_target_pairs={{0,32},{32,64},{64,96},{96,128},{128,160},{160,192},{192,224},{224... | collective-permute-start | bytes 1769480 | tf_op jit(solution)/shard_map/ppermute | solution.py:23
  48.6 0.9 pad_maximum_fusion.1
  49.5 0.1 collective-permute-start.2
  49.6 1.3 %collective-permute-done.2 = bf16[2,16,2048]{2,1,0:T(8,128)(2,1)S(1)} collective-permute-done((bf16[2,16,2048]{2,1,0:T(8,128)(2,1)S(1)}, bf16[2,16,2048]{2,1,0:T(8,128)(2,1)S(1)}, u32[]{:S(2)}, u32[]{:S(2)}) %collective-permute-start.2) | collective-permute-done | bytes 131104 | tf_op jit(solution)/shard_map/ppermute | solution.py:270
  50.9 0.9 pad_maximum_fusion.r0
  51.8 2.8 %collective-permute-start.3 = (bf16[4,16,2048]{2,1,0:T(8,128)(2,1)S(1)}, bf16[4,16,2048]{2,1,0:T(8,128)(2,1)S(1)}, u32[]{:S(2)}, u32[]{:S(2)}) collective-permute-start(bf16[4,16,2048]{2,1,0:T(8,128)(2,1)S(1)} %pad_maximum_fusion.r0), channel_id=1, source_target_pairs={{0,6},{2,0},{4,2},{6,4},{1,7},{3,1},{5,3},{7,5},{8,14},{10,8},{12,... | collective-permute-start | bytes 786440 | tf_op jit(solution)/shard_map/ppermute | solution.py:23
  54.6 0.7 copy-done.3
  55.3 3.8 %mixer_out.1 = bf16[8,136,128]{2,1,0:T(8,128)(2,1)} custom-call(s32[1]{0:T(128)} %bitcast.4.at_ref, bf16[32,8,384]{2,1,0:T(8,128)(2,1)} %copy-done.3, f32[128,8,128]{2,1,0:T(8,128)} %get-tuple-element.15.dre_ref, f32[128,8,128]{2,1,0:T(8,128)} %get-tuple-element.16.dim_ref, f32[4,8,128]{2,1,0:T(8,128)} %pad_maximum_fusion.2.table_ref, ...), custom_call_target="tpu_custom_call" | custom-call | flops 300000000 | bytes 2000000 | tf_op jit(solution)/shard_map/mixer_out/pallas_call | solution.py:232
  59.1 3.4 %all-to-all-start.1 = ((bf16[8,136,128]{2,1,0:T(8,128)(2,1)}), bf16[8,136,128]{2,1,0:T(8,128)(2,1)S(1)}, u32[]{:S(2)}, u32[]{:S(2)}) async-start(bf16[8,136,128]{2,1,0:T(8,128)(2,1)} %mixer_out.1), calls=%async_computation.1 | async-start | bytes 557056 | tf_op jit(solution)/shard_map/all_to_all | solution.py:449
  62.6 0.9 collective-permute-start.10
  63.5 2.4 %collective-permute-start.14 = (bf16[256,1152]{1,0:T(8,128)(2,1)}, bf16[256,1152]{1,0:T(8,128)(2,1)}, u32[]{:S(2)}, u32[]{:S(2)}) collective-permute-start(bf16[256,1152]{1,0:T(8,128)(2,1)} %collective-permute-done.13.refs_5_), channel_id=1, source_target_pairs={{0,32},{32,64},{64,96},{96,128},{128,160},{160,192},{192,224},{224... | collective-permute-start | bytes 1769480 | tf_op jit(solution)/shard_map/ppermute | solution.py:23
  65.9 3.3 %collective-permute-start.4 = (bf16[4,16,2048]{2,1,0:T(8,128)(2,1)S(1)}, bf16[4,16,2048]{2,1,0:T(8,128)(2,1)S(1)}, u32[]{:S(2)}, u32[]{:S(2)}) collective-permute-start(bf16[4,16,2048]{2,1,0:T(8,128)(2,1)S(1)} %pad_maximum_fusion.r0), channel_id=1, source_target_pairs={{0,4},{2,6},{4,0},{6,2},{1,5},{3,7},{5,1},{7,3},{8,12},{10,14},{12... | collective-permute-start | bytes 786440 | tf_op jit(solution)/shard_map/ppermute | solution.py:23
  69.2 0.6 collective-permute-start.5
  69.8 0.5 all-to-all-done.1.mixed_ref
  70.3 0.1 pad_add_fusion.1.at_ref
  70.3 0.1 pad_add_fusion.at_ref
  70.4 6.1 %collective-permute-done.4.r2 = bf16[4,16,2048]{2,1,0:T(8,128)(2,1)S(1)} collective-permute-done((bf16[4,16,2048]{2,1,0:T(8,128)(2,1)S(1)}, bf16[4,16,2048]{2,1,0:T(8,128)(2,1)S(1)}, u32[]{:S(2)}, u32[]{:S(2)}) %collective-permute-start.4) | collective-permute-done | bytes 262176 | tf_op jit(solution)/shard_map/ppermute | solution.py:23
  76.6 4.3 %collective-permute-done.5.r3 = bf16[4,16,2048]{2,1,0:T(8,128)(2,1)S(1)} collective-permute-done((bf16[4,16,2048]{2,1,0:T(8,128)(2,1)S(1)}, bf16[4,16,2048]{2,1,0:T(8,128)(2,1)S(1)}, u32[]{:S(2)}, u32[]{:S(2)}) %collective-permute-start.5) | collective-permute-done | bytes 262176 | tf_op jit(solution)/shard_map/ppermute | solution.py:23
  80.9 2.2 %copy-done = bf16[1024,2048]{1,0:T(8,128)(2,1)S(1)} copy-done((bf16[1024,2048]{1,0:T(8,128)(2,1)S(1)}, bf16[1024,2048]{1,0:T(8,128)(2,1)}, u32[]{:S(2)}) %copy-start) | copy-done | bytes 4194328
  83.1 1.6 %edge.1 = (bf16[1,2048]{1,0:T(2,128)(2,1)S(1)}, bf16[1,2048]{1,0:T(2,128)(2,1)S(1)}) custom-call(s32[4]{0:T(128)S(1)} %pad_add_fusion.at_ref, bf16[8,136,128]{2,1,0:T(8,128)(2,1)S(1)} %all-to-all-done.1.mixed_ref, bf16[8,136,128]{2,1,0:T(8,128)(2,1)S(1)} %collective-permute-done.beside_ref, bf16[1024,2048]{1,0:T(8,128)(2,1)S(1)} %copy-done, ...), custom_call_target="tpu_custom_call" | custom-call | flops 300000000 | bytes 6000000 | tf_op jit(solution)/shard_map/edge/pallas_call | solution.py:461
  84.6 5.1 %collective-permute-start.6 = (bf16[1,2048]{1,0:T(2,128)(2,1)S(1)}, bf16[1,2048]{1,0:T(2,128)(2,1)S(1)}, u32[]{:S(2)}, u32[]{:S(2)}) collective-permute-start(bf16[1,2048]{1,0:T(2,128)(2,1)S(1)} %get-tuple-element.19), channel_id=1, source_target_pairs={{0,16},{16,0},{1,17},{17,1},{2,18},{18,2},{3,19},{19,3},{4,20},{20... | collective-permute-start | bytes 12296 | tf_op jit(solution)/shard_map/ppermute | solution.py:280
  89.8 1.9 %collective-permute-start.7 = (bf16[1,2048]{1,0:T(2,128)(2,1)S(1)}, bf16[1,2048]{1,0:T(2,128)(2,1)S(1)}, u32[]{:S(2)}, u32[]{:S(2)}) collective-permute-start(bf16[1,2048]{1,0:T(2,128)(2,1)S(1)} %get-tuple-element.20), channel_id=1, source_target_pairs={{16,32},{48,64},{80,96},{112,128},{144,160},{176,192},{208,224},{3... | collective-permute-start | bytes 12296 | tf_op jit(solution)/shard_map/ppermute | solution.py:279
  91.7 2.5 %rows.1 = (bf16[256,2048]{1,0:T(8,128)(2,1)S(1)}, bf16[16,2048]{1,0:T(8,128)(2,1)S(1)}) custom-call(s32[4]{0:T(128)S(1)} %pad_add_fusion.at_ref, bf16[8,136,128]{2,1,0:T(8,128)(2,1)S(1)} %all-to-all-done.1.mixed_ref, bf16[8,136,128]{2,1,0:T(8,128)(2,1)S(1)} %collective-permute-done.beside_ref, bf16[1024,2048]{1,0:T(8,128)(2,1)S(1)} %copy-done.1, ...), custom_call_target="tpu_custom_call" | custom-call | flops 1000000000 | bytes 6000000 | tf_op jit(solution)/shard_map/rows/pallas_call | solution.py:474
  94.2 4.7 %collective-permute-done.7.far_ref = bf16[1,2048]{1,0:T(2,128)(2,1)S(1)} collective-permute-done((bf16[1,2048]{1,0:T(2,128)(2,1)S(1)}, bf16[1,2048]{1,0:T(2,128)(2,1)S(1)}, u32[]{:S(2)}, u32[]{:S(2)}) %collective-permute-start.7) | collective-permute-done | bytes 4128 | tf_op jit(solution)/shard_map/ppermute | solution.py:279
  98.9 4.7 %ffn.1 = (bf16[8,16,2048]{2,1,0:T(8,128)(2,1)S(1)}, bf16[8,16,2048]{2,1,0:T(8,128)(2,1)S(1)}) custom-call(s32[3]{0:T(128)S(1)} %pad_add_fusion.1.at_ref, bf16[256,2048]{1,0:T(8,128)(2,1)S(1)} %get-tuple-element.18.cells_ref, bf16[1,2048]{1,0:T(2,128)(2,1)S(1)} %collective-permute-done.6.near_ref, bf16[1,2048]{1,0:T(2,128)(2,1)S(1)} %collective-permute-done.7.far_ref, ...), custom_call_target="tpu_custom_call" | custom-call | flops 1300000000 | bytes 6000000 | tf_op jit(solution)/shard_map/ffn/pallas_call | solution.py:494
  103.6 0.1 collective-permute-start.15
  103.7 1.9 %collective-permute-done.15 = bf16[8,16,2048]{2,1,0:T(8,128)(2,1)S(1)} collective-permute-done((bf16[8,16,2048]{2,1,0:T(8,128)(2,1)S(1)}, bf16[8,16,2048]{2,1,0:T(8,128)(2,1)S(1)}, u32[]{:S(2)}, u32[]{:S(2)}) %collective-permute-start.15) | collective-permute-done | bytes 524320 | tf_op jit(solution)/shard_map/ppermute | solution.py:510
  105.6 0.1 add_convert_fusion
  105.8 14.8 %all_to_all.21 = bf16[8,16,2048]{2,1,0:T(8,128)(2,1)S(1)} all-to-all(bf16[8,16,2048]{2,1,0:T(8,128)(2,1)S(1)} %add_convert_fusion), channel_id=1, replica_groups=mesh['z'=8,'yh'=2,'yl'=2,'x'=4,'c'=2] {'yl','x'}, dimensions={0} | all-to-all | bytes 1048576 | tf_op jit(solution)/shard_map/all_to_all | solution.py:512
  120.7 0.7 add_convert_fusion.1
  (31 shorter events, 0.4 us)
Async XLA Ops:
  0.0 70.4 %copy-start.5 = (f32[3,768]{1,0:T(4,128)S(1)}, f32[3,768]{1,0:T(4,128)}, u32[]{:S(2)}) copy-start(f32[3,768]{1,0:T(4,128)} %param.27) | copy-start | bytes 27652
  0.0 70.4 %copy-start.4 = (f32[3,768]{1,0:T(4,128)S(1)}, f32[3,768]{1,0:T(4,128)}, u32[]{:S(2)}) copy-start(f32[3,768]{1,0:T(4,128)} %param.28) | copy-start | bytes 27652
  0.0 80.9 %copy-start.2 = (f32[2048]{0:T(1024)S(1)}, f32[2048]{0:T(1024)}, u32[]{:S(2)}) copy-start(f32[2048]{0:T(1024)} %param.24) | copy-start | bytes 24580
  14.4 14.4 %collective-permute-start.11 = (bf16[256,1152]{1,0:T(8,128)(2,1)S(1)}, bf16[256,1152]{1,0:T(8,128)(2,1)S(1)}, u32[]{:S(2)}, u32[]{:S(2)}) collective-permute-start(bf16[256,1152]{1,0:T(8,128)(2,1)S(1)} %bitcast.18), channel_id=1, source_target_pairs={{0,32},{32,64},{64,96},{96,128},{128,160},{160,192},{192,224},{224... | collective-permute-start | bytes 1769480 | tf_op jit(solution)/shard_map/ppermute | solution.py:23
  17.5 31.1 %collective-permute-start.1 = (bf16[16,2048]{1,0:T(8,128)(2,1)}, bf16[16,2048]{1,0:T(8,128)(2,1)S(1)}, u32[]{:S(2)}, u32[]{:S(2)}) collective-permute-start(bf16[16,2048]{1,0:T(8,128)(2,1)} %param.23), channel_id=1, source_target_pairs={{0,8},{8,0},{1,9},{9,1},{2,10},{10,2},{3,11},{11,3},{4,12},{12,4},... | collective-permute-start | bytes 196616 | tf_op jit(solution)/shard_map/ppermute | solution.py:269
  20.1 24.8 %collective-permute-start.8 = (bf16[256,1152]{1,0:T(8,128)(2,1)S(1)}, bf16[256,1152]{1,0:T(8,128)(2,1)S(1)}, u32[]{:S(2)}, u32[]{:S(2)}) collective-permute-start(bf16[256,1152]{1,0:T(8,128)(2,1)S(1)} %bitcast.19), channel_id=1, source_target_pairs={{0,224},{32,0},{64,32},{96,64},{128,96},{160,128},{192,160},{224,1... | collective-permute-start | bytes 1769480 | tf_op jit(solution)/shard_map/ppermute | solution.py:23
  28.8 16.9 %collective-permute-start.12 = (bf16[256,1152]{1,0:T(8,128)(2,1)S(1)}, bf16[256,1152]{1,0:T(8,128)(2,1)}, u32[]{:S(2)}, u32[]{:S(2)}) collective-permute-start(bf16[256,1152]{1,0:T(8,128)(2,1)S(1)} %collective-permute-done.11.refs_7_), channel_id=1, source_target_pairs={{0,32},{32,64},{64,96},{96,128},{128,160},{160,192},{192,224},{224... | collective-permute-start | bytes 1769480 | tf_op jit(solution)/shard_map/ppermute | solution.py:23
  37.2 17.4 %all-to-all-start = ((bf16[32,8,384]{2,1,0:T(8,128)(2,1)}), bf16[32,8,384]{2,1,0:T(8,128)(2,1)S(1)}, u32[]{:S(2)}, u32[]{:S(2)}) async-start(bf16[32,8,384]{2,1,0:T(8,128)(2,1)} %get-tuple-element.14), calls=%async_computation | async-start | bytes 393216 | tf_op jit(solution)/shard_map/all_to_all | solution.py:228
  45.0 17.6 %collective-permute-start.9 = (bf16[256,1152]{1,0:T(8,128)(2,1)S(1)}, bf16[256,1152]{1,0:T(8,128)(2,1)}, u32[]{:S(2)}, u32[]{:S(2)}) collective-permute-start(bf16[256,1152]{1,0:T(8,128)(2,1)S(1)} %collective-permute-done.8.refs_1_), channel_id=1, source_target_pairs={{0,224},{32,0},{64,32},{96,64},{128,96},{160,128},{192,160},{224,1... | collective-permute-start | bytes 1769480 | tf_op jit(solution)/shard_map/ppermute | solution.py:23
  45.6 17.9 %collective-permute-start.13 = (bf16[256,1152]{1,0:T(8,128)(2,1)}, bf16[256,1152]{1,0:T(8,128)(2,1)}, u32[]{:S(2)}, u32[]{:S(2)}) collective-permute-start(bf16[256,1152]{1,0:T(8,128)(2,1)} %collective-permute-done.12.refs_6_), channel_id=1, source_target_pairs={{0,32},{32,64},{64,96},{96,128},{128,160},{160,192},{192,224},{224... | collective-permute-start | bytes 1769480 | tf_op jit(solution)/shard_map/ppermute | solution.py:23
  49.5 1.4 %collective-permute-start.2 = (bf16[2,16,2048]{2,1,0:T(8,128)(2,1)S(1)}, bf16[2,16,2048]{2,1,0:T(8,128)(2,1)S(1)}, u32[]{:S(2)}, u32[]{:S(2)}) collective-permute-start(bf16[2,16,2048]{2,1,0:T(8,128)(2,1)S(1)} %pad_maximum_fusion.1), channel_id=1, source_target_pairs={{0,1},{1,0},{2,3},{3,2},{4,5},{5,4},{6,7},{7,6},{8,9},{9,8},{10,11... | collective-permute-start | bytes 393224 | tf_op jit(solution)/shard_map/ppermute | solution.py:270
  51.8 18.0 %collective-permute-start.3 = (bf16[4,16,2048]{2,1,0:T(8,128)(2,1)S(1)}, bf16[4,16,2048]{2,1,0:T(8,128)(2,1)S(1)}, u32[]{:S(2)}, u32[]{:S(2)}) collective-permute-start(bf16[4,16,2048]{2,1,0:T(8,128)(2,1)S(1)} %pad_maximum_fusion.r0), channel_id=1, source_target_pairs={{0,6},{2,0},{4,2},{6,4},{1,7},{3,1},{5,3},{7,5},{8,14},{10,8},{12,... | collective-permute-start | bytes 786440 | tf_op jit(solution)/shard_map/ppermute | solution.py:23
  54.6 0.7 copy-start.3
  59.1 11.1 %all-to-all-start.1 = ((bf16[8,136,128]{2,1,0:T(8,128)(2,1)}), bf16[8,136,128]{2,1,0:T(8,128)(2,1)S(1)}, u32[]{:S(2)}, u32[]{:S(2)}) async-start(bf16[8,136,128]{2,1,0:T(8,128)(2,1)} %mixer_out.1), calls=%async_computation.1 | async-start | bytes 557056 | tf_op jit(solution)/shard_map/all_to_all | solution.py:449
  62.6 36.4 %collective-permute-start.10 = (bf16[256,1152]{1,0:T(8,128)(2,1)}, bf16[256,1152]{1,0:T(8,128)(2,1)}, u32[]{:S(2)}, u32[]{:S(2)}) collective-permute-start(bf16[256,1152]{1,0:T(8,128)(2,1)} %collective-permute-done.9.refs_2_), channel_id=1, source_target_pairs={{0,224},{32,0},{64,32},{96,64},{128,96},{160,128},{192,160},{224,1... | collective-permute-start | bytes 1769480 | tf_op jit(solution)/shard_map/ppermute | solution.py:23
  63.5 35.4 %collective-permute-start.14 = (bf16[256,1152]{1,0:T(8,128)(2,1)}, bf16[256,1152]{1,0:T(8,128)(2,1)}, u32[]{:S(2)}, u32[]{:S(2)}) collective-permute-start(bf16[256,1152]{1,0:T(8,128)(2,1)} %collective-permute-done.13.refs_5_), channel_id=1, source_target_pairs={{0,32},{32,64},{64,96},{96,128},{128,160},{160,192},{192,224},{224... | collective-permute-start | bytes 1769480 | tf_op jit(solution)/shard_map/ppermute | solution.py:23
  65.9 10.7 %collective-permute-start.4 = (bf16[4,16,2048]{2,1,0:T(8,128)(2,1)S(1)}, bf16[4,16,2048]{2,1,0:T(8,128)(2,1)S(1)}, u32[]{:S(2)}, u32[]{:S(2)}) collective-permute-start(bf16[4,16,2048]{2,1,0:T(8,128)(2,1)S(1)} %pad_maximum_fusion.r0), channel_id=1, source_target_pairs={{0,4},{2,6},{4,0},{6,2},{1,5},{3,7},{5,1},{7,3},{8,12},{10,14},{12... | collective-permute-start | bytes 786440 | tf_op jit(solution)/shard_map/ppermute | solution.py:23
  69.2 11.6 %collective-permute-start.5 = (bf16[4,16,2048]{2,1,0:T(8,128)(2,1)S(1)}, bf16[4,16,2048]{2,1,0:T(8,128)(2,1)S(1)}, u32[]{:S(2)}, u32[]{:S(2)}) collective-permute-start(bf16[4,16,2048]{2,1,0:T(8,128)(2,1)S(1)} %pad_maximum_fusion.r0), channel_id=1, source_target_pairs={{0,2},{2,4},{4,6},{6,0},{1,3},{3,5},{5,7},{7,1},{8,10},{10,12},{12... | collective-permute-start | bytes 786440 | tf_op jit(solution)/shard_map/ppermute | solution.py:23
  70.3 10.6 %collective-permute-start = (bf16[8,136,128]{2,1,0:T(8,128)(2,1)S(1)}, bf16[8,136,128]{2,1,0:T(8,128)(2,1)S(1)}, u32[]{:S(2)}, u32[]{:S(2)}) collective-permute-start(bf16[8,136,128]{2,1,0:T(8,128)(2,1)S(1)} %all-to-all-done.1.mixed_ref), channel_id=1, source_target_pairs={{0,1},{1,0},{2,3},{3,2},{4,5},{5,4},{6,7},{7,6},{8,9},{9,8},{10,11... | collective-permute-start | bytes 835592 | tf_op jit(solution)/shard_map/ppermute | solution.py:450
  80.9 2.2 %copy-start = (bf16[1024,2048]{1,0:T(8,128)(2,1)S(1)}, bf16[1024,2048]{1,0:T(8,128)(2,1)}, u32[]{:S(2)}) copy-start(bf16[1024,2048]{1,0:T(8,128)(2,1)} %weight_ref.3) | copy-start | bytes 12582916
  83.1 8.6 %copy-start.1 = (bf16[1024,2048]{1,0:T(8,128)(2,1)S(1)}, bf16[1024,2048]{1,0:T(8,128)(2,1)}, u32[]{:S(2)}) copy-start(bf16[1024,2048]{1,0:T(8,128)(2,1)} %weight_ref.3) | copy-start | bytes 12582916
  84.6 9.5 %collective-permute-start.6 = (bf16[1,2048]{1,0:T(2,128)(2,1)S(1)}, bf16[1,2048]{1,0:T(2,128)(2,1)S(1)}, u32[]{:S(2)}, u32[]{:S(2)}) collective-permute-start(bf16[1,2048]{1,0:T(2,128)(2,1)S(1)} %get-tuple-element.19), channel_id=1, source_target_pairs={{0,16},{16,0},{1,17},{17,1},{2,18},{18,2},{3,19},{19,3},{4,20},{20... | collective-permute-start | bytes 12296 | tf_op jit(solution)/shard_map/ppermute | solution.py:280
  89.8 9.1 %collective-permute-start.7 = (bf16[1,2048]{1,0:T(2,128)(2,1)S(1)}, bf16[1,2048]{1,0:T(2,128)(2,1)S(1)}, u32[]{:S(2)}, u32[]{:S(2)}) collective-permute-start(bf16[1,2048]{1,0:T(2,128)(2,1)S(1)} %get-tuple-element.20), channel_id=1, source_target_pairs={{16,32},{48,64},{80,96},{112,128},{144,160},{176,192},{208,224},{3... | collective-permute-start | bytes 12296 | tf_op jit(solution)/shard_map/ppermute | solution.py:279
  103.6 2.0 %collective-permute-start.15 = (bf16[8,16,2048]{2,1,0:T(8,128)(2,1)S(1)}, bf16[8,16,2048]{2,1,0:T(8,128)(2,1)S(1)}, u32[]{:S(2)}, u32[]{:S(2)}) collective-permute-start(bf16[8,16,2048]{2,1,0:T(8,128)(2,1)S(1)} %get-tuple-element.22), channel_id=1, source_target_pairs={{0,1},{1,0},{2,3},{3,2},{4,5},{5,4},{6,7},{7,6},{8,9},{9,8},{10,11... | collective-permute-start | bytes 1572872 | tf_op jit(solution)/shard_map/ppermute | solution.py:510
